TPU v7x, 32 devices: a whole 2x2x4 slice. The times are simulated.
32 devices in a mesh: ep: 4 (over y, x), tp: 8 (over z, core).
Axes of the slice: x: 2, y: 2, z: 4, core: 2. Of those that a mesh axis runs over, the one named last changes fastest.
Arguments:
- stream: bfloat16 [64, 2048], P('ep'), may hold values from -6 to 6
- norm_gain_attn: float32 [2048], replicated, may hold values from 0.1 to 1.9
- w_query: bfloat16 [2048, 2048], P('ep', 'tp'), may hold values from -0.125 to 0.125
- w_key: bfloat16 [2048, 2048], P('ep', 'tp'), may hold values from -0.125 to 0.125
- w_value: bfloat16 [2048, 2048], P('ep', 'tp'), may hold values from -0.125 to 0.125
- w_forget: bfloat16 [2048, 16], replicated, may hold values from -0.125 to 0.125
- forget_bias: float32 [16], replicated, may hold values from -2 to 2
- key_cache: bfloat16 [64, 1024, 2048], P('ep', None, 'tp'), may hold values from -1500 to 1500
- value_cache: bfloat16 [64, 1024, 2048], P('ep', None, 'tp'), may hold values from -6 to 6
- gate_cache: float32 [64, 16, 1024], P('ep', 'tp'), may hold values from -1024 to 0, as said below
- lengths: int32 [64], P('ep'), may hold values from 128 to 1024
- w_output: bfloat16 [2048, 2048], P('tp'), may hold values from -0.125 to 0.125
- norm_gain_ffn: float32 [2048], replicated, may hold values from 0.1 to 1.9
- routes: int32 [64, 2], replicated, may hold values from 0 to 3, all different within a row; in each aligned block of 16 rows (0 to 15, 16 to 31, ...) at most 16 rows name the same one
- route_weights: float32 [64, 2], replicated, may hold values from 0.2 to 1
- w_expert_gate: bfloat16 [4, 2048, 5632], P('ep', None, 'tp'), may hold values from -0.125 to 0.125
- w_expert_up: bfloat16 [4, 2048, 5632], P('ep', None, 'tp'), may hold values from -0.125 to 0.125
- expert_down_weight: bfloat16 [4, 5632, 2048], P('ep', 'tp'), may hold values from -0.078125 to 0.078125
Outputs:
- result: bfloat16 [64, 2048], P('ep', 'tp')
Inputs may be any that keep to these rules, and one draw needn't show every extreme that they name: `gate_cache`: never rises along positions. `routes`: in the rows of one index of ep no expert is named by more than 16 rows, and in some such block one is named by exactly 16.
All inputs are finite; a program needn't handle non-finite values.
Results may differ from a plain program's by a relative error of at most 0.014.
Values may be sent and summed in bfloat16 or wider, within the bound.
No kernel may reach another device: no remote copies, remote signals or barrier semaphores. Data moves between devices by JAX's collectives and lax.ppermute only.
A program may use at most 64 MiB of HBM per device.

v0:
```python
import jax
import jax.numpy as jnp
from jax import lax
from jax.sharding import PartitionSpec as P


def rms_norm(values, gain):
    floats = values.astype(jnp.float32)
    scaled = floats * lax.rsqrt(jnp.mean(floats * floats, axis=-1, keepdims=True) + 1e-06)
    return (scaled * gain).astype(jnp.bfloat16)


def expert_rows(inputs, w_expert_gate, w_expert_up, expert_down_weight):
    hidden = (
        jax.nn.silu(jnp.dot(inputs, w_expert_gate[0], preferred_element_type=jnp.float32))
        * jnp.dot(inputs, w_expert_up[0], preferred_element_type=jnp.float32)
    ).astype(jnp.bfloat16)
    partial_out = jnp.dot(hidden, expert_down_weight[0], preferred_element_type=jnp.float32)
    return lax.psum_scatter(partial_out.astype(jnp.bfloat16), "tp", scatter_dimension=1, tiled=True)


def shards(
    stream,
    norm_gain_attn,
    w_query,
    w_key,
    w_value,
    w_forget,
    forget_bias,
    key_cache,
    value_cache,
    gate_cache,
    lengths,
    w_output,
    norm_gain_ffn,
    routes,
    route_weights,
    w_expert_gate,
    w_expert_up,
    expert_down_weight,
):
    seq_count = stream.shape[0]
    model_width = stream.shape[1]
    groups = lax.axis_size("ep")
    group_index = lax.axis_index("ep")
    width_index = lax.axis_index("tp")
    heads_here = gate_cache.shape[1]
    cache_len = key_cache.shape[1]
    head_dim = key_cache.shape[2] // heads_here
    width_per_device = heads_here * head_dim
    normed = rms_norm(stream, norm_gain_attn)
    spread = lax.all_to_all(normed, "ep", split_axis=1, concat_axis=0, tiled=True)
    stacked = jnp.concatenate([w_query, w_key, w_value], axis=1)
    block = spread
    projected = lax.psum_scatter(
        jnp.dot(block, stacked, preferred_element_type=jnp.float32),
        "ep",
        scatter_dimension=0,
        tiled=True,
    )
    query = (
        projected[:, :width_per_device]
        .astype(jnp.bfloat16)
        .reshape(seq_count, heads_here, head_dim)
    )
    key_new = (
        projected[:, width_per_device : 2 * width_per_device]
        .astype(jnp.bfloat16)
        .reshape(seq_count, heads_here, head_dim)
    )
    value_new = (
        projected[:, 2 * width_per_device :]
        .astype(jnp.bfloat16)
        .reshape(seq_count, heads_here, head_dim)
    )
    forget_all = jax.nn.log_sigmoid(
        jnp.dot(normed, w_forget, preferred_element_type=jnp.float32) + forget_bias
    )
    forget_new = lax.dynamic_slice_in_dim(forget_all, width_index * heads_here, heads_here, 1)
    scale = head_dim ** (-0.5)
    keys = key_cache.reshape(seq_count, cache_len, heads_here, head_dim)
    values = value_cache.reshape(seq_count, cache_len, heads_here, head_dim)
    sequence_indices = jnp.arange(cache_len, dtype=jnp.int32)
    is_live = sequence_indices[None, None, :] < lengths[:, None, None]
    last_gate = jnp.sum(
        jnp.where(sequence_indices[None, None, :] == lengths[:, None, None] - 1, gate_cache, 0.0),
        axis=-1,
    )
    scores = jnp.einsum("shd,sphd->shp", query, keys, preferred_element_type=jnp.float32) * scale
    scores = scores + forget_new[..., None] + last_gate[..., None] - gate_cache
    own_score = (
        jnp.einsum("shd,shd->sh", query, key_new, preferred_element_type=jnp.float32) * scale
    )
    hidden_from_view = jnp.where(is_live, scores, -1e30)
    largest = jnp.maximum(jnp.max(hidden_from_view, axis=-1), own_score)
    past = jnp.exp(hidden_from_view - largest[..., None])
    own_term = jnp.exp(own_score - largest)
    total = jnp.sum(past, axis=-1) + own_term
    past_weights = (past / total[..., None]).astype(jnp.bfloat16)
    own_weights = lax.optimization_barrier((own_term / total).astype(jnp.bfloat16))
    attended = jnp.einsum("shp,sphd->shd", past_weights, values, preferred_element_type=jnp.float32)
    attended = attended + own_weights.astype(jnp.float32)[..., None] * value_new.astype(jnp.float32)
    attended = attended.reshape(seq_count, width_per_device).astype(jnp.bfloat16)
    head_total = lax.psum(
        jnp.dot(attended, w_output, preferred_element_type=jnp.float32).astype(jnp.bfloat16), "tp"
    ).astype(jnp.float32)
    mixed = (stream.astype(jnp.float32) + head_total).astype(jnp.bfloat16)
    normed_ffn = rms_norm(mixed, norm_gain_ffn)
    top_count = routes.shape[1]
    capacity = 2 * seq_count * top_count // groups
    slice_width = model_width // lax.axis_size("tp")
    own_stream = lax.dynamic_slice_in_dim(mixed, width_index * slice_width, slice_width, 1)
    my_routes = lax.dynamic_slice_in_dim(routes, group_index * seq_count, seq_count, 0).reshape(-1)
    my_weights = lax.dynamic_slice_in_dim(route_weights, group_index * seq_count, seq_count, 0)
    expert_ids = jnp.arange(groups, dtype=jnp.int32)
    chosen = (my_routes[:, None] == expert_ids[None, :]).astype(jnp.int32)
    ranking = jnp.sum((jnp.cumsum(chosen, axis=0) - chosen) * chosen, axis=1)
    slot_ids = jnp.arange(capacity, dtype=jnp.int32)
    placed = (chosen[:, :, None] * (ranking[:, None, None] == slot_ids[None, None, :])).astype(
        jnp.float32
    )
    placed = placed.reshape(seq_count, top_count, groups * capacity)
    selector = jnp.sum(placed, axis=1)
    combine_weights = jnp.sum(placed * my_weights[:, :, None], axis=1)
    outgoing = jnp.dot(
        selector.T.astype(jnp.bfloat16), normed_ffn, preferred_element_type=jnp.float32
    )
    outgoing = outgoing.astype(jnp.bfloat16).reshape(groups, capacity, model_width)
    block = lax.all_to_all(outgoing, "ep", split_axis=0, concat_axis=0, tiled=True)
    item_count = block.shape[1]
    answered = expert_rows(
        block.reshape(-1, model_width), w_expert_gate, w_expert_up, expert_down_weight
    )
    answered = answered.reshape(groups, item_count, slice_width)
    returned = lax.all_to_all(answered, "ep", split_axis=0, concat_axis=0, tiled=True)
    expert_out = returned.reshape(groups * capacity, slice_width).astype(jnp.float32)
    combined = jnp.dot(
        combine_weights,
        expert_out,
        precision=lax.Precision.HIGHEST,
        preferred_element_type=jnp.float32,
    )
    return (own_stream.astype(jnp.float32) + combined).astype(jnp.bfloat16)


def solution(mesh):
    placed = (
        P("ep", None),
        P(),
        P("ep", "tp"),
        P("ep", "tp"),
        P("ep", "tp"),
        P(),
        P(),
        P("ep", None, "tp"),
        P("ep", None, "tp"),
        P("ep", "tp", None),
        P("ep"),
        P("tp", None),
        P(),
        P(),
        P(),
        P("ep", None, "tp"),
        P("ep", None, "tp"),
        P("ep", "tp", None),
    )
    return jax.shard_map(
        shards, mesh=mesh, in_specs=placed, out_specs=P("ep", "tp"), check_vma=False
    )
```

profile of v0, /device:TPU:0, one launch (start us, length us, event | category | flops | bytes accessed | tf_op | source)
XLA Modules:
  0.0 187.2 jit_solution(5887981771143218316)
XLA Ops:
  6.5 1.1 fusion.40
  7.7 0.9 fusion.42
  8.6 0.6 copy.52
  9.2 5.2 %all-to-all-start = ((bf16[16,4,512]{2,0,1:T(8,128)(2,1)}), bf16[16,4,512]{2,0,1:T(8,128)(2,1)S(1)}, u32[]{:S(2)}, u32[]{:S(2)}) async-start(bf16[16,4,512]{2,0,1:T(8,128)(2,1)} %bitcast.60), calls=%async_computation | async-start | bytes 131072 | tf_op jit(solution)/shard_map/all_to_all | solution.py:52
  14.4 0.7 constant_dynamic-slice_fusion.2
  15.9 0.8 constant_dynamic-slice_fusion
  16.6 1.0 fusion.71
  17.7 12.3 %copy.35 = bf16[16,1024,256]{1,2,0:T(8,128)(2,1)} copy(bf16[16,1024,256]{2,1,0:T(8,128)(2,1)} %param.25) | data formatting | bytes 16777216 | tf_op jit(solution)/shard_map/reshape | solution.py:81
  30.2 2.0 %fusion.26 = f32[64,768]{1,0:T(8,128)} fusion(bf16[64,512]{1,0:T(8,128)(2,1)S(1)} %bitcast.67, bf16[512,256]{1,0:T(8,128)(2,1)S(1)} %copy-done.5, bf16[512,256]{1,0:T(8,128)(2,1)} %param.21, bf16[512,256]{1,0:T(8,128)(2,1)} %param.20), kind=kOutput, calls=%fused_computation.22 | convolution fusion | flops 52690944 | bytes 1048576 | tf_op jit(solution)/shard_map/dot_general | solution.py:56
  32.4 26.0 %reduce-scatter.3.cloned.1.call-done = f32[16,768]{1,0:T(8,128)} async-done(((f32[64,768]{1,0:T(8,128)}), f32[16,768]{1,0:T(8,128)}) %reduce-scatter.3.cloned.1.call-update) | async-done | bytes 49168 | tf_op jit(solution)/shard_map/reduce_scatter | solution.py:55
  58.4 0.8 convert.6
  59.2 4.6 %fusion.73 = f32[16,2,1,1024]{3,2,1,0:T(1,128)S(1)} fusion(bf16[16,2,128,1]{2,3,1,0:T(2,128)(2,1)S(1)} %reshape.169, bf16[16,1024,2,128]{1,3,2,0:T(8,128)(2,1)} %bitcast.61), kind=kOutput, calls=%fused_computation.98 | convolution fusion | flops 8388608 | bytes 8527872 | tf_op jit(solution)/shard_map/shd,sphd->shp/dot_general | solution.py:89
  64.0 0.4 fusion.72
  64.9 4.7 %fusion.1 = f32[16,2,1,128]{3,2,1,0:T(1,128)S(1)} fusion(bf16[16,2,1024,1]{2,1,0,3:T(2,128)(2,1)S(1)} %fusion.53, bf16[16,1024,256]{2,1,0:T(8,128)(2,1)} %param.26), kind=kOutput, calls=%fused_computation.1 | convolution fusion | flops 8388608 | bytes 8470528 | tf_op jit(solution)/shard_map/shp,sphd->shd/dot_general | solution.py:101
  69.6 0.9 convolution_convert_fusion.1
  70.7 54.7 %all-reduce.2.cloned.1.call-done = bf16[16,2048]{1,0:T(8,128)(2,1)} async-done(((bf16[16,2048]{1,0:T(8,128)(2,1)}), bf16[16,2048]{1,0:T(8,128)(2,1)}) %all-reduce.2.cloned.1.call-update) | async-done | bytes 65552 | tf_op jit(solution)/shard_map/psum | solution.py:104
  125.4 1.0 fusion.37
  126.6 9.2 %all_to_all.29 = bf16[4,16,2048]{2,1,0:T(8,128)(2,1)S(1)} all-to-all(bf16[4,16,2048]{2,1,0:T(8,128)(2,1)S(1)} %bitcast.64), channel_id=1, replica_groups=mesh['ep'=4,'tp'=8] {'ep'}, dimensions={0} | all-to-all | bytes 524288 | tf_op jit(solution)/shard_map/all_to_all | solution.py:129
  135.8 2.8 %fusion.8 = f32[64,704]{1,0:T(8,128)S(1)} fusion(bf16[64,2048]{1,0:T(8,128)(2,1)S(1)} %bitcast.62, bf16[1,2048,704]{1,2,0:T(8,128)(2,1)} %param.33), kind=kOutput, calls=%fused_computation.8 | convolution fusion | flops 184549376 | bytes 3325952 | tf_op jit(solution)/shard_map/dot_general | solution.py:15
  138.6 4.4 %fusion.10 = bf16[64,2048]{1,0:T(8,128)(2,1)} fusion(bf16[1,704,2048]{2,1,0:T(8,128)(2,1)S(1)} %copy-done, bf16[64,2048]{1,0:T(8,128)(2,1)S(1)} %bitcast.63, bf16[1,2048,704]{1,2,0:T(8,128)(2,1)} %param.34, f32[64,704]{1,0:T(8,128)S(1)} %fusion.8), kind=kOutput, calls=%fused_computation.10 | convolution fusion | flops 369500160 | bytes 6471680 | tf_op jit(solution)/shard_map/dot_general | solution.py:18
  143.0 28.6 %reduce-scatter.5.cloned.1.call-done = bf16[64,256]{1,0:T(8,128)(2,1)} async-done(((bf16[64,2048]{1,0:T(8,128)(2,1)}), bf16[64,256]{1,0:T(8,128)(2,1)}) %reduce-scatter.5.cloned.1.call-update) | async-done | bytes 32784 | tf_op jit(solution)/shard_map/reduce_scatter | solution.py:19
  171.6 3.6 %all-to-all-start.2 = ((bf16[4,16,256]{2,1,0:T(8,128)(2,1)}), bf16[4,16,256]{2,1,0:T(8,128)(2,1)S(1)}, u32[]{:S(2)}, u32[]{:S(2)}) async-start(bf16[4,16,256]{2,1,0:T(8,128)(2,1)} %bitcast.69), calls=%async_computation.4 | async-start | bytes 65536 | tf_op jit(solution)/shard_map/all_to_all | solution.py:135
  175.1 4.8 %all-to-all-done.2 = bf16[4,16,256]{2,1,0:T(8,128)(2,1)S(1)} async-done(((bf16[4,16,256]{2,1,0:T(8,128)(2,1)}), bf16[4,16,256]{2,1,0:T(8,128)(2,1)S(1)}, u32[]{:S(2)}, u32[]{:S(2)}) %all-to-all-start.2) | async-done | bytes 32800 | tf_op jit(solution)/shard_map/all_to_all | solution.py:135
  179.9 0.7 fusion.22
  (50 shorter events, 2.3 us)
Async XLA Ops:
  6.5 132.0 %copy-start = (bf16[1,704,2048]{2,1,0:T(8,128)(2,1)S(1)}, bf16[1,704,2048]{2,1,0:T(8,128)(2,1)}, u32[]{:S(2)}) copy-start(bf16[1,704,2048]{2,1,0:T(8,128)(2,1)} %param.35) | copy-start | bytes 8650756
  9.2 21.0 %all-to-all-start = ((bf16[16,4,512]{2,0,1:T(8,128)(2,1)}), bf16[16,4,512]{2,0,1:T(8,128)(2,1)S(1)}, u32[]{:S(2)}, u32[]{:S(2)}) async-start(bf16[16,4,512]{2,0,1:T(8,128)(2,1)} %bitcast.60), calls=%async_computation | async-start | bytes 131072 | tf_op jit(solution)/shard_map/all_to_all | solution.py:52
  14.4 44.0 %reduce-scatter.3.cloned.1.call-start = ((), (), s32[]{:S(2)}) async-start(), calls=%async_computation.5 | async-start | bytes 245760 | tf_op jit(solution)/shard_map/reduce_scatter | solution.py:55
  17.7 12.5 %copy-start.5 = (bf16[512,256]{1,0:T(8,128)(2,1)S(1)}, bf16[512,256]{1,0:T(8,128)(2,1)}, u32[]{:S(2)}) copy-start(bf16[512,256]{1,0:T(8,128)(2,1)} %param.22) | copy-start | bytes 786436
  17.7 14.6 %copy-start.4 = (s32[16]{0:T(128)S(1)}, s32[16]{0:T(128)}, u32[]{:S(2)}) copy-start(s32[16]{0:T(128)} %param.28) | copy-start | bytes 196
  32.2 93.1 %all-reduce.2.cloned.1.call-start = ((), (), s32[]{:S(2)}) async-start(), calls=%async_computation.6 | async-start | bytes 131072 | tf_op jit(solution)/shard_map/psum | solution.py:104
  59.2 4.7 %copy-start.6 = (f32[16,2,1024]{2,1,0:T(2,128)S(1)}, f32[16,2,1024]{2,1,0:T(2,128)}, u32[]{:S(2)}) copy-start(f32[16,2,1024]{2,1,0:T(2,128)} %param.27) | copy-start | bytes 393220
  64.8 4.8 %copy-start.1 = (bf16[256,2048]{1,0:T(8,128)(2,1)S(1)}, bf16[256,2048]{1,0:T(8,128)(2,1)}, u32[]{:S(2)}) copy-start(bf16[256,2048]{1,0:T(8,128)(2,1)} %param.29) | copy-start | bytes 3145732
  64.8 60.5 %copy-start.2 = (bf16[16,2048]{1,0:T(8,128)(2,1)S(1)}, bf16[16,2048]{1,0:T(8,128)(2,1)}, u32[]{:S(2)}) copy-start(bf16[16,2048]{1,0:T(8,128)(2,1)} %param.18) | copy-start | bytes 196612
  64.9 61.5 %copy-start.3 = (f32[2048]{0:T(1024)S(1)}, f32[2048]{0:T(1024)}, u32[]{:S(2)}) copy-start(f32[2048]{0:T(1024)} %param.30) | copy-start | bytes 24580
  70.5 101.0 %reduce-scatter.5.cloned.1.call-start = ((), (), s32[]{:S(2)}) async-start(), calls=%async_computation.7 | async-start | bytes 294912 | tf_op jit(solution)/shard_map/reduce_scatter | solution.py:19
  171.6 8.4 %all-to-all-start.2 = ((bf16[4,16,256]{2,1,0:T(8,128)(2,1)}), bf16[4,16,256]{2,1,0:T(8,128)(2,1)S(1)}, u32[]{:S(2)}, u32[]{:S(2)}) async-start(bf16[4,16,256]{2,1,0:T(8,128)(2,1)} %bitcast.69), calls=%async_computation.4 | async-start | bytes 65536 | tf_op jit(solution)/shard_map/all_to_all | solution.py:135
Sparse Core Ops, SparseCore 0:
  32.4 25.9 reduce-scatter.2
  70.7 54.6 all-reduce.1
  143.1 28.4 reduce-scatter.4
where the time goes:
time: 188 us; the launch traced here: 187 us
  waiting for transfers between devices  114 us (61%)
  matrix products  21.2 us (11%)
  local copies, waits for them, and re-layouts  15 us (8%)
  between operations  13.3 us (7%)
  blocking collectives  9.18 us (5%)
  starting transfers between devices  8.87 us (5%)
  other arithmetic  5.57 us (3%)
    psum x1, waiting for transfers between devices, shards(): lax.psum(jnp.dot(attended, w_output, preferred_element_type=jnp.float32)....  54.7 us
    reduce_scatter x1, waiting for transfers between devices, expert_rows(): lax.psum_scatter(partial_out.astype(jnp.bfloat16), 'tp', scatter_dimensio...  28.6 us
    reduce_scatter x1, waiting for transfers between devices, shards(): lax.psum_scatter(jnp.dot(block, stacked, preferred_element_type=jnp.float...  26 us
    reshape x1, local copies, waits for them, and re-layouts, shards(): keys = key_cache.reshape(seq_count, cache_len, heads_here, head_dim)  12.3 us
    all_to_all x1, blocking collectives, shards(): lax.all_to_all(outgoing, 'ep', split_axis=0, concat_axis=0, tiled=True)  9.18 us
    all_to_all x1, starting transfers between devices, shards(): lax.all_to_all(normed, 'ep', split_axis=1, concat_axis=0, tiled=True)  5.19 us
    all_to_all x1, waiting for transfers between devices, shards(): lax.all_to_all(answered, 'ep', split_axis=0, concat_axis=0, tiled=True)  4.76 us
    dot_general x1, matrix products, shards(): jnp.einsum('shp,sphd->shd', past_weights, values, preferred_element_type=...  4.66 us
  transfers between devices with their start and end apart: 5, of which 4 were waited for; matrix products, arithmetic and copies ran while one was open for 9% of the time, Pallas kernels for 0%

commit v1 on v0

v1 whole, which is shorter than its diff:
```python
import jax
import jax.numpy as jnp
from jax import lax
from jax.experimental import pallas as pl
from jax.experimental.pallas import tpu as pltpu
from jax.sharding import PartitionSpec as P

F32 = jnp.float32
BF16 = jnp.bfloat16
ROWS = 8
STEP = 128
HIDDEN = -1e30


def normalized(floats, gain):
    return floats * lax.rsqrt(jnp.mean(floats * floats, axis=-1, keepdims=True) + 1e-06) * gain


def norm_kernel(stream_ref, gain_ref, out_ref):
    groups, _, width = out_ref.shape
    normed = normalized(stream_ref[...].astype(F32), gain_ref[...]).astype(BF16)
    for group in range(groups):
        out_ref[group] = normed[:, group * width : (group + 1) * width]


def project_kernel(block_ref, query_ref, key_ref, value_ref, out_ref):
    groups, count, features = block_ref.shape
    width = query_ref.shape[1]
    rows = block_ref[...].reshape(groups * count, features)
    for index, weight_ref in enumerate((query_ref, key_ref, value_ref)):
        part = jnp.dot(rows, weight_ref[...], preferred_element_type=F32)
        out_ref[:, :, index * width : (index + 1) * width] = part.reshape(groups, count, width)


def attend_kernel(
    lengths_ref,
    parts_ref,
    normed_ref,
    forget_ref,
    bias_ref,
    gates_ref,
    output_ref,
    keys_hbm,
    values_hbm,
    out_ref,
    keys_ref,
    values_ref,
    attended_ref,
    key_sems,
    value_sems,
):
    groups, count, features = normed_ref.shape
    heads = gates_ref.shape[1]
    cache_len = gates_ref.shape[2]
    width = keys_ref.shape[2]
    head_dim = width // heads
    scale = head_dim ** (-0.5)

    def copy(sequence, source, target, sems):
        live = pl.multiple_of((lengths_ref[sequence] + STEP - 1) // STEP * STEP, STEP)
        rows = pl.ds(0, live)
        return pltpu.make_async_copy(
            source.at[sequence, rows], target.at[sequence, rows], sems.at[sequence]
        )

    def key_copy(sequence):
        return copy(sequence, keys_hbm, keys_ref, key_sems)

    def value_copy(sequence):
        return copy(sequence, values_hbm, values_ref, value_sems)

    for first in range(0, count, ROWS):
        for start_copy in (key_copy, value_copy):
            for sequence in range(first, first + ROWS):
                start_copy(sequence).start()

    def clear(sequence, carry):
        length = lengths_ref[sequence]
        for start in range(STEP, cache_len, STEP):

            @pl.when(start >= length)
            def _():
                values_ref[sequence, start : start + STEP, :] = jnp.zeros((STEP, width), BF16)

        return carry

    lax.fori_loop(0, count, clear, 0)

    forget_sum = jnp.zeros((count, forget_ref.shape[1]), F32)
    for group in range(groups):
        forget_sum += jnp.dot(
            normed_ref[group],
            forget_ref[group * features : (group + 1) * features, :],
            preferred_element_type=F32,
        )
    forget_all = jax.nn.log_sigmoid(forget_sum + bias_ref[...])
    head_ids = lax.broadcasted_iota(jnp.int32, forget_all.shape, 1)
    first_head = lax.axis_index("tp") * heads
    total = parts_ref[0]
    for group in range(1, groups):
        total = total + parts_ref[group]
    query = total[:, :width].astype(BF16).astype(F32)
    key_new = total[:, width : 2 * width].astype(BF16).astype(F32)
    value_new = total[:, 2 * width :].astype(BF16).astype(F32)
    lanes = lax.broadcasted_iota(jnp.int32, (ROWS, width), 1)
    row_ids = lax.broadcasted_iota(jnp.int32, (ROWS, 1), 0)
    positions = lax.broadcasted_iota(jnp.int32, (ROWS, cache_len), 1)

    for first in range(0, count, ROWS):
        mine = slice(first, first + ROWS)
        length = jnp.zeros((ROWS, 1), jnp.int32)
        for row in range(ROWS):
            length = jnp.where(row_ids == row, lengths_ref[first + row], length)
        stacked = jnp.concatenate(
            [
                jnp.where(lanes // head_dim == head, query[mine], 0.0).astype(BF16)
                for head in range(heads)
            ],
            axis=0,
        )
        scores = [jnp.zeros((ROWS, cache_len), F32) for _ in range(heads)]
        for row in range(ROWS):
            key_copy(first + row).wait()
        for row in range(ROWS):
            products = lax.dot_general(
                stacked,
                keys_ref[first + row],
                (((1,), (1,)), ((), ())),
                preferred_element_type=F32,
            )
            for head in range(heads):
                scores[head] = jnp.where(
                    row_ids == row, products[head * ROWS : (head + 1) * ROWS], scores[head]
                )
        weights = []
        owns = []
        for head in range(heads):
            gates = gates_ref[mine, head, :]
            columns = slice(head * head_dim, (head + 1) * head_dim)
            last_gate = jnp.sum(
                jnp.where(positions == length - 1, gates, 0.0), axis=1, keepdims=True
            )
            forget_new = jnp.sum(
                jnp.where(head_ids[mine] == first_head + head, forget_all[mine], 0.0),
                axis=1,
                keepdims=True,
            )
            own_score = (
                jnp.sum(query[mine, columns] * key_new[mine, columns], axis=1, keepdims=True)
                * scale
            )
            score = scores[head] * scale + forget_new + last_gate - gates
            score = jnp.where(positions < length, score, HIDDEN)
            largest = jnp.maximum(jnp.max(score, axis=1, keepdims=True), own_score)
            past = jnp.exp(score - largest)
            own_term = jnp.exp(own_score - largest)
            norm = jnp.sum(past, axis=1, keepdims=True) + own_term
            weights.append((past / norm).astype(BF16))
            owns.append((own_term / norm).astype(BF16).astype(F32))
        weights = jnp.concatenate(weights, axis=0)
        results = [
            owns[head] * value_new[mine, head * head_dim : (head + 1) * head_dim]
            for head in range(heads)
        ]
        for row in range(ROWS):
            value_copy(first + row).wait()
        for row in range(ROWS):
            products = jnp.dot(weights, values_ref[first + row], preferred_element_type=F32)
            for head in range(heads):
                columns = slice(head * head_dim, (head + 1) * head_dim)
                results[head] = results[head] + jnp.where(
                    row_ids == row, products[head * ROWS : (head + 1) * ROWS, columns], 0.0
                )
        for head in range(heads):
            attended_ref[mine, head * head_dim : (head + 1) * head_dim] = results[head]

    attended = attended_ref[...].astype(BF16)
    pieces, _, piece = out_ref.shape
    product = jnp.dot(attended, output_ref[...], preferred_element_type=F32).astype(BF16)
    for index in range(pieces):
        out_ref[index] = product[:, index * piece : (index + 1) * piece]


def mix_kernel(parts_ref, stream_ref, mixed_ref, out_ref):
    pieces, _, piece = parts_ref.shape
    total = parts_ref[0].astype(F32)
    for index in range(1, pieces):
        total = total + parts_ref[index].astype(F32)
    mine = pl.ds(pl.multiple_of(lax.axis_index("tp") * piece, piece), piece)
    mixed = (stream_ref[:, mine].astype(F32) + total).astype(BF16)
    mixed_ref[...] = mixed
    for index in range(out_ref.shape[0]):
        out_ref[index] = mixed


def expert_kernel(
    mixed_ref, gain_ref, routes_ref, weights_ref, gate_ref, up_ref, down_ref, out_ref, rows_ref
):
    total, count, piece = mixed_ref.shape
    width = gate_ref.shape[1]
    pieces = width // piece
    groups = total // pieces
    for group in range(groups):
        blocks = [
            mixed_ref[group * pieces + index].astype(F32) for index in range(pieces)
        ]
        rows_ref[group * count : (group + 1) * count, :] = normalized(
            jnp.concatenate(blocks, axis=1), gain_ref[...]
        ).astype(BF16)
    rows = rows_ref[...]
    gated = jnp.dot(rows, gate_ref[0], preferred_element_type=F32)
    upper = jnp.dot(rows, up_ref[0], preferred_element_type=F32)
    hidden = (gated / (1.0 + jnp.exp(-gated)) * upper).astype(BF16)
    partial = jnp.dot(hidden, down_ref[0], preferred_element_type=F32)
    mine = routes_ref[...] == lax.axis_index("ep")
    share = jnp.sum(jnp.where(mine, weights_ref[...], 0.0), axis=1, keepdims=True)
    partial = (partial * share).astype(BF16)
    for group in range(groups):
        for index in range(pieces):
            out_ref[group * pieces + index] = partial[
                group * count : (group + 1) * count, index * piece : (index + 1) * piece
            ]


def finish_kernel(parts_ref, mixed_ref, out_ref):
    total = mixed_ref[...].astype(F32)
    for index in range(parts_ref.shape[0]):
        total = total + parts_ref[index].astype(F32)
    out_ref[...] = total.astype(BF16)


def shards(
    stream,
    norm_gain_attn,
    w_query,
    w_key,
    w_value,
    w_forget,
    forget_bias,
    key_cache,
    value_cache,
    gate_cache,
    lengths,
    w_output,
    norm_gain_ffn,
    routes,
    route_weights,
    w_expert_gate,
    w_expert_up,
    expert_down_weight,
):
    count, model_width = stream.shape
    groups = lax.axis_size("ep")
    pieces = lax.axis_size("tp")
    piece = model_width // pieces
    cache_len, width = key_cache.shape[1:]
    shape = jax.ShapeDtypeStruct
    in_vmem = pl.BlockSpec(memory_space=pltpu.VMEM)
    in_smem = pl.BlockSpec(memory_space=pltpu.SMEM)
    in_hbm = pl.BlockSpec(memory_space=pltpu.HBM)

    normed = pl.pallas_call(
        norm_kernel, out_shape=shape((groups, count, model_width // groups), BF16), name="norm"
    )(stream, norm_gain_attn.reshape(1, -1))
    block = lax.all_to_all(normed, "ep", 0, 0, tiled=True)
    projected = pl.pallas_call(
        project_kernel, out_shape=shape((groups, count, 3 * width), F32), name="project"
    )(block, w_query, w_key, w_value)
    parts = lax.all_to_all(projected, "ep", 0, 0, tiled=True)
    outputs = pl.pallas_call(
        attend_kernel,
        out_shape=shape((pieces, count, piece), BF16),
        in_specs=[in_smem] + [in_vmem] * 6 + [in_hbm] * 2,
        scratch_shapes=[
            pltpu.VMEM((count, cache_len, width), BF16),
            pltpu.VMEM((count, cache_len, width), BF16),
            pltpu.VMEM((count, width), F32),
            pltpu.SemaphoreType.DMA((count,)),
            pltpu.SemaphoreType.DMA((count,)),
        ],
        name="attend",
    )(
        lengths,
        parts,
        normed,
        w_forget,
        forget_bias.reshape(1, -1),
        gate_cache,
        w_output,
        key_cache,
        value_cache,
    )
    head_parts = lax.all_to_all(outputs, "tp", 0, 0, tiled=True)
    mixed, copies = pl.pallas_call(
        mix_kernel,
        out_shape=(shape((count, piece), BF16), shape((groups * pieces, count, piece), BF16)),
        name="mix",
    )(head_parts, stream)
    mixed_all = lax.all_to_all(copies, ("ep", "tp"), 0, 0, tiled=True)
    expert_parts = pl.pallas_call(
        expert_kernel,
        out_shape=shape((groups * pieces, count, piece), BF16),
        scratch_shapes=[pltpu.VMEM((groups * count, model_width), BF16)],
        name="experts",
    )(
        mixed_all,
        norm_gain_ffn.reshape(1, -1),
        routes,
        route_weights,
        w_expert_gate,
        w_expert_up,
        expert_down_weight,
    )
    returned = lax.all_to_all(expert_parts, ("ep", "tp"), 0, 0, tiled=True)
    return pl.pallas_call(finish_kernel, out_shape=shape((count, piece), BF16), name="finish")(
        returned, mixed
    )


def solution(mesh):
    placed = (
        P("ep", None),
        P(),
        P("ep", "tp"),
        P("ep", "tp"),
        P("ep", "tp"),
        P(),
        P(),
        P("ep", None, "tp"),
        P("ep", None, "tp"),
        P("ep", "tp", None),
        P("ep"),
        P("tp", None),
        P(),
        P(),
        P(),
        P("ep", None, "tp"),
        P("ep", None, "tp"),
        P("ep", "tp", None),
    )
    return jax.shard_map(
        shards, mesh=mesh, in_specs=placed, out_specs=P("ep", "tp"), check_vma=False
    )
```

time: 188 us -> 82.4 us (0.44)
  waiting for transfers between devices: 114 us -> 4.52 us
  blocking collectives: 9.18 us -> 35.9 us
  Pallas kernels: 0 us -> 22.9 us
  matrix products: 21.2 us -> 0 us
  between operations: 13.3 us -> 0.04 us
  other arithmetic: 5.57 us -> 0 us
  local copies, waits for them, and re-layouts: 15 us -> 12 us
  starting transfers between devices: 8.87 us -> 5.95 us
    psum x1 -> x0, waiting for transfers between devices: 54.7 us -> none  [shards(): lax.psum(jnp.dot(attended, w_output, preferred_element_type=jnp.float32)....]
    reduce_scatter x2 -> x0, waiting for transfers between devices: 54.6 us -> none  [the longest x1 28.6 us: expert_rows(): lax.psum_scatter(partial_out.astype(jnp.bfloat16), 'tp', scatter_dimensio...]
    all_to_all x1 -> x3, blocking collectives: 9.18 us -> 35.9 us  [the longest x1 14.7 us: shards(): returned = lax.all_to_all(expert_parts, ('ep', 'tp'), 0, 0, tiled=True)]
    pallas_call x0 -> x6, Pallas kernels: none -> 22.9 us  [the longest x1 9.75 us: shards(): pl.pallas_call(attend_kernel, out_shape=shape((pieces, count, piece), BF1...]
    dot_general x9 -> x0, matrix products: 21.2 us -> none  [the longest x1 4.66 us: shards(): jnp.einsum('shp,sphd->shd', past_weights, values, preferred_element_type=...]
    reshape x4 -> x0, local copies, waits for them, and re-layouts: 12.4 us -> none  [the longest x1 12.3 us: shards(): keys = key_cache.reshape(seq_count, cache_len, heads_here, head_dim)]
    unnamed x14 -> x15, local copies, waits for them, and re-layouts: 0.04 us -> 12 us
    all_to_all x2, starting transfers between devices: 8.78 us -> 5.95 us  [the longest x1 3.36 us: shards(): parts = lax.all_to_all(projected, 'ep', 0, 0, tiled=True)]
  transfers between devices with their start and end apart: 5 -> 2, of which waited for: 4 -> 2; matrix products, arithmetic and copies ran while one was open for 9% -> 13% of each run, Pallas kernels for 0% -> 0%
where the time goes in v1:
time: 82.4 us; the launch traced here: 81.4 us
  blocking collectives  35.9 us (44%)
  Pallas kernels  22.9 us (28%)
  local copies, waits for them, and re-layouts  12 us (15%)
  starting transfers between devices  5.95 us (7%)
  waiting for transfers between devices  4.52 us (5%)
    all_to_all x1, blocking collectives, shards(): returned = lax.all_to_all(expert_parts, ('ep', 'tp'), 0, 0, tiled=True)  14.7 us
    unnamed x15, local copies, waits for them, and re-layouts  12 us
    all_to_all x1, blocking collectives, shards(): head_parts = lax.all_to_all(outputs, 'tp', 0, 0, tiled=True)  11 us
    all_to_all x1, blocking collectives, shards(): block = lax.all_to_all(normed, 'ep', 0, 0, tiled=True)  10.1 us
    pallas_call x1, Pallas kernels, shards(): pl.pallas_call(attend_kernel, out_shape=shape((pieces, count, piece), BF1...  9.75 us
    pallas_call x1, Pallas kernels, shards(): pl.pallas_call(expert_kernel, out_shape=shape((groups * pieces, count, pi...  6.33 us
    all_to_all x1, starting transfers between devices, shards(): parts = lax.all_to_all(projected, 'ep', 0, 0, tiled=True)  3.36 us
    all_to_all x1, waiting for transfers between devices, shards(): parts = lax.all_to_all(projected, 'ep', 0, 0, tiled=True)  3.31 us
  transfers between devices with their start and end apart: 2, of which 2 were waited for; matrix products, arithmetic and copies ran while one was open for 13% of the time, Pallas kernels for 0%

profile of v1, /device:TPU:0, one launch (start us, length us, event | category | flops | bytes accessed | tf_op | source)
XLA Modules:
  0.0 81.4 jit_solution(6363175851676289265)
XLA Ops:
  0.0 1.6 %norm.1.normed_ref = bf16[4,16,512]{2,1,0:T(8,128)(2,1)} custom-call(bf16[16,2048]{1,0:T(8,128)(2,1)} %stream_ref.3, f32[1,2048]{1,0:T(1,128)} %bitcast.3), custom_call_target="tpu_custom_call" | custom-call | tf_op jit(solution)/shard_map/norm/pallas_call | solution.py:262
  1.6 10.1 %all_to_all.25.block_ref = bf16[4,16,512]{2,1,0:T(8,128)(2,1)} all-to-all(bf16[4,16,512]{2,1,0:T(8,128)(2,1)} %norm.1.normed_ref), channel_id=1, replica_groups=mesh['ep'=4,'tp'=8] {'ep'}, dimensions={0} | all-to-all | bytes 131072 | tf_op jit(solution)/shard_map/all_to_all | solution.py:265
  11.7 2.1 %project.1 = f32[4,16,768]{2,1,0:T(8,128)} custom-call(bf16[4,16,512]{2,1,0:T(8,128)(2,1)} %all_to_all.25.block_ref, bf16[512,256]{1,0:T(8,128)(2,1)} %query_ref.1, bf16[512,256]{1,0:T(8,128)(2,1)} %key_ref.1, bf16[512,256]{1,0:T(8,128)(2,1)} %value_ref.1), custom_call_target="tpu_custom_call" | custom-call | tf_op jit(solution)/shard_map/project/pallas_call | solution.py:266
  13.8 3.4 %all-to-all-start.1 = ((f32[4,16,768]{2,1,0:T(8,128)}), f32[4,16,768]{2,1,0:T(8,128)S(1)}, u32[]{:S(2)}, u32[]{:S(2)}) async-start(f32[4,16,768]{2,1,0:T(8,128)} %project.1), calls=%async_computation.1 | async-start | bytes 393216 | tf_op jit(solution)/shard_map/all_to_all | solution.py:269
  17.2 1.8 %copy.19.forget_ref = bf16[2048,16]{1,0:T(8,128)(2,1)} copy(bf16[2048,16]{0,1:T(8,128)(2,1)} %param.23) | data formatting | bytes 131072 | tf_op args[5]
  19.0 3.3 %all-to-all-done.1.parts_ref = f32[4,16,768]{2,1,0:T(8,128)S(1)} async-done(((f32[4,16,768]{2,1,0:T(8,128)}), f32[4,16,768]{2,1,0:T(8,128)S(1)}, u32[]{:S(2)}, u32[]{:S(2)}) %all-to-all-start.1) | async-done | bytes 196640 | tf_op jit(solution)/shard_map/all_to_all | solution.py:269
  22.3 0.0 copy-start.2
  22.3 0.7 copy-done.2
  23.0 9.8 %attend.1 = bf16[8,16,256]{2,1,0:T(8,128)(2,1)} custom-call(s32[16]{0:T(128)} %lengths_ref.1, f32[4,16,768]{2,1,0:T(8,128)} %copy-done.2, bf16[4,16,512]{2,1,0:T(8,128)(2,1)} %norm.1.normed_ref, bf16[2048,16]{1,0:T(8,128)(2,1)} %copy.19.forget_ref, f32[1,16]{1,0:T(1,128)} %bitcast.5, f32[16,2,1024]{2,1,0:T(2,128)} %gates_ref.1, ...), custom_call_target="tpu_custom_call" | custom-call | tf_op jit(solution)/shard_map/attend/pallas_call | solution.py:270
  32.8 11.0 %all_to_all.26.parts_ref = bf16[8,16,256]{2,1,0:T(8,128)(2,1)} all-to-all(bf16[8,16,256]{2,1,0:T(8,128)(2,1)} %attend.1), channel_id=1, replica_groups=mesh['ep'=4,'tp'=8] {'tp'}, dimensions={0} | all-to-all | bytes 131072 | tf_op jit(solution)/shard_map/all_to_all | solution.py:293
  43.8 1.6 %mix.1 = (bf16[16,256]{1,0:T(8,128)(2,1)}, bf16[32,16,256]{2,1,0:T(8,128)(2,1)}) custom-call(bf16[8,16,256]{2,1,0:T(8,128)(2,1)} %all_to_all.26.parts_ref, bf16[16,2048]{1,0:T(8,128)(2,1)} %stream_ref.3), custom_call_target="tpu_custom_call" | custom-call | tf_op jit(solution)/shard_map/mix/pallas_call | solution.py:294
  45.4 2.6 %all-to-all-start.3 = ((bf16[32,16,256]{2,1,0:T(8,128)(2,1)}), bf16[32,16,256]{2,1,0:T(8,128)(2,1)S(1)}, u32[]{:S(2)}, u32[]{:S(2)}) async-start(bf16[32,16,256]{2,1,0:T(8,128)(2,1)} %get-tuple-element.7), calls=%async_computation.3 | async-start | bytes 524288 | tf_op jit(solution)/shard_map/all_to_all | solution.py:299
  48.0 0.0 copy-done.3
  48.0 0.7 copy.20.routes_ref
  48.7 0.0 copy-done.4
  48.7 0.7 copy.21.weights_ref
  49.4 0.0 copy-done
  49.4 2.8 %copy.22.gate_ref = bf16[1,2048,704]{2,1,0:T(8,128)(2,1)} copy(bf16[1,2048,704]{1,2,0:T(8,128)(2,1)S(1)} %copy-done) | data formatting | bytes 5767168 | tf_op args[15]
  52.2 4.6 %copy.23.up_ref = bf16[1,2048,704]{2,1,0:T(8,128)(2,1)} copy(bf16[1,2048,704]{1,2,0:T(8,128)(2,1)} %param.34) | data formatting | bytes 5767168 | tf_op args[16]
  56.8 1.2 %all-to-all-done.3.mixed_ref = bf16[32,16,256]{2,1,0:T(8,128)(2,1)S(1)} async-done(((bf16[32,16,256]{2,1,0:T(8,128)(2,1)}), bf16[32,16,256]{2,1,0:T(8,128)(2,1)S(1)}, u32[]{:S(2)}, u32[]{:S(2)}) %all-to-all-start.3) | async-done | bytes 262176 | tf_op jit(solution)/shard_map/all_to_all | solution.py:299
  58.0 0.7 copy-done.1
  58.7 6.3 %experts.1 = bf16[32,16,256]{2,1,0:T(8,128)(2,1)} custom-call(bf16[32,16,256]{2,1,0:T(8,128)(2,1)} %copy-done.1, f32[1,2048]{1,0:T(1,128)} %bitcast.4, s32[64,2]{1,0:T(8,128)} %copy.20.routes_ref, f32[64,2]{1,0:T(8,128)} %copy.21.weights_ref, bf16[1,2048,704]{2,1,0:T(8,128)(2,1)} %copy.22.gate_ref, bf16[1,2048,704]{2,1,0:T(8,128)(2,1)} %copy.23.up_ref, ...), custom_call_target="tpu_custom_call" | custom-call | tf_op jit(solution)/shard_map/experts/pallas_call | solution.py:300
  65.0 14.7 %all_to_all.27.parts_ref = bf16[32,16,256]{2,1,0:T(8,128)(2,1)} all-to-all(bf16[32,16,256]{2,1,0:T(8,128)(2,1)} %experts.1), channel_id=1, replica_groups=mesh['ep'=4,'tp'=8] {'ep','tp'}, dimensions={0} | all-to-all | bytes 524288 | tf_op jit(solution)/shard_map/all_to_all | solution.py:314
  79.8 1.6 %finish.1 = bf16[16,256]{1,0:T(8,128)(2,1)} custom-call(bf16[32,16,256]{2,1,0:T(8,128)(2,1)} %all_to_all.27.parts_ref, bf16[16,256]{1,0:T(8,128)(2,1)} %get-tuple-element.8.mixed_ref), custom_call_target="tpu_custom_call" | custom-call | tf_op jit(solution)/shard_map/finish/pallas_call | solution.py:315
  (4 shorter events, 0.0 us)
Async XLA Ops:
  13.8 8.5 %all-to-all-start.1 = ((f32[4,16,768]{2,1,0:T(8,128)}), f32[4,16,768]{2,1,0:T(8,128)S(1)}, u32[]{:S(2)}, u32[]{:S(2)}) async-start(f32[4,16,768]{2,1,0:T(8,128)} %project.1), calls=%async_computation.1 | async-start | bytes 393216 | tf_op jit(solution)/shard_map/all_to_all | solution.py:269
  22.3 0.7 copy-start.2
  23.0 25.0 %copy-start.3 = (s32[64,2]{0,1:T(2,128)S(1)}, s32[64,2]{0,1:T(2,128)}, u32[]{:S(2)}) copy-start(s32[64,2]{0,1:T(2,128)} %param.31) | copy-start | bytes 1540
  23.0 25.7 %copy-start.4 = (f32[64,2]{0,1:T(2,128)S(1)}, f32[64,2]{0,1:T(2,128)}, u32[]{:S(2)}) copy-start(f32[64,2]{0,1:T(2,128)} %param.32) | copy-start | bytes 1540
  23.0 26.4 %copy-start = (bf16[1,2048,704]{1,2,0:T(8,128)(2,1)S(1)}, bf16[1,2048,704]{1,2,0:T(8,128)(2,1)}, u32[]{:S(2)}) copy-start(bf16[1,2048,704]{1,2,0:T(8,128)(2,1)} %param.33) | copy-start | bytes 8650756
  45.4 12.6 %all-to-all-start.3 = ((bf16[32,16,256]{2,1,0:T(8,128)(2,1)}), bf16[32,16,256]{2,1,0:T(8,128)(2,1)S(1)}, u32[]{:S(2)}, u32[]{:S(2)}) async-start(bf16[32,16,256]{2,1,0:T(8,128)(2,1)} %get-tuple-element.7), calls=%async_computation.3 | async-start | bytes 524288 | tf_op jit(solution)/shard_map/all_to_all | solution.py:299
  58.0 0.7 copy-start.1

commit v2 on v1

--- a/solution.py
+++ b/solution.py
@@ -8,8 +8,24 @@
 F32 = jnp.float32
 BF16 = jnp.bfloat16
 ROWS = 8
-STEP = 128
 HIDDEN = -1e30
+MIB = 1 << 20
+COVER = 40_000_000_000
+
+
+def call(kernel, name, vmem, outs, flops=0, **options):
+    return pl.pallas_call(
+        kernel,
+        out_shape=outs,
+        name=name,
+        cost_estimate=pl.CostEstimate(flops=flops, transcendentals=0, bytes_accessed=0),
+        compiler_params=pltpu.CompilerParams(vmem_limit_bytes=vmem),
+        **options,
+    )
+
+
+def dot_transposed(left, right):
+    return lax.dot_general(left, right, (((1,), (1,)), ((), ())), preferred_element_type=F32)
 
 
 def normalized(floats, gain):
@@ -40,14 +56,10 @@
     bias_ref,
     gates_ref,
     output_ref,
-    keys_hbm,
-    values_hbm,
-    out_ref,
     keys_ref,
     values_ref,
+    out_ref,
     attended_ref,
-    key_sems,
-    value_sems,
 ):
     groups, count, features = normed_ref.shape
     heads = gates_ref.shape[1]
@@ -56,42 +68,10 @@
     head_dim = width // heads
     scale = head_dim ** (-0.5)
 
-    def copy(sequence, source, target, sems):
-        live = pl.multiple_of((lengths_ref[sequence] + STEP - 1) // STEP * STEP, STEP)
-        rows = pl.ds(0, live)
-        return pltpu.make_async_copy(
-            source.at[sequence, rows], target.at[sequence, rows], sems.at[sequence]
-        )
-
-    def key_copy(sequence):
-        return copy(sequence, keys_hbm, keys_ref, key_sems)
-
-    def value_copy(sequence):
-        return copy(sequence, values_hbm, values_ref, value_sems)
-
-    for first in range(0, count, ROWS):
-        for start_copy in (key_copy, value_copy):
-            for sequence in range(first, first + ROWS):
-                start_copy(sequence).start()
-
-    def clear(sequence, carry):
-        length = lengths_ref[sequence]
-        for start in range(STEP, cache_len, STEP):
-
-            @pl.when(start >= length)
-            def _():
-                values_ref[sequence, start : start + STEP, :] = jnp.zeros((STEP, width), BF16)
-
-        return carry
-
-    lax.fori_loop(0, count, clear, 0)
-
-    forget_sum = jnp.zeros((count, forget_ref.shape[1]), F32)
+    forget_sum = jnp.zeros((count, forget_ref.shape[0]), F32)
     for group in range(groups):
-        forget_sum += jnp.dot(
-            normed_ref[group],
-            forget_ref[group * features : (group + 1) * features, :],
-            preferred_element_type=F32,
+        forget_sum += dot_transposed(
+            normed_ref[group], forget_ref[:, group * features : (group + 1) * features]
         )
     forget_all = jax.nn.log_sigmoid(forget_sum + bias_ref[...])
     head_ids = lax.broadcasted_iota(jnp.int32, forget_all.shape, 1)
@@ -120,14 +100,7 @@
         )
         scores = [jnp.zeros((ROWS, cache_len), F32) for _ in range(heads)]
         for row in range(ROWS):
-            key_copy(first + row).wait()
-        for row in range(ROWS):
-            products = lax.dot_general(
-                stacked,
-                keys_ref[first + row],
-                (((1,), (1,)), ((), ())),
-                preferred_element_type=F32,
-            )
+            products = dot_transposed(stacked, keys_ref[first + row])
             for head in range(heads):
                 scores[head] = jnp.where(
                     row_ids == row, products[head * ROWS : (head + 1) * ROWS], scores[head]
@@ -163,8 +136,6 @@
             for head in range(heads)
         ]
         for row in range(ROWS):
-            value_copy(first + row).wait()
-        for row in range(ROWS):
             products = jnp.dot(weights, values_ref[first + row], preferred_element_type=F32)
             for head in range(heads):
                 columns = slice(head * head_dim, (head + 1) * head_dim)
@@ -197,7 +168,7 @@
     mixed_ref, gain_ref, routes_ref, weights_ref, gate_ref, up_ref, down_ref, out_ref, rows_ref
 ):
     total, count, piece = mixed_ref.shape
-    width = gate_ref.shape[1]
+    width = gate_ref.shape[2]
     pieces = width // piece
     groups = total // pieces
     for group in range(groups):
@@ -208,12 +179,15 @@
             jnp.concatenate(blocks, axis=1), gain_ref[...]
         ).astype(BF16)
     rows = rows_ref[...]
-    gated = jnp.dot(rows, gate_ref[0], preferred_element_type=F32)
-    upper = jnp.dot(rows, up_ref[0], preferred_element_type=F32)
+    gated = dot_transposed(rows, gate_ref[0])
+    upper = dot_transposed(rows, up_ref[0])
     hidden = (gated / (1.0 + jnp.exp(-gated)) * upper).astype(BF16)
     partial = jnp.dot(hidden, down_ref[0], preferred_element_type=F32)
     mine = routes_ref[...] == lax.axis_index("ep")
-    share = jnp.sum(jnp.where(mine, weights_ref[...], 0.0), axis=1, keepdims=True)
+    share = jnp.sum(jnp.where(mine, weights_ref[...], 0.0), axis=0, keepdims=True)
+    square = (groups * count, groups * count)
+    same = lax.broadcasted_iota(jnp.int32, square, 0) == lax.broadcasted_iota(jnp.int32, square, 1)
+    share = jnp.sum(jnp.where(same, share, 0.0), axis=1, keepdims=True)
     partial = (partial * share).astype(BF16)
     for group in range(groups):
         for index in range(pieces):
@@ -253,37 +227,35 @@
     groups = lax.axis_size("ep")
     pieces = lax.axis_size("tp")
     piece = model_width // pieces
-    cache_len, width = key_cache.shape[1:]
+    width = key_cache.shape[2]
     shape = jax.ShapeDtypeStruct
     in_vmem = pl.BlockSpec(memory_space=pltpu.VMEM)
     in_smem = pl.BlockSpec(memory_space=pltpu.SMEM)
-    in_hbm = pl.BlockSpec(memory_space=pltpu.HBM)
-
-    normed = pl.pallas_call(
-        norm_kernel, out_shape=shape((groups, count, model_width // groups), BF16), name="norm"
+
+    normed = call(
+        norm_kernel,
+        "norm",
+        2 * MIB,
+        shape((groups, count, model_width // groups), BF16),
+        flops=COVER,
     )(stream, norm_gain_attn.reshape(1, -1))
     block = lax.all_to_all(normed, "ep", 0, 0, tiled=True)
-    projected = pl.pallas_call(
-        project_kernel, out_shape=shape((groups, count, 3 * width), F32), name="project"
+    projected = call(
+        project_kernel, "project", 4 * MIB, shape((groups, count, 3 * width), F32)
     )(block, w_query, w_key, w_value)
     parts = lax.all_to_all(projected, "ep", 0, 0, tiled=True)
-    outputs = pl.pallas_call(
+    outputs = call(
         attend_kernel,
-        out_shape=shape((pieces, count, piece), BF16),
-        in_specs=[in_smem] + [in_vmem] * 6 + [in_hbm] * 2,
-        scratch_shapes=[
-            pltpu.VMEM((count, cache_len, width), BF16),
-            pltpu.VMEM((count, cache_len, width), BF16),
-            pltpu.VMEM((count, width), F32),
-            pltpu.SemaphoreType.DMA((count,)),
-            pltpu.SemaphoreType.DMA((count,)),
-        ],
-        name="attend",
+        "attend",
+        4 * MIB,
+        shape((pieces, count, piece), BF16),
+        in_specs=[in_smem] + [in_vmem] * 8,
+        scratch_shapes=[pltpu.VMEM((count, width), F32)],
     )(
         lengths,
         parts,
         normed,
-        w_forget,
+        w_forget.T,
         forget_bias.reshape(1, -1),
         gate_cache,
         w_output,
@@ -291,30 +263,30 @@
         value_cache,
     )
     head_parts = lax.all_to_all(outputs, "tp", 0, 0, tiled=True)
-    mixed, copies = pl.pallas_call(
+    mixed, copies = call(
         mix_kernel,
-        out_shape=(shape((count, piece), BF16), shape((groups * pieces, count, piece), BF16)),
-        name="mix",
+        "mix",
+        4 * MIB,
+        (shape((count, piece), BF16), shape((groups * pieces, count, piece), BF16)),
     )(head_parts, stream)
     mixed_all = lax.all_to_all(copies, ("ep", "tp"), 0, 0, tiled=True)
-    expert_parts = pl.pallas_call(
+    expert_parts = call(
         expert_kernel,
-        out_shape=shape((groups * pieces, count, piece), BF16),
+        "experts",
+        8 * MIB,
+        shape((groups * pieces, count, piece), BF16),
         scratch_shapes=[pltpu.VMEM((groups * count, model_width), BF16)],
-        name="experts",
     )(
         mixed_all,
         norm_gain_ffn.reshape(1, -1),
-        routes,
-        route_weights,
-        w_expert_gate,
-        w_expert_up,
+        routes.T,
+        route_weights.T,
+        jnp.swapaxes(w_expert_gate, 1, 2),
+        jnp.swapaxes(w_expert_up, 1, 2),
         expert_down_weight,
     )
     returned = lax.all_to_all(expert_parts, ("ep", "tp"), 0, 0, tiled=True)
-    return pl.pallas_call(finish_kernel, out_shape=shape((count, piece), BF16), name="finish")(
-        returned, mixed
-    )
+    return call(finish_kernel, "finish", 4 * MIB, shape((count, piece), BF16))(returned, mixed)
 
 
 def solution(mesh):

time: 82.4 us -> 64.1 us (0.78)
  blocking collectives: 35.9 us -> 52.9 us
  Pallas kernels: 22.9 us -> 8.15 us
  local copies, waits for them, and re-layouts: 12 us -> 2.26 us
  starting transfers between devices: 5.95 us -> 0 us
  waiting for transfers between devices: 4.52 us -> 0 us
    all_to_all x0 -> x2, blocking collectives: none -> 19.6 us  [the longest x1 11.7 us: shards(): mixed_all = lax.all_to_all(copies, ('ep', 'tp'), 0, 0, tiled=True)]
    pallas_call x6, Pallas kernels: 22.9 us -> 8.15 us  [the longest x1 4.71 us: shards(): call(attend_kernel, 'attend', 4 * MIB, shape((pieces, count, piece), BF16...]
    unnamed x15 -> x42, local copies, waits for them, and re-layouts: 12 us -> 2.26 us
    all_to_all x2 -> x0, starting transfers between devices: 5.95 us -> none  [the longest x1 3.36 us: shards(): parts = lax.all_to_all(projected, 'ep', 0, 0, tiled=True)]
    all_to_all x2 -> x0, waiting for transfers between devices: 4.52 us -> none  [the longest x1 3.31 us: shards(): parts = lax.all_to_all(projected, 'ep', 0, 0, tiled=True)]
    all_to_all x1, blocking collectives: 14.7 us -> 12.6 us  [shards(): returned = lax.all_to_all(expert_parts, ('ep', 'tp'), 0, 0, tiled=True)]
  transfers between devices with their start and end apart: 2 -> 0, of which waited for: 2 -> 0; matrix products, arithmetic and copies ran while one was open for 13% -> 0% of each run, Pallas kernels for 0% -> 0%
where the time goes in v2:
time: 64.1 us; the launch traced here: 63.5 us
  blocking collectives  52.9 us (83%)
  Pallas kernels  8.15 us (13%)
  local copies, waits for them, and re-layouts  2.26 us (4%)
    all_to_all x1, blocking collectives, shards(): returned = lax.all_to_all(expert_parts, ('ep', 'tp'), 0, 0, tiled=True)  12.6 us
    all_to_all x1, blocking collectives, shards(): mixed_all = lax.all_to_all(copies, ('ep', 'tp'), 0, 0, tiled=True)  11.7 us
    all_to_all x1, blocking collectives, shards(): head_parts = lax.all_to_all(outputs, 'tp', 0, 0, tiled=True)  10.6 us
    all_to_all x1, blocking collectives, shards(): block = lax.all_to_all(normed, 'ep', 0, 0, tiled=True)  10.1 us
    all_to_all x1, blocking collectives, shards(): parts = lax.all_to_all(projected, 'ep', 0, 0, tiled=True)  7.91 us
    pallas_call x1, Pallas kernels, shards(): call(attend_kernel, 'attend', 4 * MIB, shape((pieces, count, piece), BF16...  4.71 us
    pallas_call x1, Pallas kernels, shards(): call(expert_kernel, 'experts', 8 * MIB, shape((groups * pieces, count, pi...  2.39 us
    unnamed x42, local copies, waits for them, and re-layouts  2.26 us

profile of v2, /device:TPU:0, one launch (start us, length us, event | category | flops | bytes accessed | tf_op | source)
XLA Modules:
  0.0 63.5 jit_solution(16602198014450379095)
XLA Ops:
  0.0 1.0 %copy-done.9 = bf16[16,2048]{1,0:T(8,128)(2,1)S(1)} copy-done((bf16[16,2048]{1,0:T(8,128)(2,1)S(1)}, bf16[16,2048]{1,0:T(8,128)(2,1)}, u32[]{:S(2)}) %copy-start.9) | copy-done | bytes 65560
  1.0 1.2 %copy-done.16 = f32[2048]{0:T(1024)S(1)} copy-done((f32[2048]{0:T(1024)S(1)}, f32[2048]{0:T(1024)}, u32[]{:S(2)}) %copy-start.16) | copy-done | bytes 8216
  2.2 0.0 slice-start.3
  2.2 0.0 copy-start.3
  2.2 0.0 copy-start.7
  2.2 0.1 norm.1.normed_ref
  2.4 10.1 %all_to_all.25.block_ref = bf16[4,16,512]{2,1,0:T(8,128)(2,1)S(1)} all-to-all(bf16[4,16,512]{2,1,0:T(8,128)(2,1)S(1)} %norm.1.normed_ref), channel_id=1, replica_groups=mesh['ep'=4,'tp'=8] {'ep'}, dimensions={0} | all-to-all | bytes 131072 | tf_op jit(solution)/shard_map/all_to_all | solution.py:242
  12.5 0.0 copy-done.5
  12.5 0.3 project.1
  12.7 7.9 %all_to_all.26.parts_ref = f32[4,16,768]{2,1,0:T(8,128)S(1)} all-to-all(f32[4,16,768]{2,1,0:T(8,128)S(1)} %project.1), channel_id=1, replica_groups=mesh['ep'=4,'tp'=8] {'ep'}, dimensions={0} | all-to-all | bytes 393216 | tf_op jit(solution)/shard_map/all_to_all | solution.py:246
  20.7 0.0 slice-done.2
  20.7 0.0 copy-start.10
  20.8 0.0 copy-start
  20.8 0.0 copy-start.1
  20.8 0.0 copy-start.2
  20.8 0.0 copy-start.11
  20.8 0.0 copy-start.12
  20.8 0.0 copy-start.13
  20.8 4.7 %attend.1 = bf16[8,16,256]{2,1,0:T(8,128)(2,1)S(1)} custom-call(s32[16]{0:T(128)S(1)} %copy-done.14, f32[4,16,768]{2,1,0:T(8,128)S(1)} %all_to_all.26.parts_ref, bf16[4,16,512]{2,1,0:T(8,128)(2,1)S(1)} %norm.1.normed_ref, bf16[16,2048]{1,0:T(8,128)(2,1)S(1)} %bitcast.14, f32[1,16]{1,0:T(1,128)S(1)} %bitcast.18, f32[16,2,1024]{2,1,0:T(2,128)S(1)} %copy-done.7, ...), custom_call_target="tpu_custom_call" | custom-call | tf_op jit(solution)/shard_map/attend/pallas_call | solution.py:247
  25.5 10.6 %all_to_all.27.parts_ref = bf16[8,16,256]{2,1,0:T(8,128)(2,1)S(1)} all-to-all(bf16[8,16,256]{2,1,0:T(8,128)(2,1)S(1)} %attend.1), channel_id=1, replica_groups=mesh['ep'=4,'tp'=8] {'tp'}, dimensions={0} | all-to-all | bytes 131072 | tf_op jit(solution)/shard_map/all_to_all | solution.py:265
  36.2 11.7 %all_to_all.28.mixed_ref = bf16[32,16,256]{2,1,0:T(8,128)(2,1)S(1)} all-to-all(bf16[32,16,256]{2,1,0:T(8,128)(2,1)S(1)} %get-tuple-element.7), channel_id=1, replica_groups=mesh['ep'=4,'tp'=8] {'ep','tp'}, dimensions={0} | all-to-all | bytes 524288 | tf_op jit(solution)/shard_map/all_to_all | solution.py:272
  47.9 2.4 %experts.1 = bf16[32,16,256]{2,1,0:T(8,128)(2,1)S(1)} custom-call(bf16[32,16,256]{2,1,0:T(8,128)(2,1)S(1)} %all_to_all.28.mixed_ref, f32[1,2048]{1,0:T(1,128)S(1)} %bitcast.15, s32[2,64]{1,0:T(2,128)S(1)} %bitcast.16, f32[2,64]{1,0:T(2,128)S(1)} %bitcast.17, bf16[1,704,2048]{2,1,0:T(8,128)(2,1)S(1)} %bitcast.12, bf16[1,704,2048]{2,1,0:T(8,128)(2,1)S(1)} %bitcast.13, ...), custom_call_target="tpu_custom_call" | custom-call | tf_op jit(solution)/shard_map/experts/pallas_call | solution.py:273
  50.3 12.6 %all_to_all.29.parts_ref = bf16[32,16,256]{2,1,0:T(8,128)(2,1)S(1)} all-to-all(bf16[32,16,256]{2,1,0:T(8,128)(2,1)S(1)} %experts.1), channel_id=1, replica_groups=mesh['ep'=4,'tp'=8] {'ep','tp'}, dimensions={0} | all-to-all | bytes 524288 | tf_op jit(solution)/shard_map/all_to_all | solution.py:288
  62.9 0.6 %finish.1 = bf16[16,256]{1,0:T(8,128)(2,1)} custom-call(bf16[32,16,256]{2,1,0:T(8,128)(2,1)S(1)} %all_to_all.29.parts_ref, bf16[16,256]{1,0:T(8,128)(2,1)S(1)} %get-tuple-element.8.mixed_ref), custom_call_target="tpu_custom_call" | custom-call | tf_op jit(solution)/shard_map/finish/pallas_call | solution.py:289
  (31 shorter events, 0.1 us)
Async XLA Ops:
  0.0 20.7 %slice-start = ((s8[8388608]{0:T(1024)(128)(4,1)}), s8[4194304]{0:T(1024)(128)(4,1)S(1)}, s32[]{:S(2)}) async-start(s8[8388608]{0:T(1024)(128)(4,1)} %bitcast.8), calls=%async_computation.5 | async-start | bytes 8388608
  0.0 20.7 %slice-start.2 = ((s8[8388608]{0:T(1024)(128)(4,1)}), s8[4194304]{0:T(1024)(128)(4,1)S(1)}, s32[]{:S(2)}) async-start(s8[8388608]{0:T(1024)(128)(4,1)} %bitcast.10), calls=%async_computation.7 | async-start | bytes 8388608
  0.0 1.0 %copy-start.9 = (bf16[16,2048]{1,0:T(8,128)(2,1)S(1)}, bf16[16,2048]{1,0:T(8,128)(2,1)}, u32[]{:S(2)}) copy-start(bf16[16,2048]{1,0:T(8,128)(2,1)} %stream_ref.3) | copy-start | bytes 196612
  1.0 1.2 %copy-start.16 = (f32[2048]{0:T(1024)S(1)}, f32[2048]{0:T(1024)}, u32[]{:S(2)}) copy-start(f32[2048]{0:T(1024)} %param.19) | copy-start | bytes 24580
  2.2 10.3 %copy-start.4 = (bf16[512,256]{1,0:T(8,128)(2,1)S(1)}, bf16[512,256]{1,0:T(8,128)(2,1)}, u32[]{:S(2)}) copy-start(bf16[512,256]{1,0:T(8,128)(2,1)} %query_ref.1) | copy-start | bytes 786436
  2.2 10.3 %copy-start.5 = (bf16[512,256]{1,0:T(8,128)(2,1)S(1)}, bf16[512,256]{1,0:T(8,128)(2,1)}, u32[]{:S(2)}) copy-start(bf16[512,256]{1,0:T(8,128)(2,1)} %key_ref.1) | copy-start | bytes 786436
  2.2 10.3 %copy-start.6 = (bf16[512,256]{1,0:T(8,128)(2,1)S(1)}, bf16[512,256]{1,0:T(8,128)(2,1)}, u32[]{:S(2)}) copy-start(bf16[512,256]{1,0:T(8,128)(2,1)} %value_ref.1) | copy-start | bytes 786436
  2.2 18.5 %slice-start.1 = ((s8[8388608]{0:T(1024)(128)(4,1)}), s8[4194304]{0:T(1024)(128)(4,1)S(1)}, s32[]{:S(2)}) async-start(s8[8388608]{0:T(1024)(128)(4,1)} %bitcast.8), calls=%async_computation.6 | async-start | bytes 8388608
  2.2 18.5 %slice-start.3 = ((s8[8388608]{0:T(1024)(128)(4,1)}), s8[4194304]{0:T(1024)(128)(4,1)S(1)}, s32[]{:S(2)}) async-start(s8[8388608]{0:T(1024)(128)(4,1)} %bitcast.10), calls=%async_computation.8 | async-start | bytes 8388608
  2.2 18.5 %copy-start.3 = (bf16[256,2048]{1,0:T(8,128)(2,1)S(1)}, bf16[256,2048]{1,0:T(8,128)(2,1)}, u32[]{:S(2)}) copy-start(bf16[256,2048]{1,0:T(8,128)(2,1)} %output_ref.1) | copy-start | bytes 3145732
  2.2 18.5 %copy-start.7 = (f32[16,2,1024]{2,1,0:T(2,128)S(1)}, f32[16,2,1024]{2,1,0:T(2,128)}, u32[]{:S(2)}) copy-start(f32[16,2,1024]{2,1,0:T(2,128)} %gates_ref.1) | copy-start | bytes 393220
  2.2 18.5 %copy-start.8 = (bf16[2048,16]{0,1:T(8,128)(2,1)S(1)}, bf16[2048,16]{0,1:T(8,128)(2,1)}, u32[]{:S(2)}) copy-start(bf16[2048,16]{0,1:T(8,128)(2,1)} %param.23) | copy-start | bytes 196612
  2.2 18.5 %copy-start.14 = (s32[16]{0:T(128)S(1)}, s32[16]{0:T(128)}, u32[]{:S(2)}) copy-start(s32[16]{0:T(128)} %lengths_ref.1) | copy-start | bytes 196
  2.2 18.5 %copy-start.15 = (f32[16]{0:T(128)S(1)}, f32[16]{0:T(128)}, u32[]{:S(2)}) copy-start(f32[16]{0:T(128)} %param.24) | copy-start | bytes 196
  20.7 15.4 %copy-start.10 = (bf16[16,2048]{1,0:T(8,128)(2,1)S(1)}, bf16[16,2048]{1,0:T(8,128)(2,1)}, u32[]{:S(2)}) copy-start(bf16[16,2048]{1,0:T(8,128)(2,1)} %stream_ref.3) | copy-start | bytes 196612
  20.8 27.1 %copy-start = (bf16[1,2048,704]{1,2,0:T(8,128)(2,1)S(1)}, bf16[1,2048,704]{1,2,0:T(8,128)(2,1)}, u32[]{:S(2)}) copy-start(bf16[1,2048,704]{1,2,0:T(8,128)(2,1)} %param.33) | copy-start | bytes 8650756
  20.8 27.1 %copy-start.1 = (bf16[1,2048,704]{1,2,0:T(8,128)(2,1)S(1)}, bf16[1,2048,704]{1,2,0:T(8,128)(2,1)}, u32[]{:S(2)}) copy-start(bf16[1,2048,704]{1,2,0:T(8,128)(2,1)} %param.34) | copy-start | bytes 8650756
  20.8 27.1 %copy-start.2 = (bf16[1,704,2048]{2,1,0:T(8,128)(2,1)S(1)}, bf16[1,704,2048]{2,1,0:T(8,128)(2,1)}, u32[]{:S(2)}) copy-start(bf16[1,704,2048]{2,1,0:T(8,128)(2,1)} %down_ref.1) | copy-start | bytes 8650756
  20.8 27.1 %copy-start.11 = (f32[2048]{0:T(1024)S(1)}, f32[2048]{0:T(1024)}, u32[]{:S(2)}) copy-start(f32[2048]{0:T(1024)} %param.30) | copy-start | bytes 24580
  20.8 27.1 %copy-start.12 = (s32[64,2]{0,1:T(2,128)S(1)}, s32[64,2]{0,1:T(2,128)}, u32[]{:S(2)}) copy-start(s32[64,2]{0,1:T(2,128)} %param.31) | copy-start | bytes 1540
  20.8 27.1 %copy-start.13 = (f32[64,2]{0,1:T(2,128)S(1)}, f32[64,2]{0,1:T(2,128)}, u32[]{:S(2)}) copy-start(f32[64,2]{0,1:T(2,128)} %param.32) | copy-start | bytes 1540

commit v3 on v2

--- a/solution.py
+++ b/solution.py
@@ -1,3 +1,5 @@
+import functools
+
 import jax
 import jax.numpy as jnp
 from jax import lax
@@ -32,25 +34,50 @@
     return floats * lax.rsqrt(jnp.mean(floats * floats, axis=-1, keepdims=True) + 1e-06) * gain
 
 
-def norm_kernel(stream_ref, gain_ref, out_ref):
-    groups, _, width = out_ref.shape
-    normed = normalized(stream_ref[...].astype(F32), gain_ref[...]).astype(BF16)
-    for group in range(groups):
-        out_ref[group] = normed[:, group * width : (group + 1) * width]
-
-
-def project_kernel(block_ref, query_ref, key_ref, value_ref, out_ref):
-    groups, count, features = block_ref.shape
-    width = query_ref.shape[1]
-    rows = block_ref[...].reshape(groups * count, features)
-    for index, weight_ref in enumerate((query_ref, key_ref, value_ref)):
+def exchange(items, axis, paired):
+    if paired:
+        size = len(items)
+        return [items[0]] + [
+            lax.ppermute(items[step], axis, [(one, one ^ step) for one in range(size)])
+            for step in range(1, size)
+        ]
+    received = lax.all_to_all(jnp.stack(items), axis, 0, 0, tiled=True)
+    return [received[index] for index in range(len(items))]
+
+
+def norm_kernel(stream_hbm, gain_hbm, *refs, paired):
+    normed_ref, *out_refs, stream_ref, gain_ref, sems = refs
+    copies = [
+        pltpu.make_async_copy(stream_hbm, stream_ref, sems.at[0]),
+        pltpu.make_async_copy(gain_hbm, gain_ref, sems.at[1]),
+    ]
+    for copy in copies:
+        copy.start()
+    for copy in copies:
+        copy.wait()
+    width = out_refs[0].shape[1]
+    normed_ref[...] = normalized(stream_ref[...].astype(F32), gain_ref[...]).astype(BF16)
+    for index, out_ref in enumerate(out_refs):
+        group = lax.axis_index("ep") ^ index if paired else index
+        out_ref[...] = normed_ref[:, pl.ds(pl.multiple_of(group * width, width), width)]
+
+
+def project_kernel(*refs):
+    groups = (len(refs) - 3) // 2
+    block_refs, weight_refs, out_refs = refs[:groups], refs[groups:-groups], refs[-groups:]
+    count = block_refs[0].shape[0]
+    width = weight_refs[0].shape[1]
+    rows = jnp.concatenate([block_ref[...] for block_ref in block_refs], axis=0)
+    for index, weight_ref in enumerate(weight_refs):
         part = jnp.dot(rows, weight_ref[...], preferred_element_type=F32)
-        out_ref[:, :, index * width : (index + 1) * width] = part.reshape(groups, count, width)
+        for group, out_ref in enumerate(out_refs):
+            out_ref[:, index * width : (index + 1) * width] = part[
+                group * count : (group + 1) * count
+            ]
 
 
 def attend_kernel(
     lengths_ref,
-    parts_ref,
     normed_ref,
     forget_ref,
     bias_ref,
@@ -58,27 +85,24 @@
     output_ref,
     keys_ref,
     values_ref,
-    out_ref,
-    attended_ref,
+    *refs,
 ):
-    groups, count, features = normed_ref.shape
+    *part_refs, out_ref, attended_ref = refs
+    count = normed_ref.shape[0]
     heads = gates_ref.shape[1]
     cache_len = gates_ref.shape[2]
     width = keys_ref.shape[2]
     head_dim = width // heads
     scale = head_dim ** (-0.5)
 
-    forget_sum = jnp.zeros((count, forget_ref.shape[0]), F32)
-    for group in range(groups):
-        forget_sum += dot_transposed(
-            normed_ref[group], forget_ref[:, group * features : (group + 1) * features]
-        )
-    forget_all = jax.nn.log_sigmoid(forget_sum + bias_ref[...])
+    forget_all = jax.nn.log_sigmoid(
+        dot_transposed(normed_ref[...], forget_ref[...]) + bias_ref[...]
+    )
     head_ids = lax.broadcasted_iota(jnp.int32, forget_all.shape, 1)
     first_head = lax.axis_index("tp") * heads
-    total = parts_ref[0]
-    for group in range(1, groups):
-        total = total + parts_ref[group]
+    total = part_refs[0][...]
+    for part_ref in part_refs[1:]:
+        total = total + part_ref[...]
     query = total[:, :width].astype(BF16).astype(F32)
     key_new = total[:, width : 2 * width].astype(BF16).astype(F32)
     value_new = total[:, 2 * width :].astype(BF16).astype(F32)
@@ -154,53 +178,77 @@
 
 def mix_kernel(parts_ref, stream_ref, mixed_ref, out_ref):
     pieces, _, piece = parts_ref.shape
+    half = out_ref.shape[1]
     total = parts_ref[0].astype(F32)
     for index in range(1, pieces):
         total = total + parts_ref[index].astype(F32)
     mine = pl.ds(pl.multiple_of(lax.axis_index("tp") * piece, piece), piece)
-    mixed = (stream_ref[:, mine].astype(F32) + total).astype(BF16)
-    mixed_ref[...] = mixed
+    mixed = stream_ref[:, mine].astype(F32) + total
+    mixed_ref[...] = mixed.astype(BF16)
     for index in range(out_ref.shape[0]):
-        out_ref[index] = mixed
+        core = index % 2
+        out_ref[index] = mixed[core * half : (core + 1) * half].astype(BF16)
 
 
 def expert_kernel(
-    mixed_ref, gain_ref, routes_ref, weights_ref, gate_ref, up_ref, down_ref, out_ref, rows_ref
+    near_ref,
+    far_ref,
+    gain_ref,
+    routes_ref,
+    weights_ref,
+    gate_ref,
+    up_ref,
+    down_ref,
+    keep_ref,
+    give_ref,
+    rows_ref,
 ):
-    total, count, piece = mixed_ref.shape
+    total, half, piece = near_ref.shape
     width = gate_ref.shape[2]
     pieces = width // piece
     groups = total // pieces
-    for group in range(groups):
-        blocks = [
-            mixed_ref[group * pieces + index].astype(F32) for index in range(pieces)
-        ]
-        rows_ref[group * count : (group + 1) * count, :] = normalized(
-            jnp.concatenate(blocks, axis=1), gain_ref[...]
-        ).astype(BF16)
-    rows = rows_ref[...]
+    tokens = 2 * groups * half
+    for side, side_ref in enumerate((near_ref, far_ref)):
+        for group in range(groups):
+            blocks = [side_ref[group * pieces + index].astype(F32) for index in range(pieces)]
+            first = (side * groups + group) * half
+            rows_ref[first : first + half, :] = normalized(
+                jnp.concatenate(blocks, axis=1), gain_ref[...]
+            )
+    rows = rows_ref[...].astype(BF16)
     gated = dot_transposed(rows, gate_ref[0])
     upper = dot_transposed(rows, up_ref[0])
     hidden = (gated / (1.0 + jnp.exp(-gated)) * upper).astype(BF16)
     partial = jnp.dot(hidden, down_ref[0], preferred_element_type=F32)
     mine = routes_ref[...] == lax.axis_index("ep")
     share = jnp.sum(jnp.where(mine, weights_ref[...], 0.0), axis=0, keepdims=True)
-    square = (groups * count, groups * count)
-    same = lax.broadcasted_iota(jnp.int32, square, 0) == lax.broadcasted_iota(jnp.int32, square, 1)
+    row = lax.broadcasted_iota(jnp.int32, (tokens, tokens), 0)
+    core = (row // (groups * half)) ^ (lax.axis_index("tp") % 2)
+    token = row // half % groups * (2 * half) + core * half + row % half
+    same = token == lax.broadcasted_iota(jnp.int32, (tokens, tokens), 1)
     share = jnp.sum(jnp.where(same, share, 0.0), axis=1, keepdims=True)
     partial = (partial * share).astype(BF16)
-    for group in range(groups):
-        for index in range(pieces):
-            out_ref[group * pieces + index] = partial[
-                group * count : (group + 1) * count, index * piece : (index + 1) * piece
-            ]
+    for side, side_ref in enumerate((keep_ref, give_ref)):
+        for group in range(groups):
+            first = (side * groups + group) * half
+            for index in range(pieces):
+                side_ref[group * pieces + index] = partial[
+                    first : first + half, index * piece : (index + 1) * piece
+                ]
+
+
+def pair_kernel(keep_ref, taken_ref, out_ref):
+    out_ref[...] = (keep_ref[...].astype(F32) + taken_ref[...].astype(F32)).astype(BF16)
 
 
 def finish_kernel(parts_ref, mixed_ref, out_ref):
-    total = mixed_ref[...].astype(F32)
-    for index in range(parts_ref.shape[0]):
-        total = total + parts_ref[index].astype(F32)
-    out_ref[...] = total.astype(BF16)
+    half = parts_ref.shape[1]
+    for core in range(2):
+        mine = slice(core * half, (core + 1) * half)
+        total = mixed_ref[...].astype(F32)[mine]
+        for index in range(core, parts_ref.shape[0], 2):
+            total = total + parts_ref[index].astype(F32)
+        out_ref[mine, :] = total.astype(BF16)
 
 
 def shards(
@@ -232,28 +280,37 @@
     in_vmem = pl.BlockSpec(memory_space=pltpu.VMEM)
     in_smem = pl.BlockSpec(memory_space=pltpu.SMEM)
 
-    normed = call(
-        norm_kernel,
+    paired = groups in (2, 4)
+    normed, *blocks = call(
+        functools.partial(norm_kernel, paired=paired),
         "norm",
         2 * MIB,
-        shape((groups, count, model_width // groups), BF16),
+        [shape(stream.shape, BF16)] + [shape((count, model_width // groups), BF16)] * groups,
         flops=COVER,
-    )(stream, norm_gain_attn.reshape(1, -1))
-    block = lax.all_to_all(normed, "ep", 0, 0, tiled=True)
-    projected = call(
-        project_kernel, "project", 4 * MIB, shape((groups, count, 3 * width), F32)
-    )(block, w_query, w_key, w_value)
-    parts = lax.all_to_all(projected, "ep", 0, 0, tiled=True)
+        in_specs=[pl.BlockSpec(memory_space=pltpu.HBM)] * 2,
+        scratch_shapes=[
+            pltpu.VMEM(stream.shape, BF16),
+            pltpu.VMEM((1, model_width), F32),
+            pltpu.SemaphoreType.DMA((2,)),
+        ],
+    )(
+        pltpu.with_memory_space_constraint(stream, pltpu.HBM),
+        pltpu.with_memory_space_constraint(norm_gain_attn.reshape(1, -1), pltpu.HBM),
+    )
+    blocks = exchange(blocks, "ep", paired)
+    parts = call(
+        project_kernel, "project", 4 * MIB, [shape((count, 3 * width), F32)] * groups
+    )(*blocks, w_query, w_key, w_value)
+    parts = exchange(parts, "ep", paired)
     outputs = call(
         attend_kernel,
         "attend",
         4 * MIB,
         shape((pieces, count, piece), BF16),
-        in_specs=[in_smem] + [in_vmem] * 8,
+        in_specs=[in_smem] + [in_vmem] * (7 + groups),
         scratch_shapes=[pltpu.VMEM((count, width), F32)],
     )(
         lengths,
-        parts,
         normed,
         w_forget.T,
         forget_bias.reshape(1, -1),
@@ -261,23 +318,30 @@
         w_output,
         key_cache,
         value_cache,
+        *parts,
     )
     head_parts = lax.all_to_all(outputs, "tp", 0, 0, tiled=True)
+    half = count // 2
+    everyone = ("ep", "tp")
+    slots = groups * pieces
+    swap = [(one, one ^ 1) for one in range(pieces)]
     mixed, copies = call(
         mix_kernel,
         "mix",
         4 * MIB,
-        (shape((count, piece), BF16), shape((groups * pieces, count, piece), BF16)),
+        (shape((count, piece), BF16), shape((slots, half, piece), BF16)),
     )(head_parts, stream)
-    mixed_all = lax.all_to_all(copies, ("ep", "tp"), 0, 0, tiled=True)
-    expert_parts = call(
+    near = lax.all_to_all(copies, everyone, 0, 0, tiled=True)
+    far = lax.ppermute(near, "tp", swap)
+    keep, give = call(
         expert_kernel,
         "experts",
         8 * MIB,
-        shape((groups * pieces, count, piece), BF16),
-        scratch_shapes=[pltpu.VMEM((groups * count, model_width), BF16)],
+        [shape((slots, half, piece), BF16)] * 2,
+        scratch_shapes=[pltpu.VMEM((groups * count, model_width), F32)],
     )(
-        mixed_all,
+        near,
+        far,
         norm_gain_ffn.reshape(1, -1),
         routes.T,
         route_weights.T,
@@ -285,7 +349,9 @@
         jnp.swapaxes(w_expert_up, 1, 2),
         expert_down_weight,
     )
-    returned = lax.all_to_all(expert_parts, ("ep", "tp"), 0, 0, tiled=True)
+    taken = lax.ppermute(give, "tp", swap)
+    summed = call(pair_kernel, "pair", 4 * MIB, shape((slots, half, piece), BF16))(keep, taken)
+    returned = lax.all_to_all(summed, everyone, 0, 0, tiled=True)
     return call(finish_kernel, "finish", 4 * MIB, shape((count, piece), BF16))(returned, mixed)
 
 

time: 64.1 us -> 59.3 us (0.925)
  blocking collectives: 52.9 us -> 32 us
  starting transfers between devices: 0 us -> 8.81 us
  waiting for transfers between devices: 0 us -> 8.79 us
  local copies, waits for them, and re-layouts: 2.26 us -> 0.09 us
  Pallas kernels: 8.15 us -> 9.19 us
    all_to_all x4 -> x2, blocking collectives: 42.3 us -> 21 us  [the longest x1 11.1 us: shards(): near = lax.all_to_all(copies, everyone, 0, 0, tiled=True)]
    ppermute x0 -> x8, starting transfers between devices: none -> 8.81 us  [the longest x6 8.14 us: exchange(): lax.ppermute(items[step], axis, [(one, one ^ step) for one in range(size)])]
    ppermute x0 -> x8, waiting for transfers between devices: none -> 8.79 us  [the longest x6 6.7 us: exchange(): lax.ppermute(items[step], axis, [(one, one ^ step) for one in range(size)])]
    unnamed x42 -> x38, local copies, waits for them, and re-layouts: 2.26 us -> 0.09 us
    pallas_call x4 -> x5, Pallas kernels: 2.8 us -> 3.85 us  [the longest x1 2.4 us: shards(): call(expert_kernel, 'experts', 8 * MIB, [shape((slots, half, piece), BF16...]
  transfers between devices with their start and end apart: 0 -> 8, of which waited for: 0 -> 8; matrix products, arithmetic and copies ran while one was open for 0% -> 0% of each run, Pallas kernels for 0% -> 0%
where the time goes in v3:
time: 59.3 us; the launch traced here: 59.1 us
  blocking collectives  32 us (54%)
  Pallas kernels  9.19 us (15%)
  starting transfers between devices  8.81 us (15%)
  waiting for transfers between devices  8.79 us (15%)
    all_to_all x1, blocking collectives, shards(): near = lax.all_to_all(copies, everyone, 0, 0, tiled=True)  11.1 us
    all_to_all x1, blocking collectives, shards(): head_parts = lax.all_to_all(outputs, 'tp', 0, 0, tiled=True)  11 us
    all_to_all x1, blocking collectives, shards(): returned = lax.all_to_all(summed, everyone, 0, 0, tiled=True)  9.86 us
    ppermute x6, starting transfers between devices, exchange(): lax.ppermute(items[step], axis, [(one, one ^ step) for one in range(size)])  8.14 us
    ppermute x6, waiting for transfers between devices, exchange(): lax.ppermute(items[step], axis, [(one, one ^ step) for one in range(size)])  6.7 us
    pallas_call x1, Pallas kernels, shards(): call(attend_kernel, 'attend', 4 * MIB, shape((pieces, count, piece), BF16...  4.71 us
    pallas_call x1, Pallas kernels, shards(): call(expert_kernel, 'experts', 8 * MIB, [shape((slots, half, piece), BF16...  2.4 us
  transfers between devices with their start and end apart: 8, of which 8 were waited for; matrix products, arithmetic and copies ran while one was open for 0% of the time, Pallas kernels for 0%

profile of v3, /device:TPU:0, one launch (start us, length us, event | category | flops | bytes accessed | tf_op | source)
XLA Modules:
  0.0 59.1 jit_solution(13558244291067219128)
XLA Ops:
  0.1 1.1 %norm.1 = (bf16[16,2048]{1,0:T(8,128)(2,1)S(1)}, bf16[16,512]{1,0:T(8,128)(2,1)S(1)}, bf16[16,512]{1,0:T(8,128)(2,1)S(1)}, bf16[16,512]{1,0:T(8,128)(2,1)S(1)}, bf16[16,512]{1,0:T(8,128)(2,1)S(1)}) custom-call(bf16[16,2048]{1,0:T(8,128)(2,1)} %stream_ref.1, f32[1,2048]{1,0:T(1,128)} %bitcast.19), custom_call_target="tpu_custom_call" | custom-call | flops 40000000000 | tf_op jit(solution)/shard_map/norm/pallas_call | solution.py:284
  1.2 3.0 %collective-permute-start = (bf16[16,512]{1,0:T(8,128)(2,1)S(1)}, bf16[16,512]{1,0:T(8,128)(2,1)S(1)}, u32[]{:S(2)}, u32[]{:S(2)}) collective-permute-start(bf16[16,512]{1,0:T(8,128)(2,1)S(1)} %get-tuple-element.20), channel_id=1, source_target_pairs={{0,8},{8,0},{16,24},{24,16},{1,9},{9,1},{17,25},{25,17},{2,10},{10... | collective-permute-start | bytes 49160 | tf_op jit(solution)/shard_map/ppermute | solution.py:41
  4.3 1.5 %collective-permute-start.1 = (bf16[16,512]{1,0:T(8,128)(2,1)S(1)}, bf16[16,512]{1,0:T(8,128)(2,1)S(1)}, u32[]{:S(2)}, u32[]{:S(2)}) collective-permute-start(bf16[16,512]{1,0:T(8,128)(2,1)S(1)} %get-tuple-element.21), channel_id=1, source_target_pairs={{0,16},{8,24},{16,0},{24,8},{1,17},{9,25},{17,1},{25,9},{2,18},{10... | collective-permute-start | bytes 49160 | tf_op jit(solution)/shard_map/ppermute | solution.py:41
  5.8 0.0 collective-permute-start.2
  5.8 0.2 collective-permute-done.refs_1_
  6.0 2.0 %collective-permute-done.1.refs_2_ = bf16[16,512]{1,0:T(8,128)(2,1)S(1)} collective-permute-done((bf16[16,512]{1,0:T(8,128)(2,1)S(1)}, bf16[16,512]{1,0:T(8,128)(2,1)S(1)}, u32[]{:S(2)}, u32[]{:S(2)}) %collective-permute-start.1) | collective-permute-done | bytes 16416 | tf_op jit(solution)/shard_map/ppermute | solution.py:41
  8.0 2.4 %collective-permute-done.2.refs_3_ = bf16[16,512]{1,0:T(8,128)(2,1)S(1)} collective-permute-done((bf16[16,512]{1,0:T(8,128)(2,1)S(1)}, bf16[16,512]{1,0:T(8,128)(2,1)S(1)}, u32[]{:S(2)}, u32[]{:S(2)}) %collective-permute-start.2) | collective-permute-done | bytes 16416 | tf_op jit(solution)/shard_map/ppermute | solution.py:41
  10.4 0.3 project.1
  10.7 0.6 %collective-permute-start.3 = (f32[16,768]{1,0:T(8,128)S(1)}, f32[16,768]{1,0:T(8,128)S(1)}, u32[]{:S(2)}, u32[]{:S(2)}) collective-permute-start(f32[16,768]{1,0:T(8,128)S(1)} %get-tuple-element.24), channel_id=1, source_target_pairs={{0,8},{8,0},{16,24},{24,16},{1,9},{9,1},{17,25},{25,17},{2,10},{10... | collective-permute-start | bytes 147464 | tf_op jit(solution)/shard_map/ppermute | solution.py:41
  11.3 0.0 collective-permute-start.4
  11.4 2.9 %collective-permute-start.5 = (f32[16,768]{1,0:T(8,128)S(1)}, f32[16,768]{1,0:T(8,128)S(1)}, u32[]{:S(2)}, u32[]{:S(2)}) collective-permute-start(f32[16,768]{1,0:T(8,128)S(1)} %get-tuple-element.26), channel_id=1, source_target_pairs={{0,24},{8,16},{16,8},{24,0},{1,25},{9,17},{17,9},{25,1},{2,26},{10... | collective-permute-start | bytes 147464 | tf_op jit(solution)/shard_map/ppermute | solution.py:41
  14.3 0.6 %collective-permute-done.3.refs_1_ = f32[16,768]{1,0:T(8,128)S(1)} collective-permute-done((f32[16,768]{1,0:T(8,128)S(1)}, f32[16,768]{1,0:T(8,128)S(1)}, u32[]{:S(2)}, u32[]{:S(2)}) %collective-permute-start.3) | collective-permute-done | bytes 49184 | tf_op jit(solution)/shard_map/ppermute | solution.py:41
  14.9 0.5 collective-permute-done.4.refs_2_
  15.4 0.9 %collective-permute-done.5.refs_3_ = f32[16,768]{1,0:T(8,128)S(1)} collective-permute-done((f32[16,768]{1,0:T(8,128)S(1)}, f32[16,768]{1,0:T(8,128)S(1)}, u32[]{:S(2)}, u32[]{:S(2)}) %collective-permute-start.5) | collective-permute-done | bytes 49184 | tf_op jit(solution)/shard_map/ppermute | solution.py:41
  16.5 4.7 %attend.1 = bf16[8,16,256]{2,1,0:T(8,128)(2,1)S(1)} custom-call(s32[16]{0:T(128)S(1)} %copy-done.13, bf16[16,2048]{1,0:T(8,128)(2,1)S(1)} %get-tuple-element.18.normed_ref, bf16[16,2048]{1,0:T(8,128)(2,1)S(1)} %bitcast.14, f32[1,16]{1,0:T(1,128)S(1)} %bitcast.18, f32[16,2,1024]{2,1,0:T(2,128)S(1)} %copy-done.7, bf16[256,2048]{1,0:T(8,128)(2,1)S(1)} %copy-done.3, ...), custom_call_target="tpu_custom_call" | custom-call | tf_op jit(solution)/shard_map/attend/pallas_call | solution.py:305
  21.2 11.0 %all_to_all.15.parts_ref = bf16[8,16,256]{2,1,0:T(8,128)(2,1)S(1)} all-to-all(bf16[8,16,256]{2,1,0:T(8,128)(2,1)S(1)} %attend.1), channel_id=1, replica_groups=mesh['ep'=4,'tp'=8] {'tp'}, dimensions={0} | all-to-all | bytes 131072 | tf_op jit(solution)/shard_map/all_to_all | solution.py:323
  32.3 11.1 %all_to_all.16.near_ref = bf16[32,8,256]{2,1,0:T(8,128)(2,1)S(1)} all-to-all(bf16[32,8,256]{2,1,0:T(8,128)(2,1)S(1)} %get-tuple-element.27), channel_id=1, replica_groups=mesh['ep'=4,'tp'=8] {'ep','tp'}, dimensions={0} | all-to-all | bytes 262144 | tf_op jit(solution)/shard_map/all_to_all | solution.py:334
  43.4 0.3 collective-permute-start.6
  43.7 1.0 %collective-permute-done.6.far_ref = bf16[32,8,256]{2,1,0:T(8,128)(2,1)S(1)} collective-permute-done((bf16[32,8,256]{2,1,0:T(8,128)(2,1)S(1)}, bf16[32,8,256]{2,1,0:T(8,128)(2,1)S(1)}, u32[]{:S(2)}, u32[]{:S(2)}) %collective-permute-start.6) | collective-permute-done | bytes 131104 | tf_op jit(solution)/shard_map/ppermute | solution.py:335
  44.8 2.4 %experts.1 = (bf16[32,8,256]{2,1,0:T(8,128)(2,1)S(1)}, bf16[32,8,256]{2,1,0:T(8,128)(2,1)S(1)}) custom-call(bf16[32,8,256]{2,1,0:T(8,128)(2,1)S(1)} %all_to_all.16.near_ref, bf16[32,8,256]{2,1,0:T(8,128)(2,1)S(1)} %collective-permute-done.6.far_ref, f32[1,2048]{1,0:T(1,128)S(1)} %bitcast.15, s32[2,64]{1,0:T(2,128)S(1)} %bitcast.16, f32[2,64]{1,0:T(2,128)S(1)} %bitcast.17, ...), custom_call_target="tpu_custom_call" | custom-call | tf_op jit(solution)/shard_map/experts/pallas_call | solution.py:336
  47.2 0.4 collective-permute-start.7
  47.6 1.0 %collective-permute-done.7.taken_ref = bf16[32,8,256]{2,1,0:T(8,128)(2,1)S(1)} collective-permute-done((bf16[32,8,256]{2,1,0:T(8,128)(2,1)S(1)}, bf16[32,8,256]{2,1,0:T(8,128)(2,1)S(1)}, u32[]{:S(2)}, u32[]{:S(2)}) %collective-permute-start.7) | collective-permute-done | bytes 131104 | tf_op jit(solution)/shard_map/ppermute | solution.py:352
  48.6 9.9 %all_to_all.17.parts_ref = bf16[32,8,256]{2,1,0:T(8,128)(2,1)S(1)} all-to-all(bf16[32,8,256]{2,1,0:T(8,128)(2,1)S(1)} %pair.1), channel_id=1, replica_groups=mesh['ep'=4,'tp'=8] {'ep','tp'}, dimensions={0} | all-to-all | bytes 262144 | tf_op jit(solution)/shard_map/all_to_all | solution.py:354
  58.5 0.6 %finish.1 = bf16[16,256]{1,0:T(8,128)(2,1)} custom-call(bf16[32,8,256]{2,1,0:T(8,128)(2,1)S(1)} %all_to_all.17.parts_ref, bf16[16,256]{1,0:T(8,128)(2,1)S(1)} %get-tuple-element.30.mixed_ref), custom_call_target="tpu_custom_call" | custom-call | tf_op jit(solution)/shard_map/finish/pallas_call | solution.py:355
  (42 shorter events, 0.1 us)
Async XLA Ops:
  0.0 16.3 %slice-start = ((s8[8388608]{0:T(1024)(128)(4,1)}), s8[4194304]{0:T(1024)(128)(4,1)S(1)}, s32[]{:S(2)}) async-start(s8[8388608]{0:T(1024)(128)(4,1)} %bitcast.8), calls=%async_computation.3 | async-start | bytes 8388608
  0.0 16.3 %slice-start.2 = ((s8[8388608]{0:T(1024)(128)(4,1)}), s8[4194304]{0:T(1024)(128)(4,1)S(1)}, s32[]{:S(2)}) async-start(s8[8388608]{0:T(1024)(128)(4,1)} %bitcast.10), calls=%async_computation.5 | async-start | bytes 8388608
  0.0 16.3 %slice-start.1 = ((s8[8388608]{0:T(1024)(128)(4,1)}), s8[4194304]{0:T(1024)(128)(4,1)S(1)}, s32[]{:S(2)}) async-start(s8[8388608]{0:T(1024)(128)(4,1)} %bitcast.8), calls=%async_computation.4 | async-start | bytes 8388608
  0.0 16.3 %slice-start.3 = ((s8[8388608]{0:T(1024)(128)(4,1)}), s8[4194304]{0:T(1024)(128)(4,1)S(1)}, s32[]{:S(2)}) async-start(s8[8388608]{0:T(1024)(128)(4,1)} %bitcast.10), calls=%async_computation.6 | async-start | bytes 8388608
  0.0 16.3 %copy-start.3 = (bf16[256,2048]{1,0:T(8,128)(2,1)S(1)}, bf16[256,2048]{1,0:T(8,128)(2,1)}, u32[]{:S(2)}) copy-start(bf16[256,2048]{1,0:T(8,128)(2,1)} %output_ref.1) | copy-start | bytes 3145732
  0.0 16.3 %copy-start.7 = (f32[16,2,1024]{2,1,0:T(2,128)S(1)}, f32[16,2,1024]{2,1,0:T(2,128)}, u32[]{:S(2)}) copy-start(f32[16,2,1024]{2,1,0:T(2,128)} %gates_ref.1) | copy-start | bytes 393220
  0.1 16.3 %copy-start.8 = (bf16[2048,16]{0,1:T(8,128)(2,1)S(1)}, bf16[2048,16]{0,1:T(8,128)(2,1)}, u32[]{:S(2)}) copy-start(bf16[2048,16]{0,1:T(8,128)(2,1)} %param.23) | copy-start | bytes 196612
  0.1 16.3 %copy-start.13 = (s32[16]{0:T(128)S(1)}, s32[16]{0:T(128)}, u32[]{:S(2)}) copy-start(s32[16]{0:T(128)} %lengths_ref.1) | copy-start | bytes 196
  0.1 16.3 %copy-start.14 = (f32[16]{0:T(128)S(1)}, f32[16]{0:T(128)}, u32[]{:S(2)}) copy-start(f32[16]{0:T(128)} %param.24) | copy-start | bytes 196
  1.2 4.8 %collective-permute-start = (bf16[16,512]{1,0:T(8,128)(2,1)S(1)}, bf16[16,512]{1,0:T(8,128)(2,1)S(1)}, u32[]{:S(2)}, u32[]{:S(2)}) collective-permute-start(bf16[16,512]{1,0:T(8,128)(2,1)S(1)} %get-tuple-element.20), channel_id=1, source_target_pairs={{0,8},{8,0},{16,24},{24,16},{1,9},{9,1},{17,25},{25,17},{2,10},{10... | collective-permute-start | bytes 49160 | tf_op jit(solution)/shard_map/ppermute | solution.py:41
  4.3 3.7 %collective-permute-start.1 = (bf16[16,512]{1,0:T(8,128)(2,1)S(1)}, bf16[16,512]{1,0:T(8,128)(2,1)S(1)}, u32[]{:S(2)}, u32[]{:S(2)}) collective-permute-start(bf16[16,512]{1,0:T(8,128)(2,1)S(1)} %get-tuple-element.21), channel_id=1, source_target_pairs={{0,16},{8,24},{16,0},{24,8},{1,17},{9,25},{17,1},{25,9},{2,18},{10... | collective-permute-start | bytes 49160 | tf_op jit(solution)/shard_map/ppermute | solution.py:41
  5.8 4.6 %collective-permute-start.2 = (bf16[16,512]{1,0:T(8,128)(2,1)S(1)}, bf16[16,512]{1,0:T(8,128)(2,1)S(1)}, u32[]{:S(2)}, u32[]{:S(2)}) collective-permute-start(bf16[16,512]{1,0:T(8,128)(2,1)S(1)} %get-tuple-element.22), channel_id=1, source_target_pairs={{0,24},{8,16},{16,8},{24,0},{1,25},{9,17},{17,9},{25,1},{2,26},{10... | collective-permute-start | bytes 49160 | tf_op jit(solution)/shard_map/ppermute | solution.py:41
  10.7 4.1 %collective-permute-start.3 = (f32[16,768]{1,0:T(8,128)S(1)}, f32[16,768]{1,0:T(8,128)S(1)}, u32[]{:S(2)}, u32[]{:S(2)}) collective-permute-start(f32[16,768]{1,0:T(8,128)S(1)} %get-tuple-element.24), channel_id=1, source_target_pairs={{0,8},{8,0},{16,24},{24,16},{1,9},{9,1},{17,25},{25,17},{2,10},{10... | collective-permute-start | bytes 147464 | tf_op jit(solution)/shard_map/ppermute | solution.py:41
  11.3 4.1 %collective-permute-start.4 = (f32[16,768]{1,0:T(8,128)S(1)}, f32[16,768]{1,0:T(8,128)S(1)}, u32[]{:S(2)}, u32[]{:S(2)}) collective-permute-start(f32[16,768]{1,0:T(8,128)S(1)} %get-tuple-element.25), channel_id=1, source_target_pairs={{0,16},{8,24},{16,0},{24,8},{1,17},{9,25},{17,1},{25,9},{2,18},{10... | collective-permute-start | bytes 147464 | tf_op jit(solution)/shard_map/ppermute | solution.py:41
  11.4 5.0 %collective-permute-start.5 = (f32[16,768]{1,0:T(8,128)S(1)}, f32[16,768]{1,0:T(8,128)S(1)}, u32[]{:S(2)}, u32[]{:S(2)}) collective-permute-start(f32[16,768]{1,0:T(8,128)S(1)} %get-tuple-element.26), channel_id=1, source_target_pairs={{0,24},{8,16},{16,8},{24,0},{1,25},{9,17},{17,9},{25,1},{2,26},{10... | collective-permute-start | bytes 147464 | tf_op jit(solution)/shard_map/ppermute | solution.py:41
  16.4 15.9 %copy-start.9 = (bf16[16,2048]{1,0:T(8,128)(2,1)S(1)}, bf16[16,2048]{1,0:T(8,128)(2,1)}, u32[]{:S(2)}) copy-start(bf16[16,2048]{1,0:T(8,128)(2,1)} %stream_ref.1) | copy-start | bytes 196612
  16.4 28.3 %copy-start = (bf16[1,2048,704]{1,2,0:T(8,128)(2,1)S(1)}, bf16[1,2048,704]{1,2,0:T(8,128)(2,1)}, u32[]{:S(2)}) copy-start(bf16[1,2048,704]{1,2,0:T(8,128)(2,1)} %param.33) | copy-start | bytes 8650756
  16.5 28.3 %copy-start.1 = (bf16[1,2048,704]{1,2,0:T(8,128)(2,1)S(1)}, bf16[1,2048,704]{1,2,0:T(8,128)(2,1)}, u32[]{:S(2)}) copy-start(bf16[1,2048,704]{1,2,0:T(8,128)(2,1)} %param.34) | copy-start | bytes 8650756
  16.5 28.3 %copy-start.2 = (bf16[1,704,2048]{2,1,0:T(8,128)(2,1)S(1)}, bf16[1,704,2048]{2,1,0:T(8,128)(2,1)}, u32[]{:S(2)}) copy-start(bf16[1,704,2048]{2,1,0:T(8,128)(2,1)} %down_ref.1) | copy-start | bytes 8650756
  16.5 28.3 %copy-start.10 = (f32[2048]{0:T(1024)S(1)}, f32[2048]{0:T(1024)}, u32[]{:S(2)}) copy-start(f32[2048]{0:T(1024)} %param.30) | copy-start | bytes 24580
  16.5 28.3 %copy-start.11 = (s32[64,2]{0,1:T(2,128)S(1)}, s32[64,2]{0,1:T(2,128)}, u32[]{:S(2)}) copy-start(s32[64,2]{0,1:T(2,128)} %param.31) | copy-start | bytes 1540
  16.5 28.3 %copy-start.12 = (f32[64,2]{0,1:T(2,128)S(1)}, f32[64,2]{0,1:T(2,128)}, u32[]{:S(2)}) copy-start(f32[64,2]{0,1:T(2,128)} %param.32) | copy-start | bytes 1540
  43.4 1.3 %collective-permute-start.6 = (bf16[32,8,256]{2,1,0:T(8,128)(2,1)S(1)}, bf16[32,8,256]{2,1,0:T(8,128)(2,1)S(1)}, u32[]{:S(2)}, u32[]{:S(2)}) collective-permute-start(bf16[32,8,256]{2,1,0:T(8,128)(2,1)S(1)} %all_to_all.16.near_ref), channel_id=1, source_target_pairs={{0,1},{1,0},{2,3},{3,2},{4,5},{5,4},{6,7},{7,6},{8,9},{9,8},{10,11... | collective-permute-start | bytes 393224 | tf_op jit(solution)/shard_map/ppermute | solution.py:335
  47.2 1.4 %collective-permute-start.7 = (bf16[32,8,256]{2,1,0:T(8,128)(2,1)S(1)}, bf16[32,8,256]{2,1,0:T(8,128)(2,1)S(1)}, u32[]{:S(2)}, u32[]{:S(2)}) collective-permute-start(bf16[32,8,256]{2,1,0:T(8,128)(2,1)S(1)} %get-tuple-element.29), channel_id=1, source_target_pairs={{0,1},{1,0},{2,3},{3,2},{4,5},{5,4},{6,7},{7,6},{8,9},{9,8},{10,11... | collective-permute-start | bytes 393224 | tf_op jit(solution)/shard_map/ppermute | solution.py:352
  (3 other events, 31.3 us)

commit v4 on v3

--- a/solution.py
+++ b/solution.py
@@ -34,15 +34,26 @@
     return floats * lax.rsqrt(jnp.mean(floats * floats, axis=-1, keepdims=True) + 1e-06) * gain
 
 
-def exchange(items, axis, paired):
+def exchange(items, axis, paired, stride=1):
+    size = len(items)
     if paired:
-        size = len(items)
         return [items[0]] + [
-            lax.ppermute(items[step], axis, [(one, one ^ step) for one in range(size)])
+            lax.ppermute(
+                items[step], axis, [(one, one ^ step * stride) for one in range(size * stride)]
+            )
             for step in range(1, size)
         ]
-    received = lax.all_to_all(jnp.stack(items), axis, 0, 0, tiled=True)
-    return [received[index] for index in range(len(items))]
+    members = [list(range(first, size * stride, stride)) for first in range(stride)]
+    received = lax.all_to_all(
+        jnp.stack(items), axis, 0, 0, tiled=True, axis_index_groups=members
+    )
+    return [received[index] for index in range(size)]
+
+
+def tree_sum(parts):
+    while len(parts) > 1:
+        parts = [left + right for left, right in zip(parts[::2], parts[1::2], strict=True)]
+    return parts[0]
 
 
 def norm_kernel(stream_hbm, gain_hbm, *refs, paired):
@@ -87,7 +98,7 @@
     values_ref,
     *refs,
 ):
-    *part_refs, out_ref, attended_ref = refs
+    *part_refs, keep_ref, give_ref, attended_ref, product_ref = refs
     count = normed_ref.shape[0]
     heads = gates_ref.shape[1]
     cache_len = gates_ref.shape[2]
@@ -170,75 +181,71 @@
             attended_ref[mine, head * head_dim : (head + 1) * head_dim] = results[head]
 
     attended = attended_ref[...].astype(BF16)
-    pieces, _, piece = out_ref.shape
-    product = jnp.dot(attended, output_ref[...], preferred_element_type=F32).astype(BF16)
-    for index in range(pieces):
-        out_ref[index] = product[:, index * piece : (index + 1) * piece]
-
-
-def mix_kernel(parts_ref, stream_ref, mixed_ref, out_ref):
-    pieces, _, piece = parts_ref.shape
+    half = keep_ref.shape[1]
+    core = lax.axis_index("tp") % 2
+    product_ref[...] = jnp.dot(attended, output_ref[...], preferred_element_type=F32)
+    keep_ref[...] = product_ref[:, pl.ds(pl.multiple_of(core * half, half), half)]
+    give_ref[...] = product_ref[:, pl.ds(pl.multiple_of((1 - core) * half, half), half)].astype(
+        BF16
+    )
+
+
+def pair_kernel(keep_ref, taken_ref, out_ref):
+    out_ref[...] = (keep_ref[...].astype(F32) + taken_ref[...].astype(F32)).astype(BF16)
+
+
+def mix_kernel(stream_ref, *refs):
+    *part_refs, out_ref = refs
     half = out_ref.shape[1]
-    total = parts_ref[0].astype(F32)
-    for index in range(1, pieces):
-        total = total + parts_ref[index].astype(F32)
-    mine = pl.ds(pl.multiple_of(lax.axis_index("tp") * piece, piece), piece)
-    mixed = stream_ref[:, mine].astype(F32) + total
-    mixed_ref[...] = mixed.astype(BF16)
-    for index in range(out_ref.shape[0]):
-        core = index % 2
-        out_ref[index] = mixed[core * half : (core + 1) * half].astype(BF16)
+    total = tree_sum([part_ref[...].astype(F32) for part_ref in part_refs])
+    mine = pl.ds(pl.multiple_of(lax.axis_index("tp") % 2 * half, half), half)
+    out_ref[...] = (stream_ref[:, mine].astype(F32) + total).astype(BF16)
+
+
+def second_norm_kernel(near_ref, far_ref, gain_ref, normed_ref, mixed_ref, row_ref):
+    half = near_ref.shape[1]
+    piece = mixed_ref.shape[1]
+    place = lax.axis_index("tp")
+    row_ref[:, pl.ds(pl.multiple_of(place % 2 * half, half), half)] = near_ref[...].astype(F32)
+    row_ref[:, pl.ds(pl.multiple_of((1 - place % 2) * half, half), half)] = far_ref[...].astype(
+        F32
+    )
+    normed_ref[...] = normalized(row_ref[...], gain_ref[...]).astype(BF16)
+    mixed_ref[...] = row_ref[:, pl.ds(pl.multiple_of(place * piece, piece), piece)].astype(BF16)
 
 
 def expert_kernel(
-    near_ref,
-    far_ref,
-    gain_ref,
-    routes_ref,
-    weights_ref,
-    gate_ref,
-    up_ref,
-    down_ref,
-    keep_ref,
-    give_ref,
-    rows_ref,
+    routes_ref, weights_ref, gate_ref, up_ref, down_ref, *refs, groups, paired
 ):
-    total, half, piece = near_ref.shape
-    width = gate_ref.shape[2]
-    pieces = width // piece
-    groups = total // pieces
-    tokens = 2 * groups * half
-    for side, side_ref in enumerate((near_ref, far_ref)):
-        for group in range(groups):
-            blocks = [side_ref[group * pieces + index].astype(F32) for index in range(pieces)]
-            first = (side * groups + group) * half
-            rows_ref[first : first + half, :] = normalized(
-                jnp.concatenate(blocks, axis=1), gain_ref[...]
-            )
-    rows = rows_ref[...].astype(BF16)
+    row_refs, (keep_ref, give_ref) = refs[:groups], refs[groups:]
+    count = row_refs[0].shape[0]
+    piece = keep_ref.shape[2]
+    pieces = keep_ref.shape[0] // groups
+    half = count // 2
+    expert = lax.axis_index("ep")
+    rows = jnp.concatenate([row_ref[...] for row_ref in row_refs], axis=0)
     gated = dot_transposed(rows, gate_ref[0])
     upper = dot_transposed(rows, up_ref[0])
     hidden = (gated / (1.0 + jnp.exp(-gated)) * upper).astype(BF16)
     partial = jnp.dot(hidden, down_ref[0], preferred_element_type=F32)
-    mine = routes_ref[...] == lax.axis_index("ep")
-    share = jnp.sum(jnp.where(mine, weights_ref[...], 0.0), axis=0, keepdims=True)
-    row = lax.broadcasted_iota(jnp.int32, (tokens, tokens), 0)
-    core = (row // (groups * half)) ^ (lax.axis_index("tp") % 2)
-    token = row // half % groups * (2 * half) + core * half + row % half
-    same = token == lax.broadcasted_iota(jnp.int32, (tokens, tokens), 1)
+    share = jnp.sum(jnp.where(routes_ref[...] == expert, weights_ref[...], 0.0), axis=0, keepdims=True)
+    square = (groups * count, groups * count)
+    row = lax.broadcasted_iota(jnp.int32, square, 0)
+    group = row // count ^ expert if paired else row // count
+    same = group * count + row % count == lax.broadcasted_iota(jnp.int32, square, 1)
     share = jnp.sum(jnp.where(same, share, 0.0), axis=1, keepdims=True)
-    partial = (partial * share).astype(BF16)
-    for side, side_ref in enumerate((keep_ref, give_ref)):
-        for group in range(groups):
-            first = (side * groups + group) * half
-            for index in range(pieces):
-                side_ref[group * pieces + index] = partial[
-                    first : first + half, index * piece : (index + 1) * piece
-                ]
-
-
-def pair_kernel(keep_ref, taken_ref, out_ref):
-    out_ref[...] = (keep_ref[...].astype(F32) + taken_ref[...].astype(F32)).astype(BF16)
+    partial = partial * share
+    first_core = lax.axis_index("tp") % 2 == 0
+    for index in range(groups):
+        lower = partial[index * count : index * count + half]
+        upper = partial[index * count + half : (index + 1) * count]
+        keep = jnp.where(first_core, lower, upper).astype(BF16)
+        give = jnp.where(first_core, upper, lower).astype(BF16)
+        group = expert ^ index if paired else index
+        for step in range(pieces):
+            columns = slice(step * piece, (step + 1) * piece)
+            keep_ref[group * pieces + step] = keep[:, columns]
+            give_ref[group * pieces + step] = give[:, columns]
 
 
 def finish_kernel(parts_ref, mixed_ref, out_ref):
@@ -302,13 +309,15 @@
         project_kernel, "project", 4 * MIB, [shape((count, 3 * width), F32)] * groups
     )(*blocks, w_query, w_key, w_value)
     parts = exchange(parts, "ep", paired)
-    outputs = call(
+    swap = [(one, one ^ 1) for one in range(pieces)]
+    side = shape((count, model_width // 2), BF16)
+    keep, give = call(
         attend_kernel,
         "attend",
         4 * MIB,
-        shape((pieces, count, piece), BF16),
+        [shape(side.shape, F32), side],
         in_specs=[in_smem] + [in_vmem] * (7 + groups),
-        scratch_shapes=[pltpu.VMEM((count, width), F32)],
+        scratch_shapes=[pltpu.VMEM((count, width), F32), pltpu.VMEM((count, model_width), F32)],
     )(
         lengths,
         normed,
@@ -320,38 +329,37 @@
         value_cache,
         *parts,
     )
-    head_parts = lax.all_to_all(outputs, "tp", 0, 0, tiled=True)
+    taken = lax.ppermute(give, "tp", swap)
+    pair = call(pair_kernel, "pair", MIB, side)(keep, taken)
+    chips = pieces // 2
+    pair_parts = exchange([pair] * chips, "tp", chips in (2, 4), 2)
+    near = call(mix_kernel, "mix", 2 * MIB, side)(stream, *pair_parts)
+    far = lax.ppermute(near, "tp", swap)
+    rows, mixed = call(
+        second_norm_kernel,
+        "second_norm",
+        2 * MIB,
+        [shape(stream.shape, BF16), shape((count, piece), BF16)],
+        scratch_shapes=[pltpu.VMEM(stream.shape, F32)],
+    )(near, far, norm_gain_ffn.reshape(1, -1))
     half = count // 2
-    everyone = ("ep", "tp")
     slots = groups * pieces
-    swap = [(one, one ^ 1) for one in range(pieces)]
-    mixed, copies = call(
-        mix_kernel,
-        "mix",
-        4 * MIB,
-        (shape((count, piece), BF16), shape((slots, half, piece), BF16)),
-    )(head_parts, stream)
-    near = lax.all_to_all(copies, everyone, 0, 0, tiled=True)
-    far = lax.ppermute(near, "tp", swap)
     keep, give = call(
-        expert_kernel,
+        functools.partial(expert_kernel, groups=groups, paired=paired),
         "experts",
         8 * MIB,
         [shape((slots, half, piece), BF16)] * 2,
-        scratch_shapes=[pltpu.VMEM((groups * count, model_width), F32)],
     )(
-        near,
-        far,
-        norm_gain_ffn.reshape(1, -1),
         routes.T,
         route_weights.T,
         jnp.swapaxes(w_expert_gate, 1, 2),
         jnp.swapaxes(w_expert_up, 1, 2),
         expert_down_weight,
+        *exchange([rows] * groups, "ep", paired),
     )
     taken = lax.ppermute(give, "tp", swap)
-    summed = call(pair_kernel, "pair", 4 * MIB, shape((slots, half, piece), BF16))(keep, taken)
-    returned = lax.all_to_all(summed, everyone, 0, 0, tiled=True)
+    summed = call(pair_kernel, "sides", 4 * MIB, shape((slots, half, piece), BF16))(keep, taken)
+    returned = lax.all_to_all(summed, ("ep", "tp"), 0, 0, tiled=True)
     return call(finish_kernel, "finish", 4 * MIB, shape((count, piece), BF16))(returned, mixed)
 
 

time: 59.3 us -> 56.1 us (0.946)
  blocking collectives: 32 us -> 11.3 us
  waiting for transfers between devices: 8.79 us -> 18.3 us
  starting transfers between devices: 8.81 us -> 16.7 us
    all_to_all x3 -> x1, blocking collectives: 32 us -> 11.3 us  [shards(): returned = lax.all_to_all(summed, ('ep', 'tp'), 0, 0, tiled=True)]
    ppermute x6 -> x12, starting transfers between devices: 8.14 us -> 16.5 us  [exchange(): lax.ppermute(items[step], axis, [(one, one ^ step * stride) for one in ra...]
    ppermute x6 -> x12, waiting for transfers between devices: 6.7 us -> 14.6 us  [exchange(): lax.ppermute(items[step], axis, [(one, one ^ step * stride) for one in ra...]
    ppermute x1 -> x2, waiting for transfers between devices: 1.04 us -> 2.53 us  [shards(): taken = lax.ppermute(give, 'tp', swap)]
    pallas_call x4 -> x6, Pallas kernels: 7.17 us -> 7.28 us  [the longest x1 4.73 us: shards(): call(attend_kernel, 'attend', 4 * MIB, [shape(side.shape, F32), side], in...]
  transfers between devices with their start and end apart: 8 -> 15, of which waited for: 8 -> 14; matrix products, arithmetic and copies ran while one was open for 0% -> 0% of each run, Pallas kernels for 0% -> 0%
where the time goes in v4:
time: 56.1 us; the launch traced here: 56 us
  waiting for transfers between devices  18.3 us (33%)
  starting transfers between devices  16.7 us (30%)
  blocking collectives  11.3 us (20%)
  Pallas kernels  9.3 us (17%)
    ppermute x12, starting transfers between devices, exchange(): lax.ppermute(items[step], axis, [(one, one ^ step * stride) for one in ra...  16.5 us
    ppermute x12, waiting for transfers between devices, exchange(): lax.ppermute(items[step], axis, [(one, one ^ step * stride) for one in ra...  14.6 us
    all_to_all x1, blocking collectives, shards(): returned = lax.all_to_all(summed, ('ep', 'tp'), 0, 0, tiled=True)  11.3 us
    pallas_call x1, Pallas kernels, shards(): call(attend_kernel, 'attend', 4 * MIB, [shape(side.shape, F32), side], in...  4.73 us
    ppermute x2, waiting for transfers between devices, shards(): taken = lax.ppermute(give, 'tp', swap)  2.53 us
    pallas_call x1, Pallas kernels, shards(): call(functools.partial(expert_kernel, groups=groups, paired=paired), 'exp...  2.35 us
    ppermute x1, waiting for transfers between devices, shards(): far = lax.ppermute(near, 'tp', swap)  1.19 us
    pallas_call x1, Pallas kernels, shards(): call(functools.partial(norm_kernel, paired=paired), 'norm', 2 * MIB, [sha...  1.13 us
  transfers between devices with their start and end apart: 15, of which 14 were waited for; matrix products, arithmetic and copies ran while one was open for 0% of the time, Pallas kernels for 0%

profile of v4, /device:TPU:0, one launch (start us, length us, event | category | flops | bytes accessed | tf_op | source)
XLA Modules:
  0.0 56.0 jit_solution(3235538802720696759)
XLA Ops:
  0.1 1.1 %norm.1 = (bf16[16,2048]{1,0:T(8,128)(2,1)S(1)}, bf16[16,512]{1,0:T(8,128)(2,1)S(1)}, bf16[16,512]{1,0:T(8,128)(2,1)S(1)}, bf16[16,512]{1,0:T(8,128)(2,1)S(1)}, bf16[16,512]{1,0:T(8,128)(2,1)S(1)}) custom-call(bf16[16,2048]{1,0:T(8,128)(2,1)} %stream_ref.1, f32[1,2048]{1,0:T(1,128)} %bitcast.19), custom_call_target="tpu_custom_call" | custom-call | flops 40000000000 | tf_op jit(solution)/shard_map/norm/pallas_call | solution.py:291
  1.2 3.0 %collective-permute-start = (bf16[16,512]{1,0:T(8,128)(2,1)S(1)}, bf16[16,512]{1,0:T(8,128)(2,1)S(1)}, u32[]{:S(2)}, u32[]{:S(2)}) collective-permute-start(bf16[16,512]{1,0:T(8,128)(2,1)S(1)} %get-tuple-element.22), channel_id=1, source_target_pairs={{0,8},{8,0},{16,24},{24,16},{1,9},{9,1},{17,25},{25,17},{2,10},{10... | collective-permute-start | bytes 49160 | tf_op jit(solution)/shard_map/ppermute | solution.py:41
  4.3 1.5 %collective-permute-start.1 = (bf16[16,512]{1,0:T(8,128)(2,1)S(1)}, bf16[16,512]{1,0:T(8,128)(2,1)S(1)}, u32[]{:S(2)}, u32[]{:S(2)}) collective-permute-start(bf16[16,512]{1,0:T(8,128)(2,1)S(1)} %get-tuple-element.23), channel_id=1, source_target_pairs={{0,16},{8,24},{16,0},{24,8},{1,17},{9,25},{17,1},{25,9},{2,18},{10... | collective-permute-start | bytes 49160 | tf_op jit(solution)/shard_map/ppermute | solution.py:41
  6.0 2.0 %collective-permute-done.1.refs_2_ = bf16[16,512]{1,0:T(8,128)(2,1)S(1)} collective-permute-done((bf16[16,512]{1,0:T(8,128)(2,1)S(1)}, bf16[16,512]{1,0:T(8,128)(2,1)S(1)}, u32[]{:S(2)}, u32[]{:S(2)}) %collective-permute-start.1) | collective-permute-done | bytes 16416 | tf_op jit(solution)/shard_map/ppermute | solution.py:41
  8.0 2.4 %collective-permute-done.2.refs_3_ = bf16[16,512]{1,0:T(8,128)(2,1)S(1)} collective-permute-done((bf16[16,512]{1,0:T(8,128)(2,1)S(1)}, bf16[16,512]{1,0:T(8,128)(2,1)S(1)}, u32[]{:S(2)}, u32[]{:S(2)}) %collective-permute-start.2) | collective-permute-done | bytes 16416 | tf_op jit(solution)/shard_map/ppermute | solution.py:41
  10.7 0.6 %collective-permute-start.3 = (f32[16,768]{1,0:T(8,128)S(1)}, f32[16,768]{1,0:T(8,128)S(1)}, u32[]{:S(2)}, u32[]{:S(2)}) collective-permute-start(f32[16,768]{1,0:T(8,128)S(1)} %get-tuple-element.26), channel_id=1, source_target_pairs={{0,8},{8,0},{16,24},{24,16},{1,9},{9,1},{17,25},{25,17},{2,10},{10... | collective-permute-start | bytes 147464 | tf_op jit(solution)/shard_map/ppermute | solution.py:41
  11.4 2.9 %collective-permute-start.5 = (f32[16,768]{1,0:T(8,128)S(1)}, f32[16,768]{1,0:T(8,128)S(1)}, u32[]{:S(2)}, u32[]{:S(2)}) collective-permute-start(f32[16,768]{1,0:T(8,128)S(1)} %get-tuple-element.28), channel_id=1, source_target_pairs={{0,24},{8,16},{16,8},{24,0},{1,25},{9,17},{17,9},{25,1},{2,26},{10... | collective-permute-start | bytes 147464 | tf_op jit(solution)/shard_map/ppermute | solution.py:41
  14.3 0.6 %collective-permute-done.3.refs_1_ = f32[16,768]{1,0:T(8,128)S(1)} collective-permute-done((f32[16,768]{1,0:T(8,128)S(1)}, f32[16,768]{1,0:T(8,128)S(1)}, u32[]{:S(2)}, u32[]{:S(2)}) %collective-permute-start.3) | collective-permute-done | bytes 49184 | tf_op jit(solution)/shard_map/ppermute | solution.py:41
  15.4 0.9 %collective-permute-done.5.refs_3_ = f32[16,768]{1,0:T(8,128)S(1)} collective-permute-done((f32[16,768]{1,0:T(8,128)S(1)}, f32[16,768]{1,0:T(8,128)S(1)}, u32[]{:S(2)}, u32[]{:S(2)}) %collective-permute-start.5) | collective-permute-done | bytes 49184 | tf_op jit(solution)/shard_map/ppermute | solution.py:41
  16.5 4.7 %attend.1 = (f32[16,1024]{1,0:T(8,128)S(1)}, bf16[16,1024]{1,0:T(8,128)(2,1)S(1)}) custom-call(s32[16]{0:T(128)S(1)} %copy-done.13, bf16[16,2048]{1,0:T(8,128)(2,1)S(1)} %get-tuple-element.20.normed_ref, bf16[16,2048]{1,0:T(8,128)(2,1)S(1)} %bitcast.14, f32[1,16]{1,0:T(1,128)S(1)} %bitcast.18, f32[16,2,1024]{2,1,0:T(2,128)S(1)} %copy-done.7, ...), custom_call_target="tpu_custom_call" | custom-call | tf_op jit(solution)/shard_map/attend/pallas_call | solution.py:314
  21.3 1.2 %collective-permute-done.6.taken_ref = bf16[16,1024]{1,0:T(8,128)(2,1)S(1)} collective-permute-done((bf16[16,1024]{1,0:T(8,128)(2,1)S(1)}, bf16[16,1024]{1,0:T(8,128)(2,1)S(1)}, u32[]{:S(2)}, u32[]{:S(2)}) %collective-permute-start.6) | collective-permute-done | bytes 32800 | tf_op jit(solution)/shard_map/ppermute | solution.py:332
  22.5 4.1 %collective-permute-start.9 = (bf16[16,1024]{1,0:T(8,128)(2,1)S(1)}, bf16[16,1024]{1,0:T(8,128)(2,1)S(1)}, u32[]{:S(2)}, u32[]{:S(2)}) collective-permute-start(bf16[16,1024]{1,0:T(8,128)(2,1)S(1)} %pair.1.refs_0_), channel_id=1, source_target_pairs={{0,6},{1,7},{2,4},{3,5},{4,2},{5,3},{6,0},{7,1},{8,14},{9,15},{10,... | collective-permute-start | bytes 98312 | tf_op jit(solution)/shard_map/ppermute | solution.py:41
  26.6 0.6 %collective-permute-start.7 = (bf16[16,1024]{1,0:T(8,128)(2,1)S(1)}, bf16[16,1024]{1,0:T(8,128)(2,1)S(1)}, u32[]{:S(2)}, u32[]{:S(2)}) collective-permute-start(bf16[16,1024]{1,0:T(8,128)(2,1)S(1)} %pair.1.refs_0_), channel_id=1, source_target_pairs={{0,2},{1,3},{2,0},{3,1},{4,6},{5,7},{6,4},{7,5},{8,10},{9,11},{10,... | collective-permute-start | bytes 98312 | tf_op jit(solution)/shard_map/ppermute | solution.py:41
  27.3 1.3 %collective-permute-done.9.refs_3_ = bf16[16,1024]{1,0:T(8,128)(2,1)S(1)} collective-permute-done((bf16[16,1024]{1,0:T(8,128)(2,1)S(1)}, bf16[16,1024]{1,0:T(8,128)(2,1)S(1)}, u32[]{:S(2)}, u32[]{:S(2)}) %collective-permute-start.9) | collective-permute-done | bytes 32800 | tf_op jit(solution)/shard_map/ppermute | solution.py:41
  28.5 2.9 %collective-permute-done.8.refs_2_ = bf16[16,1024]{1,0:T(8,128)(2,1)S(1)} collective-permute-done((bf16[16,1024]{1,0:T(8,128)(2,1)S(1)}, bf16[16,1024]{1,0:T(8,128)(2,1)S(1)}, u32[]{:S(2)}, u32[]{:S(2)}) %collective-permute-start.8) | collective-permute-done | bytes 32800 | tf_op jit(solution)/shard_map/ppermute | solution.py:41
  31.6 1.2 %collective-permute-done.10.far_ref = bf16[16,1024]{1,0:T(8,128)(2,1)S(1)} collective-permute-done((bf16[16,1024]{1,0:T(8,128)(2,1)S(1)}, bf16[16,1024]{1,0:T(8,128)(2,1)S(1)}, u32[]{:S(2)}, u32[]{:S(2)}) %collective-permute-start.10) | collective-permute-done | bytes 32800 | tf_op jit(solution)/shard_map/ppermute | solution.py:337
  32.9 2.5 %collective-permute-start.13 = (bf16[16,2048]{1,0:T(8,128)(2,1)S(1)}, bf16[16,2048]{1,0:T(8,128)(2,1)S(1)}, u32[]{:S(2)}, u32[]{:S(2)}) collective-permute-start(bf16[16,2048]{1,0:T(8,128)(2,1)S(1)} %get-tuple-element.31.refs_0_), channel_id=1, source_target_pairs={{0,24},{8,16},{16,8},{24,0},{1,25},{9,17},{17,9},{25,1},{2,26},{10... | collective-permute-start | bytes 196616 | tf_op jit(solution)/shard_map/ppermute | solution.py:41
  35.9 0.5 collective-permute-start.11
  36.5 1.7 %collective-permute-done.13.refs_3_ = bf16[16,2048]{1,0:T(8,128)(2,1)S(1)} collective-permute-done((bf16[16,2048]{1,0:T(8,128)(2,1)S(1)}, bf16[16,2048]{1,0:T(8,128)(2,1)S(1)}, u32[]{:S(2)}, u32[]{:S(2)}) %collective-permute-start.13) | collective-permute-done | bytes 65568 | tf_op jit(solution)/shard_map/ppermute | solution.py:41
  38.2 1.5 %collective-permute-done.12.refs_2_ = bf16[16,2048]{1,0:T(8,128)(2,1)S(1)} collective-permute-done((bf16[16,2048]{1,0:T(8,128)(2,1)S(1)}, bf16[16,2048]{1,0:T(8,128)(2,1)S(1)}, u32[]{:S(2)}, u32[]{:S(2)}) %collective-permute-start.12) | collective-permute-done | bytes 65568 | tf_op jit(solution)/shard_map/ppermute | solution.py:41
  40.2 2.4 %experts.1 = (bf16[32,8,256]{2,1,0:T(8,128)(2,1)S(1)}, bf16[32,8,256]{2,1,0:T(8,128)(2,1)S(1)}) custom-call(s32[2,64]{1,0:T(2,128)S(1)} %bitcast.16, f32[2,64]{1,0:T(2,128)S(1)} %bitcast.17, bf16[1,704,2048]{2,1,0:T(8,128)(2,1)S(1)} %bitcast.12, bf16[1,704,2048]{2,1,0:T(8,128)(2,1)S(1)} %bitcast.13, bf16[1,704,2048]{2,1,0:T(8,128)(2,1)S(1)} %copy-done.2, ...), custom_call_target="tpu_custom_call" | custom-call | tf_op jit(solution)/shard_map/experts/pallas_call | solution.py:347
  42.7 1.3 %collective-permute-done.14.taken_ref = bf16[32,8,256]{2,1,0:T(8,128)(2,1)S(1)} collective-permute-done((bf16[32,8,256]{2,1,0:T(8,128)(2,1)S(1)}, bf16[32,8,256]{2,1,0:T(8,128)(2,1)S(1)}, u32[]{:S(2)}, u32[]{:S(2)}) %collective-permute-start.14) | collective-permute-done | bytes 131104 | tf_op jit(solution)/shard_map/ppermute | solution.py:360
  44.0 11.3 %all_to_all.5.parts_ref = bf16[32,8,256]{2,1,0:T(8,128)(2,1)S(1)} all-to-all(bf16[32,8,256]{2,1,0:T(8,128)(2,1)S(1)} %sides.1), channel_id=1, replica_groups=mesh['ep'=4,'tp'=8] {'ep','tp'}, dimensions={0} | all-to-all | bytes 262144 | tf_op jit(solution)/shard_map/all_to_all | solution.py:362
  55.3 0.6 %finish.1 = bf16[16,256]{1,0:T(8,128)(2,1)} custom-call(bf16[32,8,256]{2,1,0:T(8,128)(2,1)S(1)} %all_to_all.5.parts_ref, bf16[16,256]{1,0:T(8,128)(2,1)S(1)} %get-tuple-element.34.mixed_ref), custom_call_target="tpu_custom_call" | custom-call | tf_op jit(solution)/shard_map/finish/pallas_call | solution.py:363
  (56 shorter events, 2.5 us)
Async XLA Ops:
  0.0 16.3 %slice-start = ((s8[8388608]{0:T(1024)(128)(4,1)}), s8[4194304]{0:T(1024)(128)(4,1)S(1)}, s32[]{:S(2)}) async-start(s8[8388608]{0:T(1024)(128)(4,1)} %bitcast.8), calls=%async_computation.1 | async-start | bytes 8388608
  0.0 16.3 %slice-start.2 = ((s8[8388608]{0:T(1024)(128)(4,1)}), s8[4194304]{0:T(1024)(128)(4,1)S(1)}, s32[]{:S(2)}) async-start(s8[8388608]{0:T(1024)(128)(4,1)} %bitcast.10), calls=%async_computation.3 | async-start | bytes 8388608
  0.0 16.3 %slice-start.1 = ((s8[8388608]{0:T(1024)(128)(4,1)}), s8[4194304]{0:T(1024)(128)(4,1)S(1)}, s32[]{:S(2)}) async-start(s8[8388608]{0:T(1024)(128)(4,1)} %bitcast.8), calls=%async_computation.2 | async-start | bytes 8388608
  0.0 16.3 %slice-start.3 = ((s8[8388608]{0:T(1024)(128)(4,1)}), s8[4194304]{0:T(1024)(128)(4,1)S(1)}, s32[]{:S(2)}) async-start(s8[8388608]{0:T(1024)(128)(4,1)} %bitcast.10), calls=%async_computation.4 | async-start | bytes 8388608
  1.2 4.8 %collective-permute-start = (bf16[16,512]{1,0:T(8,128)(2,1)S(1)}, bf16[16,512]{1,0:T(8,128)(2,1)S(1)}, u32[]{:S(2)}, u32[]{:S(2)}) collective-permute-start(bf16[16,512]{1,0:T(8,128)(2,1)S(1)} %get-tuple-element.22), channel_id=1, source_target_pairs={{0,8},{8,0},{16,24},{24,16},{1,9},{9,1},{17,25},{25,17},{2,10},{10... | collective-permute-start | bytes 49160 | tf_op jit(solution)/shard_map/ppermute | solution.py:41
  4.3 3.7 %collective-permute-start.1 = (bf16[16,512]{1,0:T(8,128)(2,1)S(1)}, bf16[16,512]{1,0:T(8,128)(2,1)S(1)}, u32[]{:S(2)}, u32[]{:S(2)}) collective-permute-start(bf16[16,512]{1,0:T(8,128)(2,1)S(1)} %get-tuple-element.23), channel_id=1, source_target_pairs={{0,16},{8,24},{16,0},{24,8},{1,17},{9,25},{17,1},{25,9},{2,18},{10... | collective-permute-start | bytes 49160 | tf_op jit(solution)/shard_map/ppermute | solution.py:41
  5.8 4.6 %collective-permute-start.2 = (bf16[16,512]{1,0:T(8,128)(2,1)S(1)}, bf16[16,512]{1,0:T(8,128)(2,1)S(1)}, u32[]{:S(2)}, u32[]{:S(2)}) collective-permute-start(bf16[16,512]{1,0:T(8,128)(2,1)S(1)} %get-tuple-element.24), channel_id=1, source_target_pairs={{0,24},{8,16},{16,8},{24,0},{1,25},{9,17},{17,9},{25,1},{2,26},{10... | collective-permute-start | bytes 49160 | tf_op jit(solution)/shard_map/ppermute | solution.py:41
  10.7 4.1 %collective-permute-start.3 = (f32[16,768]{1,0:T(8,128)S(1)}, f32[16,768]{1,0:T(8,128)S(1)}, u32[]{:S(2)}, u32[]{:S(2)}) collective-permute-start(f32[16,768]{1,0:T(8,128)S(1)} %get-tuple-element.26), channel_id=1, source_target_pairs={{0,8},{8,0},{16,24},{24,16},{1,9},{9,1},{17,25},{25,17},{2,10},{10... | collective-permute-start | bytes 147464 | tf_op jit(solution)/shard_map/ppermute | solution.py:41
  11.3 4.1 %collective-permute-start.4 = (f32[16,768]{1,0:T(8,128)S(1)}, f32[16,768]{1,0:T(8,128)S(1)}, u32[]{:S(2)}, u32[]{:S(2)}) collective-permute-start(f32[16,768]{1,0:T(8,128)S(1)} %get-tuple-element.27), channel_id=1, source_target_pairs={{0,16},{8,24},{16,0},{24,8},{1,17},{9,25},{17,1},{25,9},{2,18},{10... | collective-permute-start | bytes 147464 | tf_op jit(solution)/shard_map/ppermute | solution.py:41
  11.4 5.0 %collective-permute-start.5 = (f32[16,768]{1,0:T(8,128)S(1)}, f32[16,768]{1,0:T(8,128)S(1)}, u32[]{:S(2)}, u32[]{:S(2)}) collective-permute-start(f32[16,768]{1,0:T(8,128)S(1)} %get-tuple-element.28), channel_id=1, source_target_pairs={{0,24},{8,16},{16,8},{24,0},{1,25},{9,17},{17,9},{25,1},{2,26},{10... | collective-permute-start | bytes 147464 | tf_op jit(solution)/shard_map/ppermute | solution.py:41
  16.5 23.7 %copy-start = (bf16[1,2048,704]{1,2,0:T(8,128)(2,1)S(1)}, bf16[1,2048,704]{1,2,0:T(8,128)(2,1)}, u32[]{:S(2)}) copy-start(bf16[1,2048,704]{1,2,0:T(8,128)(2,1)} %param.33) | copy-start | bytes 8650756
  16.5 23.7 %copy-start.1 = (bf16[1,2048,704]{1,2,0:T(8,128)(2,1)S(1)}, bf16[1,2048,704]{1,2,0:T(8,128)(2,1)}, u32[]{:S(2)}) copy-start(bf16[1,2048,704]{1,2,0:T(8,128)(2,1)} %param.34) | copy-start | bytes 8650756
  16.5 23.7 %copy-start.2 = (bf16[1,704,2048]{2,1,0:T(8,128)(2,1)S(1)}, bf16[1,704,2048]{2,1,0:T(8,128)(2,1)}, u32[]{:S(2)}) copy-start(bf16[1,704,2048]{2,1,0:T(8,128)(2,1)} %down_ref.1) | copy-start | bytes 8650756
  16.5 23.7 %copy-start.11 = (s32[64,2]{0,1:T(2,128)S(1)}, s32[64,2]{0,1:T(2,128)}, u32[]{:S(2)}) copy-start(s32[64,2]{0,1:T(2,128)} %param.31) | copy-start | bytes 1540
  16.5 23.7 %copy-start.12 = (f32[64,2]{0,1:T(2,128)S(1)}, f32[64,2]{0,1:T(2,128)}, u32[]{:S(2)}) copy-start(f32[64,2]{0,1:T(2,128)} %param.32) | copy-start | bytes 1540
  21.2 1.3 %collective-permute-start.6 = (bf16[16,1024]{1,0:T(8,128)(2,1)S(1)}, bf16[16,1024]{1,0:T(8,128)(2,1)S(1)}, u32[]{:S(2)}, u32[]{:S(2)}) collective-permute-start(bf16[16,1024]{1,0:T(8,128)(2,1)S(1)} %get-tuple-element.30), channel_id=1, source_target_pairs={{0,1},{1,0},{2,3},{3,2},{4,5},{5,4},{6,7},{7,6},{8,9},{9,8},{10,11... | collective-permute-start | bytes 98312 | tf_op jit(solution)/shard_map/ppermute | solution.py:332
  22.5 6.0 %collective-permute-start.9 = (bf16[16,1024]{1,0:T(8,128)(2,1)S(1)}, bf16[16,1024]{1,0:T(8,128)(2,1)S(1)}, u32[]{:S(2)}, u32[]{:S(2)}) collective-permute-start(bf16[16,1024]{1,0:T(8,128)(2,1)S(1)} %pair.1.refs_0_), channel_id=1, source_target_pairs={{0,6},{1,7},{2,4},{3,5},{4,2},{5,3},{6,0},{7,1},{8,14},{9,15},{10,... | collective-permute-start | bytes 98312 | tf_op jit(solution)/shard_map/ppermute | solution.py:41
  26.6 4.8 %collective-permute-start.8 = (bf16[16,1024]{1,0:T(8,128)(2,1)S(1)}, bf16[16,1024]{1,0:T(8,128)(2,1)S(1)}, u32[]{:S(2)}, u32[]{:S(2)}) collective-permute-start(bf16[16,1024]{1,0:T(8,128)(2,1)S(1)} %pair.1.refs_0_), channel_id=1, source_target_pairs={{0,4},{1,5},{2,6},{3,7},{4,0},{5,1},{6,2},{7,3},{8,12},{9,13},{10,... | collective-permute-start | bytes 98312 | tf_op jit(solution)/shard_map/ppermute | solution.py:41
  26.6 4.8 %collective-permute-start.7 = (bf16[16,1024]{1,0:T(8,128)(2,1)S(1)}, bf16[16,1024]{1,0:T(8,128)(2,1)S(1)}, u32[]{:S(2)}, u32[]{:S(2)}) collective-permute-start(bf16[16,1024]{1,0:T(8,128)(2,1)S(1)} %pair.1.refs_0_), channel_id=1, source_target_pairs={{0,2},{1,3},{2,0},{3,1},{4,6},{5,7},{6,4},{7,5},{8,10},{9,11},{10,... | collective-permute-start | bytes 98312 | tf_op jit(solution)/shard_map/ppermute | solution.py:41
  31.5 1.3 %collective-permute-start.10 = (bf16[16,1024]{1,0:T(8,128)(2,1)S(1)}, bf16[16,1024]{1,0:T(8,128)(2,1)S(1)}, u32[]{:S(2)}, u32[]{:S(2)}) collective-permute-start(bf16[16,1024]{1,0:T(8,128)(2,1)S(1)} %mix.1.near_ref), channel_id=1, source_target_pairs={{0,1},{1,0},{2,3},{3,2},{4,5},{5,4},{6,7},{7,6},{8,9},{9,8},{10,11... | collective-permute-start | bytes 98312 | tf_op jit(solution)/shard_map/ppermute | solution.py:337
  32.9 5.3 %collective-permute-start.13 = (bf16[16,2048]{1,0:T(8,128)(2,1)S(1)}, bf16[16,2048]{1,0:T(8,128)(2,1)S(1)}, u32[]{:S(2)}, u32[]{:S(2)}) collective-permute-start(bf16[16,2048]{1,0:T(8,128)(2,1)S(1)} %get-tuple-element.31.refs_0_), channel_id=1, source_target_pairs={{0,24},{8,16},{16,8},{24,0},{1,25},{9,17},{17,9},{25,1},{2,26},{10... | collective-permute-start | bytes 196616 | tf_op jit(solution)/shard_map/ppermute | solution.py:41
  35.4 4.3 %collective-permute-start.12 = (bf16[16,2048]{1,0:T(8,128)(2,1)S(1)}, bf16[16,2048]{1,0:T(8,128)(2,1)S(1)}, u32[]{:S(2)}, u32[]{:S(2)}) collective-permute-start(bf16[16,2048]{1,0:T(8,128)(2,1)S(1)} %get-tuple-element.31.refs_0_), channel_id=1, source_target_pairs={{0,16},{8,24},{16,0},{24,8},{1,17},{9,25},{17,1},{25,9},{2,18},{10... | collective-permute-start | bytes 196616 | tf_op jit(solution)/shard_map/ppermute | solution.py:41
  35.9 4.3 %collective-permute-start.11 = (bf16[16,2048]{1,0:T(8,128)(2,1)S(1)}, bf16[16,2048]{1,0:T(8,128)(2,1)S(1)}, u32[]{:S(2)}, u32[]{:S(2)}) collective-permute-start(bf16[16,2048]{1,0:T(8,128)(2,1)S(1)} %get-tuple-element.31.refs_0_), channel_id=1, source_target_pairs={{0,8},{8,0},{16,24},{24,16},{1,9},{9,1},{17,25},{25,17},{2,10},{10... | collective-permute-start | bytes 196616 | tf_op jit(solution)/shard_map/ppermute | solution.py:41
  42.6 1.4 %collective-permute-start.14 = (bf16[32,8,256]{2,1,0:T(8,128)(2,1)S(1)}, bf16[32,8,256]{2,1,0:T(8,128)(2,1)S(1)}, u32[]{:S(2)}, u32[]{:S(2)}) collective-permute-start(bf16[32,8,256]{2,1,0:T(8,128)(2,1)S(1)} %get-tuple-element.33), channel_id=1, source_target_pairs={{0,1},{1,0},{2,3},{3,2},{4,5},{5,4},{6,7},{7,6},{8,9},{9,8},{10,11... | collective-permute-start | bytes 393224 | tf_op jit(solution)/shard_map/ppermute | solution.py:360
  (10 other events, 144.3 us)

commit v5 on v4

--- a/solution.py
+++ b/solution.py
@@ -10,6 +10,7 @@
 F32 = jnp.float32
 BF16 = jnp.bfloat16
 ROWS = 8
+BLOCK = 256
 HIDDEN = -1e30
 MIB = 1 << 20
 COVER = 40_000_000_000
@@ -98,7 +99,7 @@
     values_ref,
     *refs,
 ):
-    *part_refs, keep_ref, give_ref, attended_ref, product_ref = refs
+    *part_refs, keep_ref, give_ref, attended_ref, product_ref, scores_ref = refs
     count = normed_ref.shape[0]
     heads = gates_ref.shape[1]
     cache_len = gates_ref.shape[2]
@@ -121,25 +122,41 @@
     row_ids = lax.broadcasted_iota(jnp.int32, (ROWS, 1), 0)
     positions = lax.broadcasted_iota(jnp.int32, (ROWS, cache_len), 1)
 
+    def stacked(first):
+        return jnp.concatenate(
+            [
+                jnp.where(lanes // head_dim == head, query[first : first + ROWS], 0.0).astype(BF16)
+                for head in range(heads)
+            ],
+            axis=0,
+        )
+
+    for pair in range(0, count, 2 * ROWS):
+        streamed, loaded = stacked(pair), stacked(pair + ROWS)
+        lane_row = lax.broadcasted_iota(jnp.int32, (BLOCK, heads * ROWS), 1) % ROWS
+        loaded_row = lax.broadcasted_iota(jnp.int32, (heads * ROWS, BLOCK), 0) % ROWS
+        for start in range(0, cache_len, BLOCK):
+            block = slice(start, start + BLOCK)
+            down = jnp.zeros((BLOCK, heads * ROWS), F32)
+            over = jnp.zeros((heads * ROWS, BLOCK), F32)
+            for row in range(ROWS):
+                products = dot_transposed(keys_ref[pair + row, block, :], streamed)
+                down = jnp.where(lane_row == row, products, down)
+                products = dot_transposed(loaded, keys_ref[pair + ROWS + row, block, :])
+                over = jnp.where(loaded_row == row, products, over)
+            base = heads * pair
+            scores_ref[base : base + heads * ROWS, block] = down.T
+            scores_ref[base + heads * ROWS : base + 2 * heads * ROWS, block] = over
+
     for first in range(0, count, ROWS):
         mine = slice(first, first + ROWS)
         length = jnp.zeros((ROWS, 1), jnp.int32)
         for row in range(ROWS):
             length = jnp.where(row_ids == row, lengths_ref[first + row], length)
-        stacked = jnp.concatenate(
-            [
-                jnp.where(lanes // head_dim == head, query[mine], 0.0).astype(BF16)
-                for head in range(heads)
-            ],
-            axis=0,
-        )
-        scores = [jnp.zeros((ROWS, cache_len), F32) for _ in range(heads)]
-        for row in range(ROWS):
-            products = dot_transposed(stacked, keys_ref[first + row])
-            for head in range(heads):
-                scores[head] = jnp.where(
-                    row_ids == row, products[head * ROWS : (head + 1) * ROWS], scores[head]
-                )
+        base = heads * first
+        scores = [
+            scores_ref[base + head * ROWS : base + (head + 1) * ROWS, :] for head in range(heads)
+        ]
         weights = []
         owns = []
         for head in range(heads):
@@ -224,9 +241,16 @@
     half = count // 2
     expert = lax.axis_index("ep")
     rows = jnp.concatenate([row_ref[...] for row_ref in row_refs], axis=0)
-    gated = dot_transposed(rows, gate_ref[0])
-    upper = dot_transposed(rows, up_ref[0])
-    hidden = (gated / (1.0 + jnp.exp(-gated)) * upper).astype(BF16)
+    hidden = []
+    for start in range(0, gate_ref.shape[1], BLOCK):
+        units = slice(start, min(start + BLOCK, gate_ref.shape[1]))
+        gated, upper = 0.0, 0.0
+        for first in range(0, rows.shape[1], BLOCK):
+            features = slice(first, first + BLOCK)
+            gated += dot_transposed(rows[:, features], gate_ref[0, units, features])
+            upper += dot_transposed(up_ref[0, units, features], rows[:, features])
+        hidden.append((gated / (1.0 + jnp.exp(-gated)) * upper.T).astype(BF16))
+    hidden = jnp.concatenate(hidden, axis=1)
     partial = jnp.dot(hidden, down_ref[0], preferred_element_type=F32)
     share = jnp.sum(jnp.where(routes_ref[...] == expert, weights_ref[...], 0.0), axis=0, keepdims=True)
     square = (groups * count, groups * count)
@@ -317,7 +341,11 @@
         4 * MIB,
         [shape(side.shape, F32), side],
         in_specs=[in_smem] + [in_vmem] * (7 + groups),
-        scratch_shapes=[pltpu.VMEM((count, width), F32), pltpu.VMEM((count, model_width), F32)],
+        scratch_shapes=[
+            pltpu.VMEM((count, width), F32),
+            pltpu.VMEM((count, model_width), F32),
+            pltpu.VMEM((gate_cache.shape[1] * count, gate_cache.shape[2]), F32),
+        ],
     )(
         lengths,
         normed,

time: 56.1 us -> 54.7 us (0.975)
  Pallas kernels: 9.3 us -> 7.85 us
    pallas_call x1, Pallas kernels: 4.73 us -> 3.48 us  [shards(): call(attend_kernel, 'attend', 4 * MIB, [shape(side.shape, F32), side], in...]
where the time goes in v5:
time: 54.7 us; the launch traced here: 54.5 us
  waiting for transfers between devices  18.3 us (33%)
  starting transfers between devices  16.7 us (31%)
  blocking collectives  11.3 us (21%)
  Pallas kernels  7.85 us (14%)
    ppermute x12, starting transfers between devices, exchange(): lax.ppermute(items[step], axis, [(one, one ^ step * stride) for one in ra...  16.5 us
    ppermute x12, waiting for transfers between devices, exchange(): lax.ppermute(items[step], axis, [(one, one ^ step * stride) for one in ra...  14.6 us
    all_to_all x1, blocking collectives, shards(): returned = lax.all_to_all(summed, ('ep', 'tp'), 0, 0, tiled=True)  11.3 us
    pallas_call x1, Pallas kernels, shards(): call(attend_kernel, 'attend', 4 * MIB, [shape(side.shape, F32), side], in...  3.48 us
    ppermute x2, waiting for transfers between devices, shards(): taken = lax.ppermute(give, 'tp', swap)  2.53 us
    pallas_call x1, Pallas kernels, shards(): call(functools.partial(expert_kernel, groups=groups, paired=paired), 'exp...  2.14 us
    ppermute x1, waiting for transfers between devices, shards(): far = lax.ppermute(near, 'tp', swap)  1.19 us
    pallas_call x1, Pallas kernels, shards(): call(functools.partial(norm_kernel, paired=paired), 'norm', 2 * MIB, [sha...  1.13 us
  transfers between devices with their start and end apart: 15, of which 14 were waited for; matrix products, arithmetic and copies ran while one was open for 0% of the time, Pallas kernels for 0%

profile of v5, /device:TPU:0, one launch (start us, length us, event | category | flops | bytes accessed | tf_op | source)
XLA Modules:
  0.0 54.5 jit_solution(9811765855612744955)
XLA Ops:
  0.1 1.1 %norm.1 = (bf16[16,2048]{1,0:T(8,128)(2,1)S(1)}, bf16[16,512]{1,0:T(8,128)(2,1)S(1)}, bf16[16,512]{1,0:T(8,128)(2,1)S(1)}, bf16[16,512]{1,0:T(8,128)(2,1)S(1)}, bf16[16,512]{1,0:T(8,128)(2,1)S(1)}) custom-call(bf16[16,2048]{1,0:T(8,128)(2,1)} %stream_ref.1, f32[1,2048]{1,0:T(1,128)} %bitcast.19), custom_call_target="tpu_custom_call" | custom-call | flops 40000000000 | tf_op jit(solution)/shard_map/norm/pallas_call | solution.py:315
  1.2 3.0 %collective-permute-start = (bf16[16,512]{1,0:T(8,128)(2,1)S(1)}, bf16[16,512]{1,0:T(8,128)(2,1)S(1)}, u32[]{:S(2)}, u32[]{:S(2)}) collective-permute-start(bf16[16,512]{1,0:T(8,128)(2,1)S(1)} %get-tuple-element.22), channel_id=1, source_target_pairs={{0,8},{8,0},{16,24},{24,16},{1,9},{9,1},{17,25},{25,17},{2,10},{10... | collective-permute-start | bytes 49160 | tf_op jit(solution)/shard_map/ppermute | solution.py:42
  4.3 1.5 %collective-permute-start.1 = (bf16[16,512]{1,0:T(8,128)(2,1)S(1)}, bf16[16,512]{1,0:T(8,128)(2,1)S(1)}, u32[]{:S(2)}, u32[]{:S(2)}) collective-permute-start(bf16[16,512]{1,0:T(8,128)(2,1)S(1)} %get-tuple-element.23), channel_id=1, source_target_pairs={{0,16},{8,24},{16,0},{24,8},{1,17},{9,25},{17,1},{25,9},{2,18},{10... | collective-permute-start | bytes 49160 | tf_op jit(solution)/shard_map/ppermute | solution.py:42
  6.0 2.0 %collective-permute-done.1.refs_2_ = bf16[16,512]{1,0:T(8,128)(2,1)S(1)} collective-permute-done((bf16[16,512]{1,0:T(8,128)(2,1)S(1)}, bf16[16,512]{1,0:T(8,128)(2,1)S(1)}, u32[]{:S(2)}, u32[]{:S(2)}) %collective-permute-start.1) | collective-permute-done | bytes 16416 | tf_op jit(solution)/shard_map/ppermute | solution.py:42
  8.0 2.4 %collective-permute-done.2.refs_3_ = bf16[16,512]{1,0:T(8,128)(2,1)S(1)} collective-permute-done((bf16[16,512]{1,0:T(8,128)(2,1)S(1)}, bf16[16,512]{1,0:T(8,128)(2,1)S(1)}, u32[]{:S(2)}, u32[]{:S(2)}) %collective-permute-start.2) | collective-permute-done | bytes 16416 | tf_op jit(solution)/shard_map/ppermute | solution.py:42
  10.7 0.6 %collective-permute-start.3 = (f32[16,768]{1,0:T(8,128)S(1)}, f32[16,768]{1,0:T(8,128)S(1)}, u32[]{:S(2)}, u32[]{:S(2)}) collective-permute-start(f32[16,768]{1,0:T(8,128)S(1)} %get-tuple-element.26), channel_id=1, source_target_pairs={{0,8},{8,0},{16,24},{24,16},{1,9},{9,1},{17,25},{25,17},{2,10},{10... | collective-permute-start | bytes 147464 | tf_op jit(solution)/shard_map/ppermute | solution.py:42
  11.4 2.9 %collective-permute-start.5 = (f32[16,768]{1,0:T(8,128)S(1)}, f32[16,768]{1,0:T(8,128)S(1)}, u32[]{:S(2)}, u32[]{:S(2)}) collective-permute-start(f32[16,768]{1,0:T(8,128)S(1)} %get-tuple-element.28), channel_id=1, source_target_pairs={{0,24},{8,16},{16,8},{24,0},{1,25},{9,17},{17,9},{25,1},{2,26},{10... | collective-permute-start | bytes 147464 | tf_op jit(solution)/shard_map/ppermute | solution.py:42
  14.3 0.6 %collective-permute-done.3.refs_1_ = f32[16,768]{1,0:T(8,128)S(1)} collective-permute-done((f32[16,768]{1,0:T(8,128)S(1)}, f32[16,768]{1,0:T(8,128)S(1)}, u32[]{:S(2)}, u32[]{:S(2)}) %collective-permute-start.3) | collective-permute-done | bytes 49184 | tf_op jit(solution)/shard_map/ppermute | solution.py:42
  15.4 0.9 %collective-permute-done.5.refs_3_ = f32[16,768]{1,0:T(8,128)S(1)} collective-permute-done((f32[16,768]{1,0:T(8,128)S(1)}, f32[16,768]{1,0:T(8,128)S(1)}, u32[]{:S(2)}, u32[]{:S(2)}) %collective-permute-start.5) | collective-permute-done | bytes 49184 | tf_op jit(solution)/shard_map/ppermute | solution.py:42
  16.5 3.5 %attend.1 = (f32[16,1024]{1,0:T(8,128)S(1)}, bf16[16,1024]{1,0:T(8,128)(2,1)S(1)}) custom-call(s32[16]{0:T(128)S(1)} %copy-done.13, bf16[16,2048]{1,0:T(8,128)(2,1)S(1)} %get-tuple-element.20.normed_ref, bf16[16,2048]{1,0:T(8,128)(2,1)S(1)} %bitcast.14, f32[1,16]{1,0:T(1,128)S(1)} %bitcast.18, f32[16,2,1024]{2,1,0:T(2,128)S(1)} %copy-done.7, ...), custom_call_target="tpu_custom_call" | custom-call | tf_op jit(solution)/shard_map/attend/pallas_call | solution.py:338
  20.1 1.2 %collective-permute-done.6.taken_ref = bf16[16,1024]{1,0:T(8,128)(2,1)S(1)} collective-permute-done((bf16[16,1024]{1,0:T(8,128)(2,1)S(1)}, bf16[16,1024]{1,0:T(8,128)(2,1)S(1)}, u32[]{:S(2)}, u32[]{:S(2)}) %collective-permute-start.6) | collective-permute-done | bytes 32800 | tf_op jit(solution)/shard_map/ppermute | solution.py:360
  21.3 4.1 %collective-permute-start.9 = (bf16[16,1024]{1,0:T(8,128)(2,1)S(1)}, bf16[16,1024]{1,0:T(8,128)(2,1)S(1)}, u32[]{:S(2)}, u32[]{:S(2)}) collective-permute-start(bf16[16,1024]{1,0:T(8,128)(2,1)S(1)} %pair.1.refs_0_), channel_id=1, source_target_pairs={{0,6},{1,7},{2,4},{3,5},{4,2},{5,3},{6,0},{7,1},{8,14},{9,15},{10,... | collective-permute-start | bytes 98312 | tf_op jit(solution)/shard_map/ppermute | solution.py:42
  25.4 0.6 %collective-permute-start.7 = (bf16[16,1024]{1,0:T(8,128)(2,1)S(1)}, bf16[16,1024]{1,0:T(8,128)(2,1)S(1)}, u32[]{:S(2)}, u32[]{:S(2)}) collective-permute-start(bf16[16,1024]{1,0:T(8,128)(2,1)S(1)} %pair.1.refs_0_), channel_id=1, source_target_pairs={{0,2},{1,3},{2,0},{3,1},{4,6},{5,7},{6,4},{7,5},{8,10},{9,11},{10,... | collective-permute-start | bytes 98312 | tf_op jit(solution)/shard_map/ppermute | solution.py:42
  26.0 1.3 %collective-permute-done.9.refs_3_ = bf16[16,1024]{1,0:T(8,128)(2,1)S(1)} collective-permute-done((bf16[16,1024]{1,0:T(8,128)(2,1)S(1)}, bf16[16,1024]{1,0:T(8,128)(2,1)S(1)}, u32[]{:S(2)}, u32[]{:S(2)}) %collective-permute-start.9) | collective-permute-done | bytes 32800 | tf_op jit(solution)/shard_map/ppermute | solution.py:42
  27.3 2.9 %collective-permute-done.8.refs_2_ = bf16[16,1024]{1,0:T(8,128)(2,1)S(1)} collective-permute-done((bf16[16,1024]{1,0:T(8,128)(2,1)S(1)}, bf16[16,1024]{1,0:T(8,128)(2,1)S(1)}, u32[]{:S(2)}, u32[]{:S(2)}) %collective-permute-start.8) | collective-permute-done | bytes 32800 | tf_op jit(solution)/shard_map/ppermute | solution.py:42
  30.3 1.2 %collective-permute-done.10.far_ref = bf16[16,1024]{1,0:T(8,128)(2,1)S(1)} collective-permute-done((bf16[16,1024]{1,0:T(8,128)(2,1)S(1)}, bf16[16,1024]{1,0:T(8,128)(2,1)S(1)}, u32[]{:S(2)}, u32[]{:S(2)}) %collective-permute-start.10) | collective-permute-done | bytes 32800 | tf_op jit(solution)/shard_map/ppermute | solution.py:365
  31.7 2.5 %collective-permute-start.13 = (bf16[16,2048]{1,0:T(8,128)(2,1)S(1)}, bf16[16,2048]{1,0:T(8,128)(2,1)S(1)}, u32[]{:S(2)}, u32[]{:S(2)}) collective-permute-start(bf16[16,2048]{1,0:T(8,128)(2,1)S(1)} %get-tuple-element.31.refs_0_), channel_id=1, source_target_pairs={{0,24},{8,16},{16,8},{24,0},{1,25},{9,17},{17,9},{25,1},{2,26},{10... | collective-permute-start | bytes 196616 | tf_op jit(solution)/shard_map/ppermute | solution.py:42
  34.7 0.5 collective-permute-start.11
  35.2 1.7 %collective-permute-done.13.refs_3_ = bf16[16,2048]{1,0:T(8,128)(2,1)S(1)} collective-permute-done((bf16[16,2048]{1,0:T(8,128)(2,1)S(1)}, bf16[16,2048]{1,0:T(8,128)(2,1)S(1)}, u32[]{:S(2)}, u32[]{:S(2)}) %collective-permute-start.13) | collective-permute-done | bytes 65568 | tf_op jit(solution)/shard_map/ppermute | solution.py:42
  36.9 1.5 %collective-permute-done.12.refs_2_ = bf16[16,2048]{1,0:T(8,128)(2,1)S(1)} collective-permute-done((bf16[16,2048]{1,0:T(8,128)(2,1)S(1)}, bf16[16,2048]{1,0:T(8,128)(2,1)S(1)}, u32[]{:S(2)}, u32[]{:S(2)}) %collective-permute-start.12) | collective-permute-done | bytes 65568 | tf_op jit(solution)/shard_map/ppermute | solution.py:42
  39.0 2.1 %experts.1 = (bf16[32,8,256]{2,1,0:T(8,128)(2,1)S(1)}, bf16[32,8,256]{2,1,0:T(8,128)(2,1)S(1)}) custom-call(s32[2,64]{1,0:T(2,128)S(1)} %bitcast.16, f32[2,64]{1,0:T(2,128)S(1)} %bitcast.17, bf16[1,704,2048]{2,1,0:T(8,128)(2,1)S(1)} %bitcast.12, bf16[1,704,2048]{2,1,0:T(8,128)(2,1)S(1)} %bitcast.13, bf16[1,704,2048]{2,1,0:T(8,128)(2,1)S(1)} %copy-done.2, ...), custom_call_target="tpu_custom_call" | custom-call | tf_op jit(solution)/shard_map/experts/pallas_call | solution.py:375
  41.2 1.3 %collective-permute-done.14.taken_ref = bf16[32,8,256]{2,1,0:T(8,128)(2,1)S(1)} collective-permute-done((bf16[32,8,256]{2,1,0:T(8,128)(2,1)S(1)}, bf16[32,8,256]{2,1,0:T(8,128)(2,1)S(1)}, u32[]{:S(2)}, u32[]{:S(2)}) %collective-permute-start.14) | collective-permute-done | bytes 131104 | tf_op jit(solution)/shard_map/ppermute | solution.py:388
  42.6 11.3 %all_to_all.5.parts_ref = bf16[32,8,256]{2,1,0:T(8,128)(2,1)S(1)} all-to-all(bf16[32,8,256]{2,1,0:T(8,128)(2,1)S(1)} %sides.1), channel_id=1, replica_groups=mesh['ep'=4,'tp'=8] {'ep','tp'}, dimensions={0} | all-to-all | bytes 262144 | tf_op jit(solution)/shard_map/all_to_all | solution.py:390
  53.9 0.6 %finish.1 = bf16[16,256]{1,0:T(8,128)(2,1)} custom-call(bf16[32,8,256]{2,1,0:T(8,128)(2,1)S(1)} %all_to_all.5.parts_ref, bf16[16,256]{1,0:T(8,128)(2,1)S(1)} %get-tuple-element.34.mixed_ref), custom_call_target="tpu_custom_call" | custom-call | tf_op jit(solution)/shard_map/finish/pallas_call | solution.py:391
  (56 shorter events, 2.5 us)
Async XLA Ops:
  0.0 16.3 %slice-start = ((s8[8388608]{0:T(1024)(128)(4,1)}), s8[4194304]{0:T(1024)(128)(4,1)S(1)}, s32[]{:S(2)}) async-start(s8[8388608]{0:T(1024)(128)(4,1)} %bitcast.8), calls=%async_computation.1 | async-start | bytes 8388608
  0.0 16.3 %slice-start.2 = ((s8[8388608]{0:T(1024)(128)(4,1)}), s8[4194304]{0:T(1024)(128)(4,1)S(1)}, s32[]{:S(2)}) async-start(s8[8388608]{0:T(1024)(128)(4,1)} %bitcast.10), calls=%async_computation.3 | async-start | bytes 8388608
  0.0 16.3 %slice-start.1 = ((s8[8388608]{0:T(1024)(128)(4,1)}), s8[4194304]{0:T(1024)(128)(4,1)S(1)}, s32[]{:S(2)}) async-start(s8[8388608]{0:T(1024)(128)(4,1)} %bitcast.8), calls=%async_computation.2 | async-start | bytes 8388608
  0.0 16.3 %slice-start.3 = ((s8[8388608]{0:T(1024)(128)(4,1)}), s8[4194304]{0:T(1024)(128)(4,1)S(1)}, s32[]{:S(2)}) async-start(s8[8388608]{0:T(1024)(128)(4,1)} %bitcast.10), calls=%async_computation.4 | async-start | bytes 8388608
  1.2 4.8 %collective-permute-start = (bf16[16,512]{1,0:T(8,128)(2,1)S(1)}, bf16[16,512]{1,0:T(8,128)(2,1)S(1)}, u32[]{:S(2)}, u32[]{:S(2)}) collective-permute-start(bf16[16,512]{1,0:T(8,128)(2,1)S(1)} %get-tuple-element.22), channel_id=1, source_target_pairs={{0,8},{8,0},{16,24},{24,16},{1,9},{9,1},{17,25},{25,17},{2,10},{10... | collective-permute-start | bytes 49160 | tf_op jit(solution)/shard_map/ppermute | solution.py:42
  4.3 3.7 %collective-permute-start.1 = (bf16[16,512]{1,0:T(8,128)(2,1)S(1)}, bf16[16,512]{1,0:T(8,128)(2,1)S(1)}, u32[]{:S(2)}, u32[]{:S(2)}) collective-permute-start(bf16[16,512]{1,0:T(8,128)(2,1)S(1)} %get-tuple-element.23), channel_id=1, source_target_pairs={{0,16},{8,24},{16,0},{24,8},{1,17},{9,25},{17,1},{25,9},{2,18},{10... | collective-permute-start | bytes 49160 | tf_op jit(solution)/shard_map/ppermute | solution.py:42
  5.8 4.6 %collective-permute-start.2 = (bf16[16,512]{1,0:T(8,128)(2,1)S(1)}, bf16[16,512]{1,0:T(8,128)(2,1)S(1)}, u32[]{:S(2)}, u32[]{:S(2)}) collective-permute-start(bf16[16,512]{1,0:T(8,128)(2,1)S(1)} %get-tuple-element.24), channel_id=1, source_target_pairs={{0,24},{8,16},{16,8},{24,0},{1,25},{9,17},{17,9},{25,1},{2,26},{10... | collective-permute-start | bytes 49160 | tf_op jit(solution)/shard_map/ppermute | solution.py:42
  10.7 4.1 %collective-permute-start.3 = (f32[16,768]{1,0:T(8,128)S(1)}, f32[16,768]{1,0:T(8,128)S(1)}, u32[]{:S(2)}, u32[]{:S(2)}) collective-permute-start(f32[16,768]{1,0:T(8,128)S(1)} %get-tuple-element.26), channel_id=1, source_target_pairs={{0,8},{8,0},{16,24},{24,16},{1,9},{9,1},{17,25},{25,17},{2,10},{10... | collective-permute-start | bytes 147464 | tf_op jit(solution)/shard_map/ppermute | solution.py:42
  11.3 4.1 %collective-permute-start.4 = (f32[16,768]{1,0:T(8,128)S(1)}, f32[16,768]{1,0:T(8,128)S(1)}, u32[]{:S(2)}, u32[]{:S(2)}) collective-permute-start(f32[16,768]{1,0:T(8,128)S(1)} %get-tuple-element.27), channel_id=1, source_target_pairs={{0,16},{8,24},{16,0},{24,8},{1,17},{9,25},{17,1},{25,9},{2,18},{10... | collective-permute-start | bytes 147464 | tf_op jit(solution)/shard_map/ppermute | solution.py:42
  11.4 5.0 %collective-permute-start.5 = (f32[16,768]{1,0:T(8,128)S(1)}, f32[16,768]{1,0:T(8,128)S(1)}, u32[]{:S(2)}, u32[]{:S(2)}) collective-permute-start(f32[16,768]{1,0:T(8,128)S(1)} %get-tuple-element.28), channel_id=1, source_target_pairs={{0,24},{8,16},{16,8},{24,0},{1,25},{9,17},{17,9},{25,1},{2,26},{10... | collective-permute-start | bytes 147464 | tf_op jit(solution)/shard_map/ppermute | solution.py:42
  16.5 22.5 %copy-start = (bf16[1,2048,704]{1,2,0:T(8,128)(2,1)S(1)}, bf16[1,2048,704]{1,2,0:T(8,128)(2,1)}, u32[]{:S(2)}) copy-start(bf16[1,2048,704]{1,2,0:T(8,128)(2,1)} %param.33) | copy-start | bytes 8650756
  16.5 22.5 %copy-start.1 = (bf16[1,2048,704]{1,2,0:T(8,128)(2,1)S(1)}, bf16[1,2048,704]{1,2,0:T(8,128)(2,1)}, u32[]{:S(2)}) copy-start(bf16[1,2048,704]{1,2,0:T(8,128)(2,1)} %param.34) | copy-start | bytes 8650756
  16.5 22.5 %copy-start.2 = (bf16[1,704,2048]{2,1,0:T(8,128)(2,1)S(1)}, bf16[1,704,2048]{2,1,0:T(8,128)(2,1)}, u32[]{:S(2)}) copy-start(bf16[1,704,2048]{2,1,0:T(8,128)(2,1)} %down_ref.1) | copy-start | bytes 8650756
  16.5 22.5 %copy-start.11 = (s32[64,2]{0,1:T(2,128)S(1)}, s32[64,2]{0,1:T(2,128)}, u32[]{:S(2)}) copy-start(s32[64,2]{0,1:T(2,128)} %param.31) | copy-start | bytes 1540
  16.5 22.5 %copy-start.12 = (f32[64,2]{0,1:T(2,128)S(1)}, f32[64,2]{0,1:T(2,128)}, u32[]{:S(2)}) copy-start(f32[64,2]{0,1:T(2,128)} %param.32) | copy-start | bytes 1540
  20.0 1.3 %collective-permute-start.6 = (bf16[16,1024]{1,0:T(8,128)(2,1)S(1)}, bf16[16,1024]{1,0:T(8,128)(2,1)S(1)}, u32[]{:S(2)}, u32[]{:S(2)}) collective-permute-start(bf16[16,1024]{1,0:T(8,128)(2,1)S(1)} %get-tuple-element.30), channel_id=1, source_target_pairs={{0,1},{1,0},{2,3},{3,2},{4,5},{5,4},{6,7},{7,6},{8,9},{9,8},{10,11... | collective-permute-start | bytes 98312 | tf_op jit(solution)/shard_map/ppermute | solution.py:360
  21.3 6.0 %collective-permute-start.9 = (bf16[16,1024]{1,0:T(8,128)(2,1)S(1)}, bf16[16,1024]{1,0:T(8,128)(2,1)S(1)}, u32[]{:S(2)}, u32[]{:S(2)}) collective-permute-start(bf16[16,1024]{1,0:T(8,128)(2,1)S(1)} %pair.1.refs_0_), channel_id=1, source_target_pairs={{0,6},{1,7},{2,4},{3,5},{4,2},{5,3},{6,0},{7,1},{8,14},{9,15},{10,... | collective-permute-start | bytes 98312 | tf_op jit(solution)/shard_map/ppermute | solution.py:42
  25.4 4.8 %collective-permute-start.8 = (bf16[16,1024]{1,0:T(8,128)(2,1)S(1)}, bf16[16,1024]{1,0:T(8,128)(2,1)S(1)}, u32[]{:S(2)}, u32[]{:S(2)}) collective-permute-start(bf16[16,1024]{1,0:T(8,128)(2,1)S(1)} %pair.1.refs_0_), channel_id=1, source_target_pairs={{0,4},{1,5},{2,6},{3,7},{4,0},{5,1},{6,2},{7,3},{8,12},{9,13},{10,... | collective-permute-start | bytes 98312 | tf_op jit(solution)/shard_map/ppermute | solution.py:42
  25.4 4.8 %collective-permute-start.7 = (bf16[16,1024]{1,0:T(8,128)(2,1)S(1)}, bf16[16,1024]{1,0:T(8,128)(2,1)S(1)}, u32[]{:S(2)}, u32[]{:S(2)}) collective-permute-start(bf16[16,1024]{1,0:T(8,128)(2,1)S(1)} %pair.1.refs_0_), channel_id=1, source_target_pairs={{0,2},{1,3},{2,0},{3,1},{4,6},{5,7},{6,4},{7,5},{8,10},{9,11},{10,... | collective-permute-start | bytes 98312 | tf_op jit(solution)/shard_map/ppermute | solution.py:42
  30.3 1.3 %collective-permute-start.10 = (bf16[16,1024]{1,0:T(8,128)(2,1)S(1)}, bf16[16,1024]{1,0:T(8,128)(2,1)S(1)}, u32[]{:S(2)}, u32[]{:S(2)}) collective-permute-start(bf16[16,1024]{1,0:T(8,128)(2,1)S(1)} %mix.1.near_ref), channel_id=1, source_target_pairs={{0,1},{1,0},{2,3},{3,2},{4,5},{5,4},{6,7},{7,6},{8,9},{9,8},{10,11... | collective-permute-start | bytes 98312 | tf_op jit(solution)/shard_map/ppermute | solution.py:365
  31.7 5.3 %collective-permute-start.13 = (bf16[16,2048]{1,0:T(8,128)(2,1)S(1)}, bf16[16,2048]{1,0:T(8,128)(2,1)S(1)}, u32[]{:S(2)}, u32[]{:S(2)}) collective-permute-start(bf16[16,2048]{1,0:T(8,128)(2,1)S(1)} %get-tuple-element.31.refs_0_), channel_id=1, source_target_pairs={{0,24},{8,16},{16,8},{24,0},{1,25},{9,17},{17,9},{25,1},{2,26},{10... | collective-permute-start | bytes 196616 | tf_op jit(solution)/shard_map/ppermute | solution.py:42
  34.2 4.3 %collective-permute-start.12 = (bf16[16,2048]{1,0:T(8,128)(2,1)S(1)}, bf16[16,2048]{1,0:T(8,128)(2,1)S(1)}, u32[]{:S(2)}, u32[]{:S(2)}) collective-permute-start(bf16[16,2048]{1,0:T(8,128)(2,1)S(1)} %get-tuple-element.31.refs_0_), channel_id=1, source_target_pairs={{0,16},{8,24},{16,0},{24,8},{1,17},{9,25},{17,1},{25,9},{2,18},{10... | collective-permute-start | bytes 196616 | tf_op jit(solution)/shard_map/ppermute | solution.py:42
  34.7 4.3 %collective-permute-start.11 = (bf16[16,2048]{1,0:T(8,128)(2,1)S(1)}, bf16[16,2048]{1,0:T(8,128)(2,1)S(1)}, u32[]{:S(2)}, u32[]{:S(2)}) collective-permute-start(bf16[16,2048]{1,0:T(8,128)(2,1)S(1)} %get-tuple-element.31.refs_0_), channel_id=1, source_target_pairs={{0,8},{8,0},{16,24},{24,16},{1,9},{9,1},{17,25},{25,17},{2,10},{10... | collective-permute-start | bytes 196616 | tf_op jit(solution)/shard_map/ppermute | solution.py:42
  41.1 1.4 %collective-permute-start.14 = (bf16[32,8,256]{2,1,0:T(8,128)(2,1)S(1)}, bf16[32,8,256]{2,1,0:T(8,128)(2,1)S(1)}, u32[]{:S(2)}, u32[]{:S(2)}) collective-permute-start(bf16[32,8,256]{2,1,0:T(8,128)(2,1)S(1)} %get-tuple-element.33), channel_id=1, source_target_pairs={{0,1},{1,0},{2,3},{3,2},{4,5},{5,4},{6,7},{7,6},{8,9},{9,8},{10,11... | collective-permute-start | bytes 393224 | tf_op jit(solution)/shard_map/ppermute | solution.py:388
  (10 other events, 141.8 us)

commit v6 on v5

--- a/solution.py
+++ b/solution.py
@@ -35,14 +35,17 @@
     return floats * lax.rsqrt(jnp.mean(floats * floats, axis=-1, keepdims=True) + 1e-06) * gain
 
 
-def exchange(items, axis, paired, stride=1):
+def exchange(items, axis, paired, stride=1, steps=None):
     size = len(items)
+    steps = steps or range(size)
     if paired:
         return [items[0]] + [
             lax.ppermute(
-                items[step], axis, [(one, one ^ step * stride) for one in range(size * stride)]
+                items[index],
+                axis,
+                [(one, one ^ steps[index] * stride) for one in range(size * stride)],
             )
-            for step in range(1, size)
+            for index in range(1, size)
         ]
     members = [list(range(first, size * stride, stride)) for first in range(stride)]
     received = lax.all_to_all(
@@ -57,7 +60,7 @@
     return parts[0]
 
 
-def norm_kernel(stream_hbm, gain_hbm, *refs, paired):
+def norm_kernel(stream_hbm, gain_hbm, *refs, paired, steps):
     normed_ref, *out_refs, stream_ref, gain_ref, sems = refs
     copies = [
         pltpu.make_async_copy(stream_hbm, stream_ref, sems.at[0]),
@@ -70,7 +73,7 @@
     width = out_refs[0].shape[1]
     normed_ref[...] = normalized(stream_ref[...].astype(F32), gain_ref[...]).astype(BF16)
     for index, out_ref in enumerate(out_refs):
-        group = lax.axis_index("ep") ^ index if paired else index
+        group = lax.axis_index("ep") ^ steps[index] if paired else index
         out_ref[...] = normed_ref[:, pl.ds(pl.multiple_of(group * width, width), width)]
 
 
@@ -312,8 +315,9 @@
     in_smem = pl.BlockSpec(memory_space=pltpu.SMEM)
 
     paired = groups in (2, 4)
+    steps = (0, 3, 1, 2) if groups == 4 else tuple(range(groups))
     normed, *blocks = call(
-        functools.partial(norm_kernel, paired=paired),
+        functools.partial(norm_kernel, paired=paired, steps=steps),
         "norm",
         2 * MIB,
         [shape(stream.shape, BF16)] + [shape((count, model_width // groups), BF16)] * groups,
@@ -328,11 +332,11 @@
         pltpu.with_memory_space_constraint(stream, pltpu.HBM),
         pltpu.with_memory_space_constraint(norm_gain_attn.reshape(1, -1), pltpu.HBM),
     )
-    blocks = exchange(blocks, "ep", paired)
+    blocks = exchange(blocks, "ep", paired, steps=steps)
     parts = call(
         project_kernel, "project", 4 * MIB, [shape((count, 3 * width), F32)] * groups
     )(*blocks, w_query, w_key, w_value)
-    parts = exchange(parts, "ep", paired)
+    parts = exchange(parts, "ep", paired, steps=steps)
     swap = [(one, one ^ 1) for one in range(pieces)]
     side = shape((count, model_width // 2), BF16)
     keep, give = call(

time: 54.7 us -> 53.8 us (0.984)
  waiting for transfers between devices: 18.3 us -> 17.4 us
    ppermute x12, waiting for transfers between devices: 14.6 us -> 13.7 us  [exchange(): lax.ppermute(items[index], axis, [(one, one ^ steps[index] * stride) for...]
where the time goes in v6:
time: 53.8 us; the launch traced here: 53.6 us
  waiting for transfers between devices  17.4 us (32%)
  starting transfers between devices  16.7 us (31%)
  blocking collectives  11.3 us (21%)
  Pallas kernels  7.85 us (15%)
    ppermute x12, starting transfers between devices, exchange(): lax.ppermute(items[index], axis, [(one, one ^ steps[index] * stride) for...  16.5 us
    ppermute x12, waiting for transfers between devices, exchange(): lax.ppermute(items[index], axis, [(one, one ^ steps[index] * stride) for...  13.7 us
    all_to_all x1, blocking collectives, shards(): returned = lax.all_to_all(summed, ('ep', 'tp'), 0, 0, tiled=True)  11.3 us
    pallas_call x1, Pallas kernels, shards(): call(attend_kernel, 'attend', 4 * MIB, [shape(side.shape, F32), side], in...  3.48 us
    ppermute x2, waiting for transfers between devices, shards(): taken = lax.ppermute(give, 'tp', swap)  2.53 us
    pallas_call x1, Pallas kernels, shards(): call(functools.partial(expert_kernel, groups=groups, paired=paired), 'exp...  2.14 us
    ppermute x1, waiting for transfers between devices, shards(): far = lax.ppermute(near, 'tp', swap)  1.19 us
    pallas_call x1, Pallas kernels, shards(): call(functools.partial(norm_kernel, paired=paired, steps=steps), 'norm',...  1.13 us
  transfers between devices with their start and end apart: 15, of which 14 were waited for; matrix products, arithmetic and copies ran while one was open for 0% of the time, Pallas kernels for 0%

profile of v6, /device:TPU:0, one launch (start us, length us, event | category | flops | bytes accessed | tf_op | source)
XLA Modules:
  0.0 53.6 jit_solution(10507453130057781742)
XLA Ops:
  0.1 1.1 %norm.1 = (bf16[16,2048]{1,0:T(8,128)(2,1)S(1)}, bf16[16,512]{1,0:T(8,128)(2,1)S(1)}, bf16[16,512]{1,0:T(8,128)(2,1)S(1)}, bf16[16,512]{1,0:T(8,128)(2,1)S(1)}, bf16[16,512]{1,0:T(8,128)(2,1)S(1)}) custom-call(bf16[16,2048]{1,0:T(8,128)(2,1)} %stream_ref.1, f32[1,2048]{1,0:T(1,128)} %bitcast.19), custom_call_target="tpu_custom_call" | custom-call | flops 40000000000 | tf_op jit(solution)/shard_map/norm/pallas_call | solution.py:319
  1.2 4.0 %collective-permute-start = (bf16[16,512]{1,0:T(8,128)(2,1)S(1)}, bf16[16,512]{1,0:T(8,128)(2,1)S(1)}, u32[]{:S(2)}, u32[]{:S(2)}) collective-permute-start(bf16[16,512]{1,0:T(8,128)(2,1)S(1)} %get-tuple-element.22), channel_id=1, source_target_pairs={{0,24},{8,16},{16,8},{24,0},{1,25},{9,17},{17,9},{25,1},{2,26},{10... | collective-permute-start | bytes 49160 | tf_op jit(solution)/shard_map/ppermute | solution.py:43
  5.2 0.5 collective-permute-start.1
  5.9 1.1 %collective-permute-done.refs_1_ = bf16[16,512]{1,0:T(8,128)(2,1)S(1)} collective-permute-done((bf16[16,512]{1,0:T(8,128)(2,1)S(1)}, bf16[16,512]{1,0:T(8,128)(2,1)S(1)}, u32[]{:S(2)}, u32[]{:S(2)}) %collective-permute-start) | collective-permute-done | bytes 16416 | tf_op jit(solution)/shard_map/ppermute | solution.py:43
  7.0 2.0 %collective-permute-done.1.refs_2_ = bf16[16,512]{1,0:T(8,128)(2,1)S(1)} collective-permute-done((bf16[16,512]{1,0:T(8,128)(2,1)S(1)}, bf16[16,512]{1,0:T(8,128)(2,1)S(1)}, u32[]{:S(2)}, u32[]{:S(2)}) %collective-permute-start.1) | collective-permute-done | bytes 16416 | tf_op jit(solution)/shard_map/ppermute | solution.py:43
  9.0 0.5 collective-permute-done.2.refs_3_
  9.8 1.5 %collective-permute-start.3 = (f32[16,768]{1,0:T(8,128)S(1)}, f32[16,768]{1,0:T(8,128)S(1)}, u32[]{:S(2)}, u32[]{:S(2)}) collective-permute-start(f32[16,768]{1,0:T(8,128)S(1)} %get-tuple-element.26), channel_id=1, source_target_pairs={{0,24},{8,16},{16,8},{24,0},{1,25},{9,17},{17,9},{25,1},{2,26},{10... | collective-permute-start | bytes 147464 | tf_op jit(solution)/shard_map/ppermute | solution.py:43
  11.4 1.9 %collective-permute-start.5 = (f32[16,768]{1,0:T(8,128)S(1)}, f32[16,768]{1,0:T(8,128)S(1)}, u32[]{:S(2)}, u32[]{:S(2)}) collective-permute-start(f32[16,768]{1,0:T(8,128)S(1)} %get-tuple-element.28), channel_id=1, source_target_pairs={{0,16},{8,24},{16,0},{24,8},{1,17},{9,25},{17,1},{25,9},{2,18},{10... | collective-permute-start | bytes 147464 | tf_op jit(solution)/shard_map/ppermute | solution.py:43
  13.3 1.5 %collective-permute-done.3.refs_1_ = f32[16,768]{1,0:T(8,128)S(1)} collective-permute-done((f32[16,768]{1,0:T(8,128)S(1)}, f32[16,768]{1,0:T(8,128)S(1)}, u32[]{:S(2)}, u32[]{:S(2)}) %collective-permute-start.3) | collective-permute-done | bytes 49184 | tf_op jit(solution)/shard_map/ppermute | solution.py:43
  15.7 3.5 %attend.1 = (f32[16,1024]{1,0:T(8,128)S(1)}, bf16[16,1024]{1,0:T(8,128)(2,1)S(1)}) custom-call(s32[16]{0:T(128)S(1)} %copy-done.13, bf16[16,2048]{1,0:T(8,128)(2,1)S(1)} %get-tuple-element.20.normed_ref, bf16[16,2048]{1,0:T(8,128)(2,1)S(1)} %bitcast.14, f32[1,16]{1,0:T(1,128)S(1)} %bitcast.18, f32[16,2,1024]{2,1,0:T(2,128)S(1)} %copy-done.7, ...), custom_call_target="tpu_custom_call" | custom-call | tf_op jit(solution)/shard_map/attend/pallas_call | solution.py:342
  19.2 1.2 %collective-permute-done.6.taken_ref = bf16[16,1024]{1,0:T(8,128)(2,1)S(1)} collective-permute-done((bf16[16,1024]{1,0:T(8,128)(2,1)S(1)}, bf16[16,1024]{1,0:T(8,128)(2,1)S(1)}, u32[]{:S(2)}, u32[]{:S(2)}) %collective-permute-start.6) | collective-permute-done | bytes 32800 | tf_op jit(solution)/shard_map/ppermute | solution.py:364
  20.4 4.1 %collective-permute-start.9 = (bf16[16,1024]{1,0:T(8,128)(2,1)S(1)}, bf16[16,1024]{1,0:T(8,128)(2,1)S(1)}, u32[]{:S(2)}, u32[]{:S(2)}) collective-permute-start(bf16[16,1024]{1,0:T(8,128)(2,1)S(1)} %pair.1.refs_0_), channel_id=1, source_target_pairs={{0,6},{1,7},{2,4},{3,5},{4,2},{5,3},{6,0},{7,1},{8,14},{9,15},{10,... | collective-permute-start | bytes 98312 | tf_op jit(solution)/shard_map/ppermute | solution.py:43
  24.5 0.6 %collective-permute-start.7 = (bf16[16,1024]{1,0:T(8,128)(2,1)S(1)}, bf16[16,1024]{1,0:T(8,128)(2,1)S(1)}, u32[]{:S(2)}, u32[]{:S(2)}) collective-permute-start(bf16[16,1024]{1,0:T(8,128)(2,1)S(1)} %pair.1.refs_0_), channel_id=1, source_target_pairs={{0,2},{1,3},{2,0},{3,1},{4,6},{5,7},{6,4},{7,5},{8,10},{9,11},{10,... | collective-permute-start | bytes 98312 | tf_op jit(solution)/shard_map/ppermute | solution.py:43
  25.1 1.3 %collective-permute-done.9.refs_3_ = bf16[16,1024]{1,0:T(8,128)(2,1)S(1)} collective-permute-done((bf16[16,1024]{1,0:T(8,128)(2,1)S(1)}, bf16[16,1024]{1,0:T(8,128)(2,1)S(1)}, u32[]{:S(2)}, u32[]{:S(2)}) %collective-permute-start.9) | collective-permute-done | bytes 32800 | tf_op jit(solution)/shard_map/ppermute | solution.py:43
  26.4 2.9 %collective-permute-done.8.refs_2_ = bf16[16,1024]{1,0:T(8,128)(2,1)S(1)} collective-permute-done((bf16[16,1024]{1,0:T(8,128)(2,1)S(1)}, bf16[16,1024]{1,0:T(8,128)(2,1)S(1)}, u32[]{:S(2)}, u32[]{:S(2)}) %collective-permute-start.8) | collective-permute-done | bytes 32800 | tf_op jit(solution)/shard_map/ppermute | solution.py:43
  29.4 1.2 %collective-permute-done.10.far_ref = bf16[16,1024]{1,0:T(8,128)(2,1)S(1)} collective-permute-done((bf16[16,1024]{1,0:T(8,128)(2,1)S(1)}, bf16[16,1024]{1,0:T(8,128)(2,1)S(1)}, u32[]{:S(2)}, u32[]{:S(2)}) %collective-permute-start.10) | collective-permute-done | bytes 32800 | tf_op jit(solution)/shard_map/ppermute | solution.py:369
  30.8 2.5 %collective-permute-start.13 = (bf16[16,2048]{1,0:T(8,128)(2,1)S(1)}, bf16[16,2048]{1,0:T(8,128)(2,1)S(1)}, u32[]{:S(2)}, u32[]{:S(2)}) collective-permute-start(bf16[16,2048]{1,0:T(8,128)(2,1)S(1)} %get-tuple-element.31.refs_0_), channel_id=1, source_target_pairs={{0,24},{8,16},{16,8},{24,0},{1,25},{9,17},{17,9},{25,1},{2,26},{10... | collective-permute-start | bytes 196616 | tf_op jit(solution)/shard_map/ppermute | solution.py:43
  33.8 0.5 %collective-permute-start.11 = (bf16[16,2048]{1,0:T(8,128)(2,1)S(1)}, bf16[16,2048]{1,0:T(8,128)(2,1)S(1)}, u32[]{:S(2)}, u32[]{:S(2)}) collective-permute-start(bf16[16,2048]{1,0:T(8,128)(2,1)S(1)} %get-tuple-element.31.refs_0_), channel_id=1, source_target_pairs={{0,8},{8,0},{16,24},{24,16},{1,9},{9,1},{17,25},{25,17},{2,10},{10... | collective-permute-start | bytes 196616 | tf_op jit(solution)/shard_map/ppermute | solution.py:43
  34.3 1.7 %collective-permute-done.13.refs_3_ = bf16[16,2048]{1,0:T(8,128)(2,1)S(1)} collective-permute-done((bf16[16,2048]{1,0:T(8,128)(2,1)S(1)}, bf16[16,2048]{1,0:T(8,128)(2,1)S(1)}, u32[]{:S(2)}, u32[]{:S(2)}) %collective-permute-start.13) | collective-permute-done | bytes 65568 | tf_op jit(solution)/shard_map/ppermute | solution.py:43
  36.0 1.5 %collective-permute-done.12.refs_2_ = bf16[16,2048]{1,0:T(8,128)(2,1)S(1)} collective-permute-done((bf16[16,2048]{1,0:T(8,128)(2,1)S(1)}, bf16[16,2048]{1,0:T(8,128)(2,1)S(1)}, u32[]{:S(2)}, u32[]{:S(2)}) %collective-permute-start.12) | collective-permute-done | bytes 65568 | tf_op jit(solution)/shard_map/ppermute | solution.py:43
  38.1 2.1 %experts.1 = (bf16[32,8,256]{2,1,0:T(8,128)(2,1)S(1)}, bf16[32,8,256]{2,1,0:T(8,128)(2,1)S(1)}) custom-call(s32[2,64]{1,0:T(2,128)S(1)} %bitcast.16, f32[2,64]{1,0:T(2,128)S(1)} %bitcast.17, bf16[1,704,2048]{2,1,0:T(8,128)(2,1)S(1)} %bitcast.12, bf16[1,704,2048]{2,1,0:T(8,128)(2,1)S(1)} %bitcast.13, bf16[1,704,2048]{2,1,0:T(8,128)(2,1)S(1)} %copy-done.2, ...), custom_call_target="tpu_custom_call" | custom-call | tf_op jit(solution)/shard_map/experts/pallas_call | solution.py:379
  40.3 1.3 %collective-permute-done.14.taken_ref = bf16[32,8,256]{2,1,0:T(8,128)(2,1)S(1)} collective-permute-done((bf16[32,8,256]{2,1,0:T(8,128)(2,1)S(1)}, bf16[32,8,256]{2,1,0:T(8,128)(2,1)S(1)}, u32[]{:S(2)}, u32[]{:S(2)}) %collective-permute-start.14) | collective-permute-done | bytes 131104 | tf_op jit(solution)/shard_map/ppermute | solution.py:392
  41.7 11.3 %all_to_all.5.parts_ref = bf16[32,8,256]{2,1,0:T(8,128)(2,1)S(1)} all-to-all(bf16[32,8,256]{2,1,0:T(8,128)(2,1)S(1)} %sides.1), channel_id=1, replica_groups=mesh['ep'=4,'tp'=8] {'ep','tp'}, dimensions={0} | all-to-all | bytes 262144 | tf_op jit(solution)/shard_map/all_to_all | solution.py:394
  53.0 0.6 %finish.1 = bf16[16,256]{1,0:T(8,128)(2,1)} custom-call(bf16[32,8,256]{2,1,0:T(8,128)(2,1)S(1)} %all_to_all.5.parts_ref, bf16[16,256]{1,0:T(8,128)(2,1)S(1)} %get-tuple-element.34.mixed_ref), custom_call_target="tpu_custom_call" | custom-call | tf_op jit(solution)/shard_map/finish/pallas_call | solution.py:395
  (56 shorter events, 2.7 us)
Async XLA Ops:
  0.0 15.5 %slice-start = ((s8[8388608]{0:T(1024)(128)(4,1)}), s8[4194304]{0:T(1024)(128)(4,1)S(1)}, s32[]{:S(2)}) async-start(s8[8388608]{0:T(1024)(128)(4,1)} %bitcast.8), calls=%async_computation.1 | async-start | bytes 8388608
  0.0 15.5 %slice-start.2 = ((s8[8388608]{0:T(1024)(128)(4,1)}), s8[4194304]{0:T(1024)(128)(4,1)S(1)}, s32[]{:S(2)}) async-start(s8[8388608]{0:T(1024)(128)(4,1)} %bitcast.10), calls=%async_computation.3 | async-start | bytes 8388608
  0.0 15.5 %slice-start.1 = ((s8[8388608]{0:T(1024)(128)(4,1)}), s8[4194304]{0:T(1024)(128)(4,1)S(1)}, s32[]{:S(2)}) async-start(s8[8388608]{0:T(1024)(128)(4,1)} %bitcast.8), calls=%async_computation.2 | async-start | bytes 8388608
  0.0 15.5 %slice-start.3 = ((s8[8388608]{0:T(1024)(128)(4,1)}), s8[4194304]{0:T(1024)(128)(4,1)S(1)}, s32[]{:S(2)}) async-start(s8[8388608]{0:T(1024)(128)(4,1)} %bitcast.10), calls=%async_computation.4 | async-start | bytes 8388608
  1.2 5.7 %collective-permute-start = (bf16[16,512]{1,0:T(8,128)(2,1)S(1)}, bf16[16,512]{1,0:T(8,128)(2,1)S(1)}, u32[]{:S(2)}, u32[]{:S(2)}) collective-permute-start(bf16[16,512]{1,0:T(8,128)(2,1)S(1)} %get-tuple-element.22), channel_id=1, source_target_pairs={{0,24},{8,16},{16,8},{24,0},{1,25},{9,17},{17,9},{25,1},{2,26},{10... | collective-permute-start | bytes 49160 | tf_op jit(solution)/shard_map/ppermute | solution.py:43
  5.2 3.7 %collective-permute-start.1 = (bf16[16,512]{1,0:T(8,128)(2,1)S(1)}, bf16[16,512]{1,0:T(8,128)(2,1)S(1)}, u32[]{:S(2)}, u32[]{:S(2)}) collective-permute-start(bf16[16,512]{1,0:T(8,128)(2,1)S(1)} %get-tuple-element.23), channel_id=1, source_target_pairs={{0,8},{8,0},{16,24},{24,16},{1,9},{9,1},{17,25},{25,17},{2,10},{10... | collective-permute-start | bytes 49160 | tf_op jit(solution)/shard_map/ppermute | solution.py:43
  5.8 3.7 %collective-permute-start.2 = (bf16[16,512]{1,0:T(8,128)(2,1)S(1)}, bf16[16,512]{1,0:T(8,128)(2,1)S(1)}, u32[]{:S(2)}, u32[]{:S(2)}) collective-permute-start(bf16[16,512]{1,0:T(8,128)(2,1)S(1)} %get-tuple-element.24), channel_id=1, source_target_pairs={{0,16},{8,24},{16,0},{24,8},{1,17},{9,25},{17,1},{25,9},{2,18},{10... | collective-permute-start | bytes 49160 | tf_op jit(solution)/shard_map/ppermute | solution.py:43
  9.8 5.0 %collective-permute-start.3 = (f32[16,768]{1,0:T(8,128)S(1)}, f32[16,768]{1,0:T(8,128)S(1)}, u32[]{:S(2)}, u32[]{:S(2)}) collective-permute-start(f32[16,768]{1,0:T(8,128)S(1)} %get-tuple-element.26), channel_id=1, source_target_pairs={{0,24},{8,16},{16,8},{24,0},{1,25},{9,17},{17,9},{25,1},{2,26},{10... | collective-permute-start | bytes 147464 | tf_op jit(solution)/shard_map/ppermute | solution.py:43
  11.3 4.1 %collective-permute-start.4 = (f32[16,768]{1,0:T(8,128)S(1)}, f32[16,768]{1,0:T(8,128)S(1)}, u32[]{:S(2)}, u32[]{:S(2)}) collective-permute-start(f32[16,768]{1,0:T(8,128)S(1)} %get-tuple-element.27), channel_id=1, source_target_pairs={{0,8},{8,0},{16,24},{24,16},{1,9},{9,1},{17,25},{25,17},{2,10},{10... | collective-permute-start | bytes 147464 | tf_op jit(solution)/shard_map/ppermute | solution.py:43
  11.4 4.1 %collective-permute-start.5 = (f32[16,768]{1,0:T(8,128)S(1)}, f32[16,768]{1,0:T(8,128)S(1)}, u32[]{:S(2)}, u32[]{:S(2)}) collective-permute-start(f32[16,768]{1,0:T(8,128)S(1)} %get-tuple-element.28), channel_id=1, source_target_pairs={{0,16},{8,24},{16,0},{24,8},{1,17},{9,25},{17,1},{25,9},{2,18},{10... | collective-permute-start | bytes 147464 | tf_op jit(solution)/shard_map/ppermute | solution.py:43
  15.6 22.4 %copy-start = (bf16[1,2048,704]{1,2,0:T(8,128)(2,1)S(1)}, bf16[1,2048,704]{1,2,0:T(8,128)(2,1)}, u32[]{:S(2)}) copy-start(bf16[1,2048,704]{1,2,0:T(8,128)(2,1)} %param.33) | copy-start | bytes 8650756
  15.6 22.4 %copy-start.1 = (bf16[1,2048,704]{1,2,0:T(8,128)(2,1)S(1)}, bf16[1,2048,704]{1,2,0:T(8,128)(2,1)}, u32[]{:S(2)}) copy-start(bf16[1,2048,704]{1,2,0:T(8,128)(2,1)} %param.34) | copy-start | bytes 8650756
  15.6 22.4 %copy-start.2 = (bf16[1,704,2048]{2,1,0:T(8,128)(2,1)S(1)}, bf16[1,704,2048]{2,1,0:T(8,128)(2,1)}, u32[]{:S(2)}) copy-start(bf16[1,704,2048]{2,1,0:T(8,128)(2,1)} %down_ref.1) | copy-start | bytes 8650756
  15.7 22.4 %copy-start.11 = (s32[64,2]{0,1:T(2,128)S(1)}, s32[64,2]{0,1:T(2,128)}, u32[]{:S(2)}) copy-start(s32[64,2]{0,1:T(2,128)} %param.31) | copy-start | bytes 1540
  15.7 22.4 %copy-start.12 = (f32[64,2]{0,1:T(2,128)S(1)}, f32[64,2]{0,1:T(2,128)}, u32[]{:S(2)}) copy-start(f32[64,2]{0,1:T(2,128)} %param.32) | copy-start | bytes 1540
  19.2 1.3 %collective-permute-start.6 = (bf16[16,1024]{1,0:T(8,128)(2,1)S(1)}, bf16[16,1024]{1,0:T(8,128)(2,1)S(1)}, u32[]{:S(2)}, u32[]{:S(2)}) collective-permute-start(bf16[16,1024]{1,0:T(8,128)(2,1)S(1)} %get-tuple-element.30), channel_id=1, source_target_pairs={{0,1},{1,0},{2,3},{3,2},{4,5},{5,4},{6,7},{7,6},{8,9},{9,8},{10,11... | collective-permute-start | bytes 98312 | tf_op jit(solution)/shard_map/ppermute | solution.py:364
  20.4 6.0 %collective-permute-start.9 = (bf16[16,1024]{1,0:T(8,128)(2,1)S(1)}, bf16[16,1024]{1,0:T(8,128)(2,1)S(1)}, u32[]{:S(2)}, u32[]{:S(2)}) collective-permute-start(bf16[16,1024]{1,0:T(8,128)(2,1)S(1)} %pair.1.refs_0_), channel_id=1, source_target_pairs={{0,6},{1,7},{2,4},{3,5},{4,2},{5,3},{6,0},{7,1},{8,14},{9,15},{10,... | collective-permute-start | bytes 98312 | tf_op jit(solution)/shard_map/ppermute | solution.py:43
  24.5 4.8 %collective-permute-start.8 = (bf16[16,1024]{1,0:T(8,128)(2,1)S(1)}, bf16[16,1024]{1,0:T(8,128)(2,1)S(1)}, u32[]{:S(2)}, u32[]{:S(2)}) collective-permute-start(bf16[16,1024]{1,0:T(8,128)(2,1)S(1)} %pair.1.refs_0_), channel_id=1, source_target_pairs={{0,4},{1,5},{2,6},{3,7},{4,0},{5,1},{6,2},{7,3},{8,12},{9,13},{10,... | collective-permute-start | bytes 98312 | tf_op jit(solution)/shard_map/ppermute | solution.py:43
  24.5 4.8 %collective-permute-start.7 = (bf16[16,1024]{1,0:T(8,128)(2,1)S(1)}, bf16[16,1024]{1,0:T(8,128)(2,1)S(1)}, u32[]{:S(2)}, u32[]{:S(2)}) collective-permute-start(bf16[16,1024]{1,0:T(8,128)(2,1)S(1)} %pair.1.refs_0_), channel_id=1, source_target_pairs={{0,2},{1,3},{2,0},{3,1},{4,6},{5,7},{6,4},{7,5},{8,10},{9,11},{10,... | collective-permute-start | bytes 98312 | tf_op jit(solution)/shard_map/ppermute | solution.py:43
  29.4 1.3 %collective-permute-start.10 = (bf16[16,1024]{1,0:T(8,128)(2,1)S(1)}, bf16[16,1024]{1,0:T(8,128)(2,1)S(1)}, u32[]{:S(2)}, u32[]{:S(2)}) collective-permute-start(bf16[16,1024]{1,0:T(8,128)(2,1)S(1)} %mix.1.near_ref), channel_id=1, source_target_pairs={{0,1},{1,0},{2,3},{3,2},{4,5},{5,4},{6,7},{7,6},{8,9},{9,8},{10,11... | collective-permute-start | bytes 98312 | tf_op jit(solution)/shard_map/ppermute | solution.py:369
  30.8 5.3 %collective-permute-start.13 = (bf16[16,2048]{1,0:T(8,128)(2,1)S(1)}, bf16[16,2048]{1,0:T(8,128)(2,1)S(1)}, u32[]{:S(2)}, u32[]{:S(2)}) collective-permute-start(bf16[16,2048]{1,0:T(8,128)(2,1)S(1)} %get-tuple-element.31.refs_0_), channel_id=1, source_target_pairs={{0,24},{8,16},{16,8},{24,0},{1,25},{9,17},{17,9},{25,1},{2,26},{10... | collective-permute-start | bytes 196616 | tf_op jit(solution)/shard_map/ppermute | solution.py:43
  33.3 4.3 %collective-permute-start.12 = (bf16[16,2048]{1,0:T(8,128)(2,1)S(1)}, bf16[16,2048]{1,0:T(8,128)(2,1)S(1)}, u32[]{:S(2)}, u32[]{:S(2)}) collective-permute-start(bf16[16,2048]{1,0:T(8,128)(2,1)S(1)} %get-tuple-element.31.refs_0_), channel_id=1, source_target_pairs={{0,16},{8,24},{16,0},{24,8},{1,17},{9,25},{17,1},{25,9},{2,18},{10... | collective-permute-start | bytes 196616 | tf_op jit(solution)/shard_map/ppermute | solution.py:43
  33.8 4.3 %collective-permute-start.11 = (bf16[16,2048]{1,0:T(8,128)(2,1)S(1)}, bf16[16,2048]{1,0:T(8,128)(2,1)S(1)}, u32[]{:S(2)}, u32[]{:S(2)}) collective-permute-start(bf16[16,2048]{1,0:T(8,128)(2,1)S(1)} %get-tuple-element.31.refs_0_), channel_id=1, source_target_pairs={{0,8},{8,0},{16,24},{24,16},{1,9},{9,1},{17,25},{25,17},{2,10},{10... | collective-permute-start | bytes 196616 | tf_op jit(solution)/shard_map/ppermute | solution.py:43
  40.2 1.4 %collective-permute-start.14 = (bf16[32,8,256]{2,1,0:T(8,128)(2,1)S(1)}, bf16[32,8,256]{2,1,0:T(8,128)(2,1)S(1)}, u32[]{:S(2)}, u32[]{:S(2)}) collective-permute-start(bf16[32,8,256]{2,1,0:T(8,128)(2,1)S(1)} %get-tuple-element.33), channel_id=1, source_target_pairs={{0,1},{1,0},{2,3},{3,2},{4,5},{5,4},{6,7},{7,6},{8,9},{9,8},{10,11... | collective-permute-start | bytes 393224 | tf_op jit(solution)/shard_map/ppermute | solution.py:392
  (10 other events, 134.7 us)

commit v7 on v6

--- a/solution.py
+++ b/solution.py
@@ -83,10 +83,15 @@
     count = block_refs[0].shape[0]
     width = weight_refs[0].shape[1]
     rows = jnp.concatenate([block_ref[...] for block_ref in block_refs], axis=0)
-    for index, weight_ref in enumerate(weight_refs):
-        part = jnp.dot(rows, weight_ref[...], preferred_element_type=F32)
-        for group, out_ref in enumerate(out_refs):
-            out_ref[:, index * width : (index + 1) * width] = part[
+    query, key, value = [
+        jnp.dot(rows, weight_ref[...], preferred_element_type=F32) for weight_ref in weight_refs
+    ]
+    high = query.astype(BF16)
+    low = (query - high.astype(F32)).astype(BF16)
+    terms = (high, low, key.astype(BF16), value.astype(BF16))
+    for group, out_ref in enumerate(out_refs):
+        for index, term in enumerate(terms):
+            out_ref[:, index * width : (index + 1) * width] = term[
                 group * count : (group + 1) * count
             ]
 
@@ -115,12 +120,12 @@
     )
     head_ids = lax.broadcasted_iota(jnp.int32, forget_all.shape, 1)
     first_head = lax.axis_index("tp") * heads
-    total = part_refs[0][...]
+    total = part_refs[0][...].astype(F32)
     for part_ref in part_refs[1:]:
-        total = total + part_ref[...]
-    query = total[:, :width].astype(BF16).astype(F32)
-    key_new = total[:, width : 2 * width].astype(BF16).astype(F32)
-    value_new = total[:, 2 * width :].astype(BF16).astype(F32)
+        total = total + part_ref[...].astype(F32)
+    query = (total[:, :width] + total[:, width : 2 * width]).astype(BF16).astype(F32)
+    key_new = total[:, 2 * width : 3 * width].astype(BF16).astype(F32)
+    value_new = total[:, 3 * width :].astype(BF16).astype(F32)
     lanes = lax.broadcasted_iota(jnp.int32, (ROWS, width), 1)
     row_ids = lax.broadcasted_iota(jnp.int32, (ROWS, 1), 0)
     positions = lax.broadcasted_iota(jnp.int32, (ROWS, cache_len), 1)
@@ -334,7 +339,7 @@
     )
     blocks = exchange(blocks, "ep", paired, steps=steps)
     parts = call(
-        project_kernel, "project", 4 * MIB, [shape((count, 3 * width), F32)] * groups
+        project_kernel, "project", 4 * MIB, [shape((count, 4 * width), BF16)] * groups
     )(*blocks, w_query, w_key, w_value)
     parts = exchange(parts, "ep", paired, steps=steps)
     swap = [(one, one ^ 1) for one in range(pieces)]

time: 53.8 us -> 53.6 us (level)
  no operation moved by 1% of the time
where the time goes in v7:
time: 53.6 us; the launch traced here: 53.4 us
  waiting for transfers between devices  17.2 us (32%)
  starting transfers between devices  16.7 us (31%)
  blocking collectives  11.3 us (21%)
  Pallas kernels  7.85 us (15%)
    ppermute x12, starting transfers between devices, exchange(): lax.ppermute(items[index], axis, [(one, one ^ steps[index] * stride) for...  16.5 us
    ppermute x12, waiting for transfers between devices, exchange(): lax.ppermute(items[index], axis, [(one, one ^ steps[index] * stride) for...  13.5 us
    all_to_all x1, blocking collectives, shards(): returned = lax.all_to_all(summed, ('ep', 'tp'), 0, 0, tiled=True)  11.3 us
    pallas_call x1, Pallas kernels, shards(): call(attend_kernel, 'attend', 4 * MIB, [shape(side.shape, F32), side], in...  3.49 us
    ppermute x2, waiting for transfers between devices, shards(): taken = lax.ppermute(give, 'tp', swap)  2.53 us
    pallas_call x1, Pallas kernels, shards(): call(functools.partial(expert_kernel, groups=groups, paired=paired), 'exp...  2.14 us
    ppermute x1, waiting for transfers between devices, shards(): far = lax.ppermute(near, 'tp', swap)  1.19 us
    pallas_call x1, Pallas kernels, shards(): call(functools.partial(norm_kernel, paired=paired, steps=steps), 'norm',...  1.13 us
  transfers between devices with their start and end apart: 15, of which 14 were waited for; matrix products, arithmetic and copies ran while one was open for 0% of the time, Pallas kernels for 0%

profile of v7, /device:TPU:0, one launch (start us, length us, event | category | flops | bytes accessed | tf_op | source)
XLA Modules:
  0.0 53.4 jit_solution(7560455853521174)
XLA Ops:
  0.1 1.1 %norm.1 = (bf16[16,2048]{1,0:T(8,128)(2,1)S(1)}, bf16[16,512]{1,0:T(8,128)(2,1)S(1)}, bf16[16,512]{1,0:T(8,128)(2,1)S(1)}, bf16[16,512]{1,0:T(8,128)(2,1)S(1)}, bf16[16,512]{1,0:T(8,128)(2,1)S(1)}) custom-call(bf16[16,2048]{1,0:T(8,128)(2,1)} %stream_ref.1, f32[1,2048]{1,0:T(1,128)} %bitcast.19), custom_call_target="tpu_custom_call" | custom-call | flops 40000000000 | tf_op jit(solution)/shard_map/norm/pallas_call | solution.py:324
  1.2 4.0 %collective-permute-start = (bf16[16,512]{1,0:T(8,128)(2,1)S(1)}, bf16[16,512]{1,0:T(8,128)(2,1)S(1)}, u32[]{:S(2)}, u32[]{:S(2)}) collective-permute-start(bf16[16,512]{1,0:T(8,128)(2,1)S(1)} %get-tuple-element.22), channel_id=1, source_target_pairs={{0,24},{8,16},{16,8},{24,0},{1,25},{9,17},{17,9},{25,1},{2,26},{10... | collective-permute-start | bytes 49160 | tf_op jit(solution)/shard_map/ppermute | solution.py:43
  5.2 0.5 collective-permute-start.1
  5.9 1.1 %collective-permute-done.refs_1_ = bf16[16,512]{1,0:T(8,128)(2,1)S(1)} collective-permute-done((bf16[16,512]{1,0:T(8,128)(2,1)S(1)}, bf16[16,512]{1,0:T(8,128)(2,1)S(1)}, u32[]{:S(2)}, u32[]{:S(2)}) %collective-permute-start) | collective-permute-done | bytes 16416 | tf_op jit(solution)/shard_map/ppermute | solution.py:43
  7.0 2.0 %collective-permute-done.1.refs_2_ = bf16[16,512]{1,0:T(8,128)(2,1)S(1)} collective-permute-done((bf16[16,512]{1,0:T(8,128)(2,1)S(1)}, bf16[16,512]{1,0:T(8,128)(2,1)S(1)}, u32[]{:S(2)}, u32[]{:S(2)}) %collective-permute-start.1) | collective-permute-done | bytes 16416 | tf_op jit(solution)/shard_map/ppermute | solution.py:43
  9.0 0.5 collective-permute-done.2.refs_3_
  9.8 1.5 %collective-permute-start.3 = (bf16[16,1024]{1,0:T(8,128)(2,1)S(1)}, bf16[16,1024]{1,0:T(8,128)(2,1)S(1)}, u32[]{:S(2)}, u32[]{:S(2)}) collective-permute-start(bf16[16,1024]{1,0:T(8,128)(2,1)S(1)} %get-tuple-element.26), channel_id=1, source_target_pairs={{0,24},{8,16},{16,8},{24,0},{1,25},{9,17},{17,9},{25,1},{2,26},{10... | collective-permute-start | bytes 98312 | tf_op jit(solution)/shard_map/ppermute | solution.py:43
  11.4 1.9 %collective-permute-start.5 = (bf16[16,1024]{1,0:T(8,128)(2,1)S(1)}, bf16[16,1024]{1,0:T(8,128)(2,1)S(1)}, u32[]{:S(2)}, u32[]{:S(2)}) collective-permute-start(bf16[16,1024]{1,0:T(8,128)(2,1)S(1)} %get-tuple-element.28), channel_id=1, source_target_pairs={{0,16},{8,24},{16,0},{24,8},{1,17},{9,25},{17,1},{25,9},{2,18},{10... | collective-permute-start | bytes 98312 | tf_op jit(solution)/shard_map/ppermute | solution.py:43
  13.3 1.3 %collective-permute-done.3.refs_1_ = bf16[16,1024]{1,0:T(8,128)(2,1)S(1)} collective-permute-done((bf16[16,1024]{1,0:T(8,128)(2,1)S(1)}, bf16[16,1024]{1,0:T(8,128)(2,1)S(1)}, u32[]{:S(2)}, u32[]{:S(2)}) %collective-permute-start.3) | collective-permute-done | bytes 32800 | tf_op jit(solution)/shard_map/ppermute | solution.py:43
  15.5 3.5 %attend.1 = (f32[16,1024]{1,0:T(8,128)S(1)}, bf16[16,1024]{1,0:T(8,128)(2,1)S(1)}) custom-call(s32[16]{0:T(128)S(1)} %copy-done.13, bf16[16,2048]{1,0:T(8,128)(2,1)S(1)} %get-tuple-element.20.normed_ref, bf16[16,2048]{1,0:T(8,128)(2,1)S(1)} %bitcast.14, f32[1,16]{1,0:T(1,128)S(1)} %bitcast.18, f32[16,2,1024]{2,1,0:T(2,128)S(1)} %copy-done.7, ...), custom_call_target="tpu_custom_call" | custom-call | tf_op jit(solution)/shard_map/attend/pallas_call | solution.py:347
  19.1 1.2 %collective-permute-done.6.taken_ref = bf16[16,1024]{1,0:T(8,128)(2,1)S(1)} collective-permute-done((bf16[16,1024]{1,0:T(8,128)(2,1)S(1)}, bf16[16,1024]{1,0:T(8,128)(2,1)S(1)}, u32[]{:S(2)}, u32[]{:S(2)}) %collective-permute-start.6) | collective-permute-done | bytes 32800 | tf_op jit(solution)/shard_map/ppermute | solution.py:369
  20.3 4.1 %collective-permute-start.9 = (bf16[16,1024]{1,0:T(8,128)(2,1)S(1)}, bf16[16,1024]{1,0:T(8,128)(2,1)S(1)}, u32[]{:S(2)}, u32[]{:S(2)}) collective-permute-start(bf16[16,1024]{1,0:T(8,128)(2,1)S(1)} %pair.1.refs_0_), channel_id=1, source_target_pairs={{0,6},{1,7},{2,4},{3,5},{4,2},{5,3},{6,0},{7,1},{8,14},{9,15},{10,... | collective-permute-start | bytes 98312 | tf_op jit(solution)/shard_map/ppermute | solution.py:43
  24.3 0.6 %collective-permute-start.7 = (bf16[16,1024]{1,0:T(8,128)(2,1)S(1)}, bf16[16,1024]{1,0:T(8,128)(2,1)S(1)}, u32[]{:S(2)}, u32[]{:S(2)}) collective-permute-start(bf16[16,1024]{1,0:T(8,128)(2,1)S(1)} %pair.1.refs_0_), channel_id=1, source_target_pairs={{0,2},{1,3},{2,0},{3,1},{4,6},{5,7},{6,4},{7,5},{8,10},{9,11},{10,... | collective-permute-start | bytes 98312 | tf_op jit(solution)/shard_map/ppermute | solution.py:43
  25.0 1.3 %collective-permute-done.9.refs_3_ = bf16[16,1024]{1,0:T(8,128)(2,1)S(1)} collective-permute-done((bf16[16,1024]{1,0:T(8,128)(2,1)S(1)}, bf16[16,1024]{1,0:T(8,128)(2,1)S(1)}, u32[]{:S(2)}, u32[]{:S(2)}) %collective-permute-start.9) | collective-permute-done | bytes 32800 | tf_op jit(solution)/shard_map/ppermute | solution.py:43
  26.2 2.9 %collective-permute-done.8.refs_2_ = bf16[16,1024]{1,0:T(8,128)(2,1)S(1)} collective-permute-done((bf16[16,1024]{1,0:T(8,128)(2,1)S(1)}, bf16[16,1024]{1,0:T(8,128)(2,1)S(1)}, u32[]{:S(2)}, u32[]{:S(2)}) %collective-permute-start.8) | collective-permute-done | bytes 32800 | tf_op jit(solution)/shard_map/ppermute | solution.py:43
  29.3 1.2 %collective-permute-done.10.far_ref = bf16[16,1024]{1,0:T(8,128)(2,1)S(1)} collective-permute-done((bf16[16,1024]{1,0:T(8,128)(2,1)S(1)}, bf16[16,1024]{1,0:T(8,128)(2,1)S(1)}, u32[]{:S(2)}, u32[]{:S(2)}) %collective-permute-start.10) | collective-permute-done | bytes 32800 | tf_op jit(solution)/shard_map/ppermute | solution.py:374
  30.6 2.5 %collective-permute-start.13 = (bf16[16,2048]{1,0:T(8,128)(2,1)S(1)}, bf16[16,2048]{1,0:T(8,128)(2,1)S(1)}, u32[]{:S(2)}, u32[]{:S(2)}) collective-permute-start(bf16[16,2048]{1,0:T(8,128)(2,1)S(1)} %get-tuple-element.31.refs_0_), channel_id=1, source_target_pairs={{0,24},{8,16},{16,8},{24,0},{1,25},{9,17},{17,9},{25,1},{2,26},{10... | collective-permute-start | bytes 196616 | tf_op jit(solution)/shard_map/ppermute | solution.py:43
  33.6 0.5 %collective-permute-start.11 = (bf16[16,2048]{1,0:T(8,128)(2,1)S(1)}, bf16[16,2048]{1,0:T(8,128)(2,1)S(1)}, u32[]{:S(2)}, u32[]{:S(2)}) collective-permute-start(bf16[16,2048]{1,0:T(8,128)(2,1)S(1)} %get-tuple-element.31.refs_0_), channel_id=1, source_target_pairs={{0,8},{8,0},{16,24},{24,16},{1,9},{9,1},{17,25},{25,17},{2,10},{10... | collective-permute-start | bytes 196616 | tf_op jit(solution)/shard_map/ppermute | solution.py:43
  34.1 1.7 %collective-permute-done.13.refs_3_ = bf16[16,2048]{1,0:T(8,128)(2,1)S(1)} collective-permute-done((bf16[16,2048]{1,0:T(8,128)(2,1)S(1)}, bf16[16,2048]{1,0:T(8,128)(2,1)S(1)}, u32[]{:S(2)}, u32[]{:S(2)}) %collective-permute-start.13) | collective-permute-done | bytes 65568 | tf_op jit(solution)/shard_map/ppermute | solution.py:43
  35.8 1.5 %collective-permute-done.12.refs_2_ = bf16[16,2048]{1,0:T(8,128)(2,1)S(1)} collective-permute-done((bf16[16,2048]{1,0:T(8,128)(2,1)S(1)}, bf16[16,2048]{1,0:T(8,128)(2,1)S(1)}, u32[]{:S(2)}, u32[]{:S(2)}) %collective-permute-start.12) | collective-permute-done | bytes 65568 | tf_op jit(solution)/shard_map/ppermute | solution.py:43
  37.9 2.1 %experts.1 = (bf16[32,8,256]{2,1,0:T(8,128)(2,1)S(1)}, bf16[32,8,256]{2,1,0:T(8,128)(2,1)S(1)}) custom-call(s32[2,64]{1,0:T(2,128)S(1)} %bitcast.16, f32[2,64]{1,0:T(2,128)S(1)} %bitcast.17, bf16[1,704,2048]{2,1,0:T(8,128)(2,1)S(1)} %bitcast.12, bf16[1,704,2048]{2,1,0:T(8,128)(2,1)S(1)} %bitcast.13, bf16[1,704,2048]{2,1,0:T(8,128)(2,1)S(1)} %copy-done.2, ...), custom_call_target="tpu_custom_call" | custom-call | tf_op jit(solution)/shard_map/experts/pallas_call | solution.py:384
  40.1 1.3 %collective-permute-done.14.taken_ref = bf16[32,8,256]{2,1,0:T(8,128)(2,1)S(1)} collective-permute-done((bf16[32,8,256]{2,1,0:T(8,128)(2,1)S(1)}, bf16[32,8,256]{2,1,0:T(8,128)(2,1)S(1)}, u32[]{:S(2)}, u32[]{:S(2)}) %collective-permute-start.14) | collective-permute-done | bytes 131104 | tf_op jit(solution)/shard_map/ppermute | solution.py:397
  41.5 11.3 %all_to_all.5.parts_ref = bf16[32,8,256]{2,1,0:T(8,128)(2,1)S(1)} all-to-all(bf16[32,8,256]{2,1,0:T(8,128)(2,1)S(1)} %sides.1), channel_id=1, replica_groups=mesh['ep'=4,'tp'=8] {'ep','tp'}, dimensions={0} | all-to-all | bytes 262144 | tf_op jit(solution)/shard_map/all_to_all | solution.py:399
  52.8 0.6 %finish.1 = bf16[16,256]{1,0:T(8,128)(2,1)} custom-call(bf16[32,8,256]{2,1,0:T(8,128)(2,1)S(1)} %all_to_all.5.parts_ref, bf16[16,256]{1,0:T(8,128)(2,1)S(1)} %get-tuple-element.34.mixed_ref), custom_call_target="tpu_custom_call" | custom-call | tf_op jit(solution)/shard_map/finish/pallas_call | solution.py:400
  (56 shorter events, 2.7 us)
Async XLA Ops:
  0.0 15.3 %slice-start = ((s8[8388608]{0:T(1024)(128)(4,1)}), s8[4194304]{0:T(1024)(128)(4,1)S(1)}, s32[]{:S(2)}) async-start(s8[8388608]{0:T(1024)(128)(4,1)} %bitcast.8), calls=%async_computation.1 | async-start | bytes 8388608
  0.0 15.3 %slice-start.2 = ((s8[8388608]{0:T(1024)(128)(4,1)}), s8[4194304]{0:T(1024)(128)(4,1)S(1)}, s32[]{:S(2)}) async-start(s8[8388608]{0:T(1024)(128)(4,1)} %bitcast.10), calls=%async_computation.3 | async-start | bytes 8388608
  0.0 15.3 %slice-start.1 = ((s8[8388608]{0:T(1024)(128)(4,1)}), s8[4194304]{0:T(1024)(128)(4,1)S(1)}, s32[]{:S(2)}) async-start(s8[8388608]{0:T(1024)(128)(4,1)} %bitcast.8), calls=%async_computation.2 | async-start | bytes 8388608
  0.0 15.3 %slice-start.3 = ((s8[8388608]{0:T(1024)(128)(4,1)}), s8[4194304]{0:T(1024)(128)(4,1)S(1)}, s32[]{:S(2)}) async-start(s8[8388608]{0:T(1024)(128)(4,1)} %bitcast.10), calls=%async_computation.4 | async-start | bytes 8388608
  1.2 5.7 %collective-permute-start = (bf16[16,512]{1,0:T(8,128)(2,1)S(1)}, bf16[16,512]{1,0:T(8,128)(2,1)S(1)}, u32[]{:S(2)}, u32[]{:S(2)}) collective-permute-start(bf16[16,512]{1,0:T(8,128)(2,1)S(1)} %get-tuple-element.22), channel_id=1, source_target_pairs={{0,24},{8,16},{16,8},{24,0},{1,25},{9,17},{17,9},{25,1},{2,26},{10... | collective-permute-start | bytes 49160 | tf_op jit(solution)/shard_map/ppermute | solution.py:43
  5.2 3.7 %collective-permute-start.1 = (bf16[16,512]{1,0:T(8,128)(2,1)S(1)}, bf16[16,512]{1,0:T(8,128)(2,1)S(1)}, u32[]{:S(2)}, u32[]{:S(2)}) collective-permute-start(bf16[16,512]{1,0:T(8,128)(2,1)S(1)} %get-tuple-element.23), channel_id=1, source_target_pairs={{0,8},{8,0},{16,24},{24,16},{1,9},{9,1},{17,25},{25,17},{2,10},{10... | collective-permute-start | bytes 49160 | tf_op jit(solution)/shard_map/ppermute | solution.py:43
  5.8 3.7 %collective-permute-start.2 = (bf16[16,512]{1,0:T(8,128)(2,1)S(1)}, bf16[16,512]{1,0:T(8,128)(2,1)S(1)}, u32[]{:S(2)}, u32[]{:S(2)}) collective-permute-start(bf16[16,512]{1,0:T(8,128)(2,1)S(1)} %get-tuple-element.24), channel_id=1, source_target_pairs={{0,16},{8,24},{16,0},{24,8},{1,17},{9,25},{17,1},{25,9},{2,18},{10... | collective-permute-start | bytes 49160 | tf_op jit(solution)/shard_map/ppermute | solution.py:43
  9.8 4.9 %collective-permute-start.3 = (bf16[16,1024]{1,0:T(8,128)(2,1)S(1)}, bf16[16,1024]{1,0:T(8,128)(2,1)S(1)}, u32[]{:S(2)}, u32[]{:S(2)}) collective-permute-start(bf16[16,1024]{1,0:T(8,128)(2,1)S(1)} %get-tuple-element.26), channel_id=1, source_target_pairs={{0,24},{8,16},{16,8},{24,0},{1,25},{9,17},{17,9},{25,1},{2,26},{10... | collective-permute-start | bytes 98312 | tf_op jit(solution)/shard_map/ppermute | solution.py:43
  11.3 3.9 %collective-permute-start.4 = (bf16[16,1024]{1,0:T(8,128)(2,1)S(1)}, bf16[16,1024]{1,0:T(8,128)(2,1)S(1)}, u32[]{:S(2)}, u32[]{:S(2)}) collective-permute-start(bf16[16,1024]{1,0:T(8,128)(2,1)S(1)} %get-tuple-element.27), channel_id=1, source_target_pairs={{0,8},{8,0},{16,24},{24,16},{1,9},{9,1},{17,25},{25,17},{2,10},{10... | collective-permute-start | bytes 98312 | tf_op jit(solution)/shard_map/ppermute | solution.py:43
  11.4 3.9 %collective-permute-start.5 = (bf16[16,1024]{1,0:T(8,128)(2,1)S(1)}, bf16[16,1024]{1,0:T(8,128)(2,1)S(1)}, u32[]{:S(2)}, u32[]{:S(2)}) collective-permute-start(bf16[16,1024]{1,0:T(8,128)(2,1)S(1)} %get-tuple-element.28), channel_id=1, source_target_pairs={{0,16},{8,24},{16,0},{24,8},{1,17},{9,25},{17,1},{25,9},{2,18},{10... | collective-permute-start | bytes 98312 | tf_op jit(solution)/shard_map/ppermute | solution.py:43
  15.4 22.4 %copy-start = (bf16[1,2048,704]{1,2,0:T(8,128)(2,1)S(1)}, bf16[1,2048,704]{1,2,0:T(8,128)(2,1)}, u32[]{:S(2)}) copy-start(bf16[1,2048,704]{1,2,0:T(8,128)(2,1)} %param.33) | copy-start | bytes 8650756
  15.5 22.4 %copy-start.1 = (bf16[1,2048,704]{1,2,0:T(8,128)(2,1)S(1)}, bf16[1,2048,704]{1,2,0:T(8,128)(2,1)}, u32[]{:S(2)}) copy-start(bf16[1,2048,704]{1,2,0:T(8,128)(2,1)} %param.34) | copy-start | bytes 8650756
  15.5 22.4 %copy-start.2 = (bf16[1,704,2048]{2,1,0:T(8,128)(2,1)S(1)}, bf16[1,704,2048]{2,1,0:T(8,128)(2,1)}, u32[]{:S(2)}) copy-start(bf16[1,704,2048]{2,1,0:T(8,128)(2,1)} %down_ref.1) | copy-start | bytes 8650756
  15.5 22.4 %copy-start.11 = (s32[64,2]{0,1:T(2,128)S(1)}, s32[64,2]{0,1:T(2,128)}, u32[]{:S(2)}) copy-start(s32[64,2]{0,1:T(2,128)} %param.31) | copy-start | bytes 1540
  15.5 22.4 %copy-start.12 = (f32[64,2]{0,1:T(2,128)S(1)}, f32[64,2]{0,1:T(2,128)}, u32[]{:S(2)}) copy-start(f32[64,2]{0,1:T(2,128)} %param.32) | copy-start | bytes 1540
  19.0 1.3 %collective-permute-start.6 = (bf16[16,1024]{1,0:T(8,128)(2,1)S(1)}, bf16[16,1024]{1,0:T(8,128)(2,1)S(1)}, u32[]{:S(2)}, u32[]{:S(2)}) collective-permute-start(bf16[16,1024]{1,0:T(8,128)(2,1)S(1)} %get-tuple-element.30), channel_id=1, source_target_pairs={{0,1},{1,0},{2,3},{3,2},{4,5},{5,4},{6,7},{7,6},{8,9},{9,8},{10,11... | collective-permute-start | bytes 98312 | tf_op jit(solution)/shard_map/ppermute | solution.py:369
  20.3 6.0 %collective-permute-start.9 = (bf16[16,1024]{1,0:T(8,128)(2,1)S(1)}, bf16[16,1024]{1,0:T(8,128)(2,1)S(1)}, u32[]{:S(2)}, u32[]{:S(2)}) collective-permute-start(bf16[16,1024]{1,0:T(8,128)(2,1)S(1)} %pair.1.refs_0_), channel_id=1, source_target_pairs={{0,6},{1,7},{2,4},{3,5},{4,2},{5,3},{6,0},{7,1},{8,14},{9,15},{10,... | collective-permute-start | bytes 98312 | tf_op jit(solution)/shard_map/ppermute | solution.py:43
  24.3 4.8 %collective-permute-start.8 = (bf16[16,1024]{1,0:T(8,128)(2,1)S(1)}, bf16[16,1024]{1,0:T(8,128)(2,1)S(1)}, u32[]{:S(2)}, u32[]{:S(2)}) collective-permute-start(bf16[16,1024]{1,0:T(8,128)(2,1)S(1)} %pair.1.refs_0_), channel_id=1, source_target_pairs={{0,4},{1,5},{2,6},{3,7},{4,0},{5,1},{6,2},{7,3},{8,12},{9,13},{10,... | collective-permute-start | bytes 98312 | tf_op jit(solution)/shard_map/ppermute | solution.py:43
  24.3 4.8 %collective-permute-start.7 = (bf16[16,1024]{1,0:T(8,128)(2,1)S(1)}, bf16[16,1024]{1,0:T(8,128)(2,1)S(1)}, u32[]{:S(2)}, u32[]{:S(2)}) collective-permute-start(bf16[16,1024]{1,0:T(8,128)(2,1)S(1)} %pair.1.refs_0_), channel_id=1, source_target_pairs={{0,2},{1,3},{2,0},{3,1},{4,6},{5,7},{6,4},{7,5},{8,10},{9,11},{10,... | collective-permute-start | bytes 98312 | tf_op jit(solution)/shard_map/ppermute | solution.py:43
  29.2 1.3 %collective-permute-start.10 = (bf16[16,1024]{1,0:T(8,128)(2,1)S(1)}, bf16[16,1024]{1,0:T(8,128)(2,1)S(1)}, u32[]{:S(2)}, u32[]{:S(2)}) collective-permute-start(bf16[16,1024]{1,0:T(8,128)(2,1)S(1)} %mix.1.near_ref), channel_id=1, source_target_pairs={{0,1},{1,0},{2,3},{3,2},{4,5},{5,4},{6,7},{7,6},{8,9},{9,8},{10,11... | collective-permute-start | bytes 98312 | tf_op jit(solution)/shard_map/ppermute | solution.py:374
  30.6 5.3 %collective-permute-start.13 = (bf16[16,2048]{1,0:T(8,128)(2,1)S(1)}, bf16[16,2048]{1,0:T(8,128)(2,1)S(1)}, u32[]{:S(2)}, u32[]{:S(2)}) collective-permute-start(bf16[16,2048]{1,0:T(8,128)(2,1)S(1)} %get-tuple-element.31.refs_0_), channel_id=1, source_target_pairs={{0,24},{8,16},{16,8},{24,0},{1,25},{9,17},{17,9},{25,1},{2,26},{10... | collective-permute-start | bytes 196616 | tf_op jit(solution)/shard_map/ppermute | solution.py:43
  33.1 4.3 %collective-permute-start.12 = (bf16[16,2048]{1,0:T(8,128)(2,1)S(1)}, bf16[16,2048]{1,0:T(8,128)(2,1)S(1)}, u32[]{:S(2)}, u32[]{:S(2)}) collective-permute-start(bf16[16,2048]{1,0:T(8,128)(2,1)S(1)} %get-tuple-element.31.refs_0_), channel_id=1, source_target_pairs={{0,16},{8,24},{16,0},{24,8},{1,17},{9,25},{17,1},{25,9},{2,18},{10... | collective-permute-start | bytes 196616 | tf_op jit(solution)/shard_map/ppermute | solution.py:43
  33.6 4.3 %collective-permute-start.11 = (bf16[16,2048]{1,0:T(8,128)(2,1)S(1)}, bf16[16,2048]{1,0:T(8,128)(2,1)S(1)}, u32[]{:S(2)}, u32[]{:S(2)}) collective-permute-start(bf16[16,2048]{1,0:T(8,128)(2,1)S(1)} %get-tuple-element.31.refs_0_), channel_id=1, source_target_pairs={{0,8},{8,0},{16,24},{24,16},{1,9},{9,1},{17,25},{25,17},{2,10},{10... | collective-permute-start | bytes 196616 | tf_op jit(solution)/shard_map/ppermute | solution.py:43
  40.1 1.4 %collective-permute-start.14 = (bf16[32,8,256]{2,1,0:T(8,128)(2,1)S(1)}, bf16[32,8,256]{2,1,0:T(8,128)(2,1)S(1)}, u32[]{:S(2)}, u32[]{:S(2)}) collective-permute-start(bf16[32,8,256]{2,1,0:T(8,128)(2,1)S(1)} %get-tuple-element.33), channel_id=1, source_target_pairs={{0,1},{1,0},{2,3},{3,2},{4,5},{5,4},{6,7},{7,6},{8,9},{9,8},{10,11... | collective-permute-start | bytes 393224 | tf_op jit(solution)/shard_map/ppermute | solution.py:397
  (10 other events, 133.9 us)
